TPU v7x, 32 devices: a whole 2x2x4 slice. The times are simulated.
32 devices in a mesh: sp: 4 (over z), fs: 4 (over y, x), tp: 2 (over core).
Axes of the slice: x: 2, y: 2, z: 4, core: 2. Of those that a mesh axis runs over, the one named last changes fastest.
Arguments:
- tokens: bfloat16 [4, 512, 2048], P('fs', ('sp', 'tp')), may hold values from -6 to 6
- input_norm_gain: float32 [2048], replicated, may hold values from 0.1 to 1.9
- pooling_input_weight: bfloat16 [2048, 1024], P('sp', 'tp'), may hold values from -0.125 to 0.125
- query_weight: bfloat16 [2048, 1024], P('sp', 'tp'), may hold values from -0.125 to 0.125
- forget_weight: bfloat16 [2048, 1024], P('sp', 'tp'), may hold values from -0.125 to 0.125
- value_weight: bfloat16 [2048, 1024], P('sp', 'tp'), may hold values from -0.125 to 0.125
- pooling_group_maps: bfloat16 [4, 256, 256], P('tp'), may hold values from -0.375 to 0.375
- pooling_scale: float32 [1024], P('tp'), may hold values from 0.1 to 1.9
- lower_bound_logits: float32 [1024], P('tp')
- decay_spike: float32 [4, 512, 8], P('fs', 'sp', 'tp'), may hold values from -0.75 to 0
- head_norm_gain: float32 [1024], P('tp'), may hold values from 0.1 to 1.9
- pooling_output_weight: bfloat16 [1024, 2048], P('tp', 'sp'), may hold values from -0.125 to 0.125
- recurrent_output_weight: bfloat16 [1024, 2048], P('tp', 'sp'), may hold values from -0.125 to 0.125
Outputs:
- mixed: bfloat16 [4, 512, 2048], P('fs', ('sp', 'tp'))
All inputs are finite; a program needn't handle non-finite values.
Results may differ from a plain program's by a relative error of at most 0.013.
Values may be sent and summed in bfloat16 or wider, within the bound.
No kernel may reach another device: no remote copies, remote signals or barrier semaphores. Data moves between devices by JAX's collectives and lax.ppermute only.
A program may use at most 64 MiB of HBM per device.

v0:
```python
import jax
import jax.numpy as jnp
from jax import lax
from jax.sharding import PartitionSpec as P

BLOCK = 64


EPSILON = 1e-06
HIGHEST = lax.Precision.HIGHEST


def shifted(value, axis, steps):
    count = lax.axis_size(axis)
    first, last = (max(0, -steps), min(count, count - steps))
    return lax.ppermute(value, axis, [(source, source + steps) for source in range(first, last)])


def entering(shard, axis, join, neutral):
    place = lax.axis_index(axis)
    gathered = jax.tree.map(
        lambda a, kind: lax.all_gather(a.astype(kind), axis), shard, (jnp.bfloat16, jnp.bfloat16)
    )
    state = jax.tree.map(lambda a, e: jnp.zeros_like(a) + jnp.asarray(e, a.dtype), shard, neutral)

    def one(step, state):
        return join(
            state,
            jax.tree.map(
                lambda a, own: lax.dynamic_index_in_dim(a, step, 0, False).astype(own.dtype),
                gathered,
                shard,
            ),
        )

    return lax.fori_loop(0, place, one, state)


def rms_scale(values, gain):
    return values * lax.rsqrt(jnp.mean(values * values, axis=-1, keepdims=True) + EPSILON) * gain


def join_state(earlier, later):
    decay_one, state_one = earlier
    decay_two, state_two = later
    return (decay_one * decay_two, decay_two[..., None] * state_one + state_two)


def body(
    tokens,
    input_norm_gain,
    pooling_input_weight,
    query_weight,
    forget_weight,
    value_weight,
    pooling_group_maps,
    pooling_scale,
    lower_bound_logits,
    decay_spike,
    head_norm_gain,
    pooling_output_weight,
    recurrent_output_weight,
):
    gathered = lax.all_gather(tokens, "tp", axis=1, tiled=True)[0]
    length_total = gathered.shape[0]
    normed = rms_scale(gathered.astype(jnp.float32), input_norm_gain).astype(jnp.bfloat16)
    pool_width = pooling_input_weight.shape[1]
    rec_width = query_weight.shape[1]
    stacked = jnp.concatenate(
        [pooling_input_weight, query_weight, forget_weight, value_weight], axis=1
    )
    out_local = jnp.concatenate([pooling_output_weight, recurrent_output_weight], axis=0)
    groups_fs = lax.axis_size("fs")
    member = lax.axis_index("fs")
    slice_width = stacked.shape[1] // groups_fs
    own_slice = lax.dynamic_slice_in_dim(stacked, member * slice_width, slice_width, 1)
    column_part = lax.all_gather(own_slice, "sp", axis=0, tiled=True)
    full_input = lax.all_gather(column_part, "fs", axis=1, tiled=True)
    projected = jnp.dot(normed, full_input, preferred_element_type=jnp.float32)
    slice_height = out_local.shape[0] // groups_fs
    own_rows = lax.dynamic_slice_in_dim(out_local, member * slice_height, slice_height, 0)
    row_part = lax.all_gather(own_rows, "sp", axis=1, tiled=True)
    out_full = lax.all_gather(row_part, "fs", axis=0, tiled=True)
    rounded = lax.optimization_barrier(projected.astype(jnp.bfloat16))
    pool_input = rounded[:, :pool_width]
    query_matrix = rounded[:, pool_width : pool_width + rec_width].astype(jnp.float32)
    forget_gate_logit = rounded[:, pool_width + rec_width : pool_width + 2 * rec_width].astype(
        jnp.float32
    )
    value_projected = rounded[:, pool_width + 2 * rec_width :].astype(jnp.float32)
    groups_local = pooling_group_maps.shape[0]
    group_size = pooling_group_maps.shape[1]
    reach_rows = 2 ** (groups_local * lax.axis_size("tp"))
    previous = shifted(pool_input[length_total - reach_rows :], "sp", 1)
    extended = jnp.concatenate([previous, pool_input], axis=0).astype(jnp.float32)
    extended = extended.reshape(reach_rows + length_total, groups_local, group_size)
    group_ids = lax.axis_index("tp") * groups_local + jnp.arange(groups_local, dtype=jnp.int32)
    windows = jnp.left_shift(jnp.int32(2), group_ids)
    window_sum = jnp.zeros((length_total, groups_local, group_size), jnp.float32)
    for offset in range(reach_rows):
        inside = (offset < windows).astype(jnp.float32)
        window_sum = (
            window_sum
            + extended[reach_rows - offset : reach_rows - offset + length_total] * inside[:, None]
        )
    position_index = lax.axis_index("sp") * length_total + jnp.arange(length_total, dtype=jnp.int32)
    counts = jnp.minimum(position_index[:, None] + 1, windows[None, :]).astype(jnp.float32)
    pool_diff = (window_sum / counts[:, :, None] - extended[reach_rows:]).astype(jnp.bfloat16)
    pool_mapped = jnp.einsum(
        "tgc,gcd->tgd", pool_diff, pooling_group_maps, preferred_element_type=jnp.float32
    )
    pool_out = (pool_mapped.reshape(length_total, pool_width) * pooling_scale).astype(jnp.bfloat16)
    local_heads = decay_spike.shape[2]
    head_width = rec_width // local_heads
    blocks = length_total // BLOCK
    block_layout = (blocks, BLOCK, local_heads, head_width)
    reader = jax.nn.silu(query_matrix).reshape(block_layout)
    key_gate_value = jax.nn.sigmoid(-lower_bound_logits) * jax.nn.sigmoid(-forget_gate_logit)
    decay_logarithm = (
        jnp.log1p(-key_gate_value).reshape(length_total, local_heads, head_width)
        + decay_spike[0][:, :, None]
    ).reshape(block_layout)
    key_rows = key_gate_value.reshape(block_layout)
    value_rows = value_projected.reshape(block_layout)
    inner_log = jnp.cumsum(decay_logarithm, axis=1)
    read_scaled = reader * jnp.exp(inner_log)
    key_scaled = key_rows * jnp.exp(-inner_log)
    causal = (jnp.arange(BLOCK)[:, None] >= jnp.arange(BLOCK)[None, :]).astype(jnp.float32)
    scores = jnp.einsum("nthd,nshd->nhts", read_scaled, key_scaled, precision=HIGHEST) * causal
    within = jnp.einsum("nhts,nshe->nthe", scores, value_rows, precision=HIGHEST)
    closing = inner_log[:, -1]
    key_tail = key_rows * jnp.exp(closing[:, None] - inner_log)
    deltas = jnp.einsum("nshd,nshe->nhde", key_tail, value_rows, precision=HIGHEST)
    block_decay = jnp.exp(closing)

    def advance(carried, input_batch):
        decay_now, delta_now = input_batch
        return (decay_now[..., None] * carried + delta_now, carried)

    initial = jnp.zeros((local_heads, head_width, head_width), jnp.float32)
    device_state, entry_states = lax.scan(advance, initial, (block_decay, deltas))
    device_decay = jnp.exp(jnp.sum(closing, axis=0))
    scanned = entering(
        (device_decay, device_state),
        "sp",
        join_state,
        (jnp.ones_like(device_decay), jnp.zeros_like(device_state)),
    )
    prior_state = scanned[1]
    before = jnp.cumsum(closing, axis=0) - closing
    start_states = entry_states + jnp.exp(before)[..., None] * prior_state[None]
    read_out = within + jnp.einsum("nthd,nhde->nthe", read_scaled, start_states, precision=HIGHEST)
    read_out = read_out.reshape(length_total, local_heads, head_width)
    recurrent_output = (
        rms_scale(read_out, 1.0).reshape(length_total, rec_width) * head_norm_gain
    ).astype(jnp.bfloat16)
    mixed_rows = jnp.concatenate([pool_out, recurrent_output], axis=1)
    summed = lax.psum_scatter(
        jnp.dot(mixed_rows, out_full, preferred_element_type=jnp.float32).astype(jnp.bfloat16),
        "tp",
        scatter_dimension=0,
        tiled=True,
    )
    return summed[None]


def solution(mesh):
    placed = (
        P("fs", ("sp", "tp"), None),
        P(),
        P("sp", "tp"),
        P("sp", "tp"),
        P("sp", "tp"),
        P("sp", "tp"),
        P("tp", None, None),
        P("tp"),
        P("tp"),
        P("fs", "sp", "tp"),
        P("tp"),
        P("tp", "sp"),
        P("tp", "sp"),
    )
    return jax.shard_map(
        body, mesh=mesh, in_specs=placed, out_specs=P("fs", ("sp", "tp"), None), check_vma=False
    )
```

profile of v0, /device:TPU:0, one launch (start us, length us, event | category | flops | bytes accessed | tf_op | source)
XLA Modules:
  0.0 247.2 jit_solution(11630460486678041191)
XLA Ops:
  6.6 2.3 fusion.8
  9.0 1.8 fusion.17
  10.9 46.6 %all-gather.8.cloned.1.call-done = bf16[2048,512]{1,0:T(8,128)(2,1)} async-done(((bf16[512,512]{1,0:T(8,128)(2,1)}), bf16[2048,512]{1,0:T(8,128)(2,1)}) %all-gather.8.cloned.1.call-update) | async-done | bytes 2097168 | tf_op jit(solution)/shard_map/all_gather | solution.py:77
  57.6 0.1 copy.116
  57.9 2.2 all_gather.25
  60.1 0.2 fusion.2
  60.3 25.6 %all-gather.12.cloned.1.call-done = bf16[256,2048]{1,0:T(8,128)(2,1)} async-done(((bf16[256,512]{1,0:T(8,128)(2,1)}), bf16[256,2048]{1,0:T(8,128)(2,1)}) %all-gather.12.cloned.1.call-update) | async-done | bytes 1048592 | tf_op jit(solution)/shard_map/all_gather | solution.py:82
  86.0 88.5 %all-gather.10.cloned.1.call-done = bf16[2048,2048]{1,0:T(8,128)(2,1)} async-done(((bf16[2048,512]{1,0:T(8,128)(2,1)}), bf16[2048,2048]{1,0:T(8,128)(2,1)}) %all-gather.10.cloned.1.call-update) | async-done | bytes 8388624 | tf_op jit(solution)/shard_map/all_gather | solution.py:78
  174.5 4.7 %convolution_convert_fusion = bf16[128,2048]{1,0:T(8,128)(2,1)S(1)} fusion(bf16[2048,2048]{1,0:T(8,128)(2,1)} %all-gather.10.cloned.1.call-done, bf16[1,128,2048]{2,1,0:T(8,128)(2,1)S(1)} %all_gather.25, f32[2048]{0:T(1024)S(1)} %copy-done.2, f32[128]{0:T(128)S(1)} %add_rsqrt_fusion.1), kind=kOutput, calls=%fused_computation.5 | convolution fusion | flops 1075052544 | bytes 9445888 | tf_op jit(solution)/shard_map/dot_general | solution.py:79
  179.2 3.4 %collective-permute-start = (bf16[16,512]{1,0:T(8,128)(2,1)S(1)}, bf16[16,512]{1,0:T(8,128)(2,1)S(1)}, u32[]{:S(2)}, u32[]{:S(2)}) collective-permute-start(bf16[16,512]{1,0:T(8,128)(2,1)S(1)} %slice.154), channel_id=1, source_target_pairs={{0,8},{8,16},{16,24},{1,9},{9,17},{17,25},{2,10},{10,18},{18,26},{... | collective-permute-start | bytes 49160 | tf_op jit(solution)/shard_map/ppermute | solution.py:16
  182.6 0.2 negate_log-plus-one_fusion
  183.2 0.2 fusion.46
  183.4 0.2 exponential_multiply_fusion
  183.6 0.6 fusion.41
  184.2 0.5 while.26
  184.3 0.2 bitcast_add_fusion.2
  184.5 0.2 bitcast_add_fusion.2
  184.8 9.1 %all-gather.2 = bf16[4,4,128]{2,1,0:T(4,128)(2,1)S(1)} all-gather(bf16[1,4,128]{2,1,0:T(4,128)(2,1)S(1)} %fusion.57), channel_id=2, replica_groups=mesh['sp'=4,'fs'=4,'tp'=2] {'sp'}, dimensions={0}, use_global_device_ids=true | all-gather | bytes 5120 | tf_op jit(solution)/shard_map/all_gather | solution.py:22
  193.8 14.9 %all-gather.1 = bf16[16,128,128]{2,1,0:T(8,128)(2,1)S(1)} all-gather(bf16[4,128,128]{2,1,0:T(8,128)(2,1)S(1)} %convert_element_type.223), channel_id=3, replica_groups=mesh['sp'=4,'fs'=4,'tp'=2] {'sp'}, dimensions={0}, use_global_device_ids=true | all-gather | bytes 655360 | tf_op jit(solution)/shard_map/all_gather | solution.py:22
  208.7 0.5 convolution_multiply_fusion
  209.3 0.3 fusion.54
  209.6 0.8 multiply_reduce_fusion
  210.4 0.3 copy.117
  210.7 0.3 reshape.244
  211.1 0.1 fusion.39
  211.3 0.5 fusion.61
  211.8 0.5 convolution_bitcast_fusion
  212.3 0.1 copy.105
  212.4 0.1 fusion.40
  212.6 16.2 %all-gather.14.cloned.1.call-done = bf16[1024,2048]{1,0:T(8,128)(2,1)} async-done(((bf16[256,2048]{1,0:T(8,128)(2,1)}), bf16[1024,2048]{1,0:T(8,128)(2,1)}) %all-gather.14.cloned.1.call-update) | async-done | bytes 4194320 | tf_op jit(solution)/shard_map/all_gather | solution.py:83
  228.8 3.7 %convolution_convert_fusion.1 = bf16[128,2048]{1,0:T(8,128)(2,1)} fusion(bf16[1024,2048]{1,0:T(8,128)(2,1)} %all-gather.14.cloned.1.call-done, bf16[128,512]{0,1:T(8,128)(2,1)S(1)} %fusion.39, bf16[128,512]{0,1:T(8,128)(2,1)S(1)} %fusion.40), kind=kOutput, calls=%fused_computation.6 | convolution fusion | flops 537657344 | bytes 4980736 | tf_op jit(solution)/shard_map/dot_general | solution.py:159
  232.5 8.1 %reduce-scatter.2.cloned.1.call-done = bf16[64,2048]{1,0:T(8,128)(2,1)} async-done(((bf16[128,2048]{1,0:T(8,128)(2,1)}), bf16[64,2048]{1,0:T(8,128)(2,1)}) %reduce-scatter.2.cloned.1.call-update) | async-done | bytes 262160 | tf_op jit(solution)/shard_map/reduce_scatter | solution.py:158
  (62 shorter events, 1.1 us)
Async XLA Ops:
  6.5 205.2 %copy-start = (bf16[2,256,256]{2,1,0:T(8,128)(2,1)S(1)}, bf16[2,256,256]{2,1,0:T(8,128)(2,1)}, u32[]{:S(2)}) copy-start(bf16[2,256,256]{2,1,0:T(8,128)(2,1)} %param.23) | copy-start | bytes 786436
  6.5 51.1 %copy-start.5 = (f32[1,128,4]{1,2,0:T(4,128)S(1)}, f32[1,128,4]{1,2,0:T(4,128)}, u32[]{:S(2)}) copy-start(f32[1,128,4]{1,2,0:T(4,128)} %param.26) | copy-start | bytes 6148
  6.5 51.3 %copy-start.1 = (bf16[1,64,2048]{2,1,0:T(8,128)(2,1)S(1)}, bf16[1,64,2048]{2,1,0:T(8,128)(2,1)}, u32[]{:S(2)}) copy-start(bf16[1,64,2048]{2,1,0:T(8,128)(2,1)} %param.17) | copy-start | bytes 786436
  6.5 53.8 %copy-start.6 = (f32[512]{0:T(512)S(1)}, f32[512]{0:T(512)}, u32[]{:S(2)}) copy-start(f32[512]{0:T(512)} %param.25) | copy-start | bytes 6148
  6.5 51.0 %all-gather.8.cloned.1.call-start = ((), (), s32[]{:S(2)}) async-start(), calls=%async_computation.1 | async-start | bytes 2621440 | tf_op jit(solution)/shard_map/all_gather | solution.py:77
  6.6 167.9 %copy-start.2 = (f32[2048]{0:T(1024)S(1)}, f32[2048]{0:T(1024)}, u32[]{:S(2)}) copy-start(f32[2048]{0:T(1024)} %param.18) | copy-start | bytes 24580
  8.9 77.0 %all-gather.12.cloned.1.call-start = ((), (), s32[]{:S(2)}) async-start(), calls=%async_computation.3 | async-start | bytes 1310720 | tf_op jit(solution)/shard_map/all_gather | solution.py:82
  10.9 163.6 %all-gather.10.cloned.1.call-start = ((), (), s32[]{:S(2)}) async-start(), calls=%async_computation.2 | async-start | bytes 10485760 | tf_op jit(solution)/shard_map/all_gather | solution.py:78
  57.5 171.3 %all-gather.14.cloned.1.call-start = ((), (), s32[]{:S(2)}) async-start(), calls=%async_computation.4 | async-start | bytes 5242880 | tf_op jit(solution)/shard_map/all_gather | solution.py:83
  85.9 154.7 %reduce-scatter.2.cloned.1.call-start = ((), (), s32[]{:S(2)}) async-start(), calls=%async_computation.5 | async-start | bytes 786432 | tf_op jit(solution)/shard_map/reduce_scatter | solution.py:158
  179.2 32.0 %collective-permute-start = (bf16[16,512]{1,0:T(8,128)(2,1)S(1)}, bf16[16,512]{1,0:T(8,128)(2,1)S(1)}, u32[]{:S(2)}, u32[]{:S(2)}) collective-permute-start(bf16[16,512]{1,0:T(8,128)(2,1)S(1)} %slice.154), channel_id=1, source_target_pairs={{0,8},{8,16},{16,24},{1,9},{9,17},{17,25},{2,10},{10,18},{18,26},{... | collective-permute-start | bytes 49160 | tf_op jit(solution)/shard_map/ppermute | solution.py:16
  208.7 2.4 copy-start.3
  211.8 0.7 copy-start.4
Sparse Core Ops, SparseCore 0:
  9.1 48.4 all-gather.7
  59.1 26.7 all-gather.11
  87.7 86.7 all-gather.9
  176.2 52.5 all-gather.13
  232.7 7.9 reduce-scatter.1
where the time goes:
time: 247 us
  waiting for transfers between devices  185 us (75%)
  blocking collectives  26.1 us (11%)
  between operations  13.5 us (5%)
  matrix products  11.1 us (4%)
  other arithmetic  5.86 us (2%)
  starting transfers between devices  3.58 us (1%)
    all_gather x1, waiting for transfers between devices, body(): full_input = lax.all_gather(column_part, 'fs', axis=1, tiled=True)  88.5 us
    all_gather x1, waiting for transfers between devices, body(): column_part = lax.all_gather(own_slice, 'sp', axis=0, tiled=True)  46.6 us
    all_gather x1, waiting for transfers between devices, body(): row_part = lax.all_gather(own_rows, 'sp', axis=1, tiled=True)  25.6 us
    all_gather x2, blocking collectives, entering(): lax.all_gather(a.astype(kind), axis)  23.9 us
    all_gather x1, waiting for transfers between devices, body(): out_full = lax.all_gather(row_part, 'fs', axis=0, tiled=True)  16.2 us
    reduce_scatter x1, waiting for transfers between devices, body(): lax.psum_scatter(jnp.dot(mixed_rows, out_full, preferred_element_type=jnp...  8.08 us
  transfers between devices with their start and end apart: 6, of which 5 were waited for; matrix products, arithmetic and copies ran while one was open for 5% of the time, Pallas kernels for 0%

commit v1 on v0

--- a/solution.py
+++ b/solution.py
@@ -46,7 +46,241 @@
     return (decay_one * decay_two, decay_two[..., None] * state_one + state_two)
 
 
-def body(
+def swapped(value, axis, bits):
+    count = lax.axis_size(axis)
+    return lax.ppermute(value, axis, [(source, source ^ bits) for source in range(count)])
+
+
+def turned(value, axis, steps):
+    count = lax.axis_size(axis)
+    return lax.ppermute(value, axis, [(source, (source + steps) % count) for source in range(count)])
+
+
+def picked(stack, place):
+    return lax.dynamic_index_in_dim(stack, place, 0, False)
+
+
+def heads_divide(tokens, query_weight, pooling_input_weight, pooling_group_maps, decay_spike, out_weight):
+    planes, members, cores = (lax.axis_size(axis) for axis in ("sp", "fs", "tp"))
+    heads = decay_spike.shape[2]
+    head_width = query_weight.shape[1] // heads
+    return (
+        cores == 2
+        and members & (members - 1) == 0
+        and heads == planes
+        and pooling_group_maps.shape[0] * cores == heads
+        and pooling_input_weight.shape[1] == query_weight.shape[1]
+        and tokens.shape[0] == 1
+        and decay_spike.shape[1] == cores * tokens.shape[1]
+        and query_weight.shape[0] % members == 0
+        and out_weight.shape[1] == members * head_width
+        and (planes * decay_spike.shape[1]) % BLOCK == 0
+    )
+
+
+def by_heads(
+    tokens,
+    input_norm_gain,
+    pooling_input_weight,
+    query_weight,
+    forget_weight,
+    value_weight,
+    pooling_group_maps,
+    pooling_scale,
+    lower_bound_logits,
+    decay_spike,
+    head_norm_gain,
+    pooling_output_weight,
+    recurrent_output_weight,
+):
+    planes, members, cores = (lax.axis_size(axis) for axis in ("sp", "fs", "tp"))
+    plane, member, core = (lax.axis_index(axis) for axis in ("sp", "fs", "tp"))
+    heads = decay_spike.shape[2]
+    head = cores * plane + core
+    column = head % heads
+    partner_column = (cores * plane + 1 - core) % heads
+    owns = head // heads == core
+    rows_local, width_local = query_weight.shape
+    width = width_local // heads
+    row_slice = rows_local // members
+    features = tokens.shape[2]
+    inputs = (pooling_input_weight, query_weight, forget_weight, value_weight)
+    outputs = (pooling_output_weight, recurrent_output_weight)
+    count_in = len(inputs) * row_slice
+
+    def packed(place, part):
+        return jnp.concatenate(
+            [
+                lax.dynamic_slice(w, (part * row_slice, place * width), (row_slice, width))
+                for w in inputs
+            ]
+            + [
+                lax.dynamic_slice(w, (place * width, part * width), (width, width))
+                for w in outputs
+            ],
+            axis=0,
+        )
+
+    arrived = []
+    for step in range(planes):
+        pairs = [
+            (p * cores + c, heads * c + (p + step) % heads)
+            for p in range(planes)
+            for c in range(cores)
+        ]
+        arrived.append(
+            lax.ppermute(packed((plane + step) % heads, member), ("sp", "tp"), pairs)
+        )
+    group_local = plane % pooling_group_maps.shape[0]
+    group_map = picked(pooling_group_maps, group_local)
+
+    def own_block(place, side):
+        return jnp.concatenate(
+            [packed(place, part) for part in range(members)]
+            + [lax.dynamic_slice_in_dim(group_map, side * width, width, 1)],
+            axis=0,
+        )
+
+    def own_vectors(place):
+        return jnp.stack(
+            [
+                lax.dynamic_slice_in_dim(v, place * width, width, 0)
+                for v in (pooling_scale, lower_bound_logits, head_norm_gain)
+            ]
+        )
+
+    block_rows = count_in + len(outputs) * width
+    block = jnp.where(
+        owns, own_block(column, core), swapped(own_block(partner_column, 1 - core), "tp", 1)
+    )
+    vectors = jnp.where(
+        owns, own_vectors(column), swapped(own_vectors(partner_column), "tp", 1)
+    )
+    map_columns = block[members * block_rows :]
+    own_parts = block[: members * block_rows].reshape(members, block_rows, width)
+
+    normed = rms_scale(tokens[0].astype(jnp.float32), input_norm_gain).astype(jnp.bfloat16)
+    spikes = decay_spike[0].T
+    spikes_high = lax.reduce_precision(spikes, 8, 7)
+    spike_rows = jnp.concatenate([spikes_high, spikes - spikes_high], axis=0).astype(jnp.bfloat16)
+    message = jnp.concatenate(
+        [normed, jnp.pad(spike_rows, ((0, 0), (0, features - spike_rows.shape[1])))], axis=0
+    )
+    own_rows = [message] + [turned(message, "sp", step) for step in range(1, planes)]
+    partner_rows = [swapped(rows, "tp", 1) for rows in own_rows]
+    rows_each = normed.shape[0]
+
+    gathered = jnp.stack(arrived)
+    others = jnp.stack(
+        [picked(gathered, (column - plane - k) % planes) for k in range(1, planes)]
+    )
+    shared = jnp.stack([others] + [swapped(others, "fs", bits) for bits in range(1, members)])
+    by_member = jnp.stack([picked(shared, member ^ part) for part in range(members)])
+    by_offset = jnp.concatenate([own_parts[:, None], by_member], axis=1)
+    weights = jnp.stack(
+        [
+            lax.dynamic_index_in_dim(by_offset, (p - plane) % planes, 1, False)
+            for p in range(planes)
+        ]
+    )
+    weights_in = weights[:, :, :count_in].reshape(planes, members, len(inputs), row_slice, width)
+    weights_in = jnp.moveaxis(weights_in, 2, 3).reshape(features, len(inputs) * width)
+    weights_out = weights[:, :, count_in:].reshape(planes, members, len(outputs), width, width)
+    weights_out = jnp.moveaxis(weights_out, (2, 3), (0, 1)).reshape(
+        len(outputs) * width, planes * members * width
+    )
+
+    both = jnp.stack([jnp.stack(own_rows), jnp.stack(partner_rows)])
+    ordered = jnp.stack([picked(both, core ^ side) for side in range(cores)])
+    ordered = jnp.stack(
+        [
+            lax.dynamic_index_in_dim(ordered, (plane - p) % planes, 1, False)
+            for p in range(planes)
+        ]
+    )
+    all_tokens = ordered[:, :, :rows_each].reshape(-1, features)
+    length = all_tokens.shape[0]
+    spike_parts = picked(jnp.moveaxis(ordered, 1, 0), head // heads)[
+        :, rows_each:, : spikes.shape[1]
+    ]
+    spike_parts = spike_parts.astype(jnp.float32)
+    spike_all = spike_parts[:, :heads] + spike_parts[:, heads:]
+    spike = lax.dynamic_index_in_dim(spike_all, column, 1, False).reshape(length)
+
+    projected = jnp.dot(all_tokens, weights_in, preferred_element_type=jnp.float32)
+    projected = projected.astype(jnp.bfloat16)
+    pool_input, query, forget_logit, value = (
+        projected[:, n * width : (n + 1) * width].astype(jnp.float32) for n in range(len(inputs))
+    )
+    pool_scale, lower_bound, head_gain = vectors
+
+    window = jnp.left_shift(jnp.int32(2), plane)
+    window_sum = pool_input
+    chosen = jnp.zeros_like(pool_input)
+    for group in range(planes):
+        reach = 2**group
+        window_sum = window_sum + jnp.pad(window_sum, ((reach, 0), (0, 0)))[:length]
+        chosen = jnp.where(plane == group, window_sum, chosen)
+    counts = jnp.minimum(jnp.arange(length, dtype=jnp.int32) + 1, window).astype(jnp.float32)
+    pool_diff = (chosen / counts[:, None] - pool_input).astype(jnp.bfloat16)
+    pool_other = swapped(pool_diff, "tp", 1)
+    pool_both = jnp.where(
+        core == 0,
+        jnp.concatenate([pool_diff, pool_other], axis=1),
+        jnp.concatenate([pool_other, pool_diff], axis=1),
+    )
+    pool_out = jnp.dot(pool_both, map_columns, preferred_element_type=jnp.float32) * pool_scale
+    pool_out = pool_out.astype(jnp.bfloat16)
+
+    blocks = length // BLOCK
+    layout = (blocks, BLOCK, width)
+    reader = jax.nn.silu(query).reshape(layout)
+    key_gate = jax.nn.sigmoid(-lower_bound) * jax.nn.sigmoid(-forget_logit)
+    log_decay = (jnp.log1p(-key_gate) + spike[:, None]).reshape(layout)
+    key_rows = key_gate.reshape(layout)
+    value_rows = value.reshape(layout)
+    inner_log = jnp.cumsum(log_decay, axis=1)
+    read_scaled = reader * jnp.exp(inner_log)
+    key_scaled = key_rows * jnp.exp(-inner_log)
+    causal = (jnp.arange(BLOCK)[:, None] >= jnp.arange(BLOCK)[None, :]).astype(jnp.float32)
+    scores = jnp.einsum("ntd,nsd->nts", read_scaled, key_scaled, precision=HIGHEST) * causal
+    within = jnp.einsum("nts,nse->nte", scores, value_rows, precision=HIGHEST)
+    closing = inner_log[:, -1]
+    key_tail = key_rows * jnp.exp(closing[:, None] - inner_log)
+    deltas = jnp.einsum("nsd,nse->nde", key_tail, value_rows, precision=HIGHEST)
+    block_decay = jnp.exp(closing)
+    state = jnp.zeros((width, width), jnp.float32)
+    entry_states = []
+    for n in range(blocks):
+        entry_states.append(state)
+        state = block_decay[n][:, None] * state + deltas[n]
+    start_states = jnp.stack(entry_states)
+    read_out = within + jnp.einsum("ntd,nde->nte", read_scaled, start_states, precision=HIGHEST)
+    rec_out = (rms_scale(read_out, 1.0) * head_gain).astype(jnp.bfloat16).reshape(length, width)
+
+    mixed = jnp.concatenate([pool_out, rec_out], axis=1).reshape(planes, cores, rows_each, -1)
+
+    def partial_rows(side):
+        part = lax.dynamic_index_in_dim(mixed, side, 1, False)
+        return jnp.einsum("prc,cd->prd", part, weights_out, preferred_element_type=jnp.float32)
+
+    from_partner = swapped(partial_rows(1 - core).astype(jnp.bfloat16), "tp", 1)
+    plane_sums = partial_rows(core) + from_partner.astype(jnp.float32)
+    total = picked(plane_sums, plane)
+    for step in range(1, planes):
+        sent = picked(plane_sums, (plane + step) % planes).astype(jnp.bfloat16)
+        total = total + turned(sent, "sp", step).astype(jnp.float32)
+    return total.astype(jnp.bfloat16)[None]
+
+
+def body(*arrays):
+    tokens, _, pool_in, query_in, _, _, maps, _, _, spike, _, pool_out, _ = arrays
+    if heads_divide(tokens, query_in, pool_in, maps, spike, pool_out):
+        return by_heads(*arrays)
+    return by_positions(*arrays)
+
+
+def by_positions(
     tokens,
     input_norm_gain,
     pooling_input_weight,

time: 247 us -> 146 us (0.59)
  waiting for transfers between devices: 185 us -> 56.5 us
  local copies, waits for them, and re-layouts: 1.8 us -> 40.2 us
  blocking collectives: 26.1 us -> 0 us
  starting transfers between devices: 3.58 us -> 29.1 us
  between operations: 13.5 us -> 0.86 us
  other arithmetic: 5.86 us -> 11.8 us
  matrix products: 11.1 us -> 5.71 us
    all_gather x4 -> x0, waiting for transfers between devices: 177 us -> none  [the longest x1 88.5 us: body(): full_input = lax.all_gather(column_part, 'fs', axis=1, tiled=True)]
    ppermute x1 -> x21, waiting for transfers between devices: 0.01 us -> 56.5 us  [the longest x11 25.4 us: swapped(): lax.ppermute(value, axis, [(source, source ^ bits) for source in range(co...]
    unnamed x14 -> x41, local copies, waits for them, and re-layouts: 0.04 us -> 33.4 us
    all_gather x3 -> x0, blocking collectives: 26.1 us -> none  [the longest x2 23.9 us: entering(): lax.all_gather(a.astype(kind), axis)]
    ppermute x1 -> x21, starting transfers between devices: 3.39 us -> 29.1 us  [the longest x6 10 us: turned(): lax.ppermute(value, axis, [(source, (source + steps) % count) for source...]
    reduce_scatter x1 -> x0, waiting for transfers between devices: 8.08 us -> none  [body(): lax.psum_scatter(jnp.dot(mixed_rows, out_full, preferred_element_type=jnp...]
    dot_general x7 -> x8, matrix products: 11.1 us -> 5.71 us  [the longest x2 2.1 us: partial_rows(): jnp.einsum('prc,cd->prd', part, weights_out, preferred_element_type=jnp.f...]
    concatenate x2, other arithmetic: 4.15 us -> 0.68 us  [the longest x1 0.67 us: by_heads(): by_offset = jnp.concatenate([own_parts[:, None], by_member], axis=1)]
  transfers between devices with their start and end apart: 6 -> 21, of which waited for: 5 -> 10; matrix products, arithmetic and copies ran while one was open for 5% -> 28% of each run, Pallas kernels for 0% -> 0%
where the time goes in v1:
time: 146 us; the launch traced here: 144 us
  waiting for transfers between devices  56.5 us (39%)
  local copies, waits for them, and re-layouts  40.2 us (28%)
  starting transfers between devices  29.1 us (20%)
  other arithmetic  11.8 us (8%)
  matrix products  5.71 us (4%)
    unnamed x41, local copies, waits for them, and re-layouts  33.4 us
    ppermute x11, waiting for transfers between devices, swapped(): lax.ppermute(value, axis, [(source, source ^ bits) for source in range(co...  25.4 us
    ppermute x6, waiting for transfers between devices, turned(): lax.ppermute(value, axis, [(source, (source + steps) % count) for source...  21.3 us
    ppermute x6, starting transfers between devices, turned(): lax.ppermute(value, axis, [(source, (source + steps) % count) for source...  10 us
    ppermute x4, waiting for transfers between devices, by_heads(): lax.ppermute(packed((plane + step) % heads, member), ('sp', 'tp'), pairs)  9.87 us
    ppermute x4, starting transfers between devices, by_heads(): lax.ppermute(packed((plane + step) % heads, member), ('sp', 'tp'), pairs)  9.65 us
    ppermute x11, starting transfers between devices, swapped(): lax.ppermute(value, axis, [(source, source ^ bits) for source in range(co...  9.4 us
  transfers between devices with their start and end apart: 21, of which 10 were waited for; matrix products, arithmetic and copies ran while one was open for 28% of the time, Pallas kernels for 0%

profile of v1, /device:TPU:0, one launch (start us, length us, event | category | flops | bytes accessed | tf_op | source)
XLA Modules:
  0.0 144.2 jit_solution(3141727258002079638)
XLA Ops:
  3.0 5.1 %collective-permute-start.2 = (bf16[72,2048]{1,0:T(8,128)(2,1)S(1)}, bf16[72,2048]{1,0:T(8,128)(2,1)S(1)}, u32[]{:S(2)}, u32[]{:S(2)}) collective-permute-start(bf16[72,2048]{1,0:T(8,128)(2,1)S(1)} %get-tuple-element.116), channel_id=1, source_target_pairs={{0,24},{8,0},{16,8},{24,16},{1,25},{9,1},{17,9},{25,17},{2,26},{10... | collective-permute-start | bytes 884744 | tf_op jit(solution)/shard_map/ppermute | solution.py:56
  11.0 1.4 constant_dynamic-update-slice_fusion.49
  12.4 1.4 %constant_dynamic-update-slice_fusion.48 = (bf16[3328,128]{1,0:T(8,128)(2,1)}, bf16[3328,128]{1,0:T(8,128)(2,1)S(1)}) fusion(bf16[3328,128]{1,0:T(8,128)(2,1)} %get-tuple-element.113, bf16[512,512]{1,0:T(8,128)(2,1)} %param.16, s32[]{:T(128)S(6)} %select_n.369, bf16[3328,128]{1,0:T(8,128)(2,1)S(1)} %get-tuple-element.114, s32[]{:T(128)S(6)} %select_n.362), kind=kLoop, calls=%fused_computation.155 | loop fusion | bytes 131080
  20.0 1.4 constant_dynamic-update-slice_fusion.42
  22.8 1.4 constant_dynamic-update-slice_fusion.40
  24.3 1.4 constant_dynamic-update-slice_fusion.39
  34.5 1.5 %constant_dynamic-update-slice_fusion.30 = (bf16[3328,128]{1,0:T(8,128)(2,1)}, bf16[768,128]{1,0:T(8,128)(2,1)}, bf16[768,128]{1,0:T(8,128)(2,1)S(1)}, bf16[3328...) fusion(bf16[3328,128]{1,0:T(8,128)(2,1)} %get-tuple-element.73, ...), kind=kLoop, calls=%fused_computation.137 | loop fusion | bytes 393244
  36.0 1.5 %constant_dynamic-update-slice_fusion.29 = (bf16[3328,128]{1,0:T(8,128)(2,1)}, bf16[768,128]{1,0:T(8,128)(2,1)}, bf16[768,128]{1,0:T(8,128)(2,1)S(1)}, bf16[3328...) fusion(bf16[3328,128]{1,0:T(8,128)(2,1)} %get-tuple-element.67, ...), kind=kLoop, calls=%fused_computation.136 | loop fusion | bytes 393244
  37.5 1.5 %constant_dynamic-update-slice_fusion.28 = (bf16[3328,128]{1,0:T(8,128)(2,1)}, bf16[768,128]{1,0:T(8,128)(2,1)}, bf16[768,128]{1,0:T(8,128)(2,1)S(1)}, bf16[3328...) fusion(bf16[3328,128]{1,0:T(8,128)(2,1)} %get-tuple-element.61, ...), kind=kLoop, calls=%fused_computation.135 | loop fusion | bytes 393244
  38.9 1.5 %constant_dynamic-update-slice_fusion.27 = (bf16[3328,128]{1,0:T(8,128)(2,1)}, bf16[768,128]{1,0:T(8,128)(2,1)}, bf16[768,128]{1,0:T(8,128)(2,1)S(1)}, bf16[3328...) fusion(bf16[3328,128]{1,0:T(8,128)(2,1)} %get-tuple-element.55, ...), kind=kLoop, calls=%fused_computation.134 | loop fusion | bytes 393244
  42.5 2.3 %collective-permute-start.9 = (bf16[768,128]{1,0:T(8,128)(2,1)}, bf16[768,128]{1,0:T(8,128)(2,1)S(1)}, u32[]{:S(2)}, u32[]{:S(2)}) collective-permute-start(bf16[768,128]{1,0:T(8,128)(2,1)} %get-tuple-element.44), channel_id=1, source_target_pairs={{0,1},{1,17},{8,8},{9,24},{16,9},{17,25},{24,0},{25,16},{2,3},{3,1... | collective-permute-start | bytes 589832 | tf_op jit(solution)/shard_map/ppermute | solution.py:132
  46.5 1.6 %collective-permute-start.8 = (bf16[768,128]{1,0:T(8,128)(2,1)}, bf16[768,128]{1,0:T(8,128)(2,1)S(1)}, u32[]{:S(2)}, u32[]{:S(2)}) collective-permute-start(bf16[768,128]{1,0:T(8,128)(2,1)} %copy-done.5), channel_id=1, source_target_pairs={{0,0},{1,16},{8,1},{9,17},{16,8},{17,24},{24,9},{25,25},{2,2},{3,1... | collective-permute-start | bytes 589832 | tf_op jit(solution)/shard_map/ppermute | solution.py:132
  48.1 5.2 %collective-permute-done.9 = bf16[768,128]{1,0:T(8,128)(2,1)S(1)} collective-permute-done((bf16[768,128]{1,0:T(8,128)(2,1)}, bf16[768,128]{1,0:T(8,128)(2,1)S(1)}, u32[]{:S(2)}, u32[]{:S(2)}) %collective-permute-start.9) | collective-permute-done | bytes 196640 | tf_op jit(solution)/shard_map/ppermute | solution.py:132
  53.3 2.9 %collective-permute-start.11 = (bf16[768,128]{1,0:T(8,128)(2,1)}, bf16[768,128]{1,0:T(8,128)(2,1)S(1)}, u32[]{:S(2)}, u32[]{:S(2)}) collective-permute-start(bf16[768,128]{1,0:T(8,128)(2,1)} %copy-done.6), channel_id=1, source_target_pairs={{0,9},{1,25},{8,0},{9,16},{16,1},{17,17},{24,8},{25,24},{2,11},{3,... | collective-permute-start | bytes 589832 | tf_op jit(solution)/shard_map/ppermute | solution.py:132
  56.2 2.9 %collective-permute-start.10 = (bf16[768,128]{1,0:T(8,128)(2,1)}, bf16[768,128]{1,0:T(8,128)(2,1)S(1)}, u32[]{:S(2)}, u32[]{:S(2)}) collective-permute-start(bf16[768,128]{1,0:T(8,128)(2,1)} %copy-done.7), channel_id=1, source_target_pairs={{0,8},{1,24},{8,9},{9,25},{16,0},{17,16},{24,1},{25,17},{2,10},{3,... | collective-permute-start | bytes 589832 | tf_op jit(solution)/shard_map/ppermute | solution.py:132
  59.1 2.4 %collective-permute-done.11 = bf16[768,128]{1,0:T(8,128)(2,1)S(1)} collective-permute-done((bf16[768,128]{1,0:T(8,128)(2,1)}, bf16[768,128]{1,0:T(8,128)(2,1)S(1)}, u32[]{:S(2)}, u32[]{:S(2)}) %collective-permute-start.11) | collective-permute-done | bytes 196640 | tf_op jit(solution)/shard_map/ppermute | solution.py:132
  61.5 3.2 %collective-permute-start.3 = (bf16[72,2048]{1,0:T(8,128)(2,1)S(1)}, bf16[72,2048]{1,0:T(8,128)(2,1)S(1)}, u32[]{:S(2)}, u32[]{:S(2)}) collective-permute-start(bf16[72,2048]{1,0:T(8,128)(2,1)S(1)} %get-tuple-element.116), channel_id=1, source_target_pairs={{0,1},{1,0},{2,3},{3,2},{4,5},{5,4},{6,7},{7,6},{8,9},{9,8},{10,11... | collective-permute-start | bytes 884744 | tf_op jit(solution)/shard_map/ppermute | solution.py:51
  64.6 2.3 %collective-permute-done.10 = bf16[768,128]{1,0:T(8,128)(2,1)S(1)} collective-permute-done((bf16[768,128]{1,0:T(8,128)(2,1)}, bf16[768,128]{1,0:T(8,128)(2,1)S(1)}, u32[]{:S(2)}, u32[]{:S(2)}) %collective-permute-start.10) | collective-permute-done | bytes 196640 | tf_op jit(solution)/shard_map/ppermute | solution.py:132
  68.4 1.6 %collective-permute-start.13 = (bf16[3,768,128]{2,1,0:T(8,128)(2,1)S(1)}, bf16[3,768,128]{2,1,0:T(8,128)(2,1)S(1)}, u32[]{:S(2)}, u32[]{:S(2)}) collective-permute-start(bf16[3,768,128]{2,1,0:T(8,128)(2,1)S(1)} %get-tuple-element.32), channel_id=1, source_target_pairs={{0,4},{2,6},{4,0},{6,2},{1,5},{3,7},{5,1},{7,3},{8,12},{10,14},{12... | collective-permute-start | bytes 1769480 | tf_op jit(solution)/shard_map/ppermute | solution.py:51
  70.0 1.6 %collective-permute-start.12 = (bf16[3,768,128]{2,1,0:T(8,128)(2,1)S(1)}, bf16[3,768,128]{2,1,0:T(8,128)(2,1)S(1)}, u32[]{:S(2)}, u32[]{:S(2)}) collective-permute-start(bf16[3,768,128]{2,1,0:T(8,128)(2,1)S(1)} %get-tuple-element.32), channel_id=1, source_target_pairs={{0,2},{2,0},{4,6},{6,4},{1,3},{3,1},{5,7},{7,5},{8,10},{10,8},{12,... | collective-permute-start | bytes 1769480 | tf_op jit(solution)/shard_map/ppermute | solution.py:51
  76.0 7.9 %collective-permute-done.13 = bf16[3,768,128]{2,1,0:T(8,128)(2,1)S(1)} collective-permute-done((bf16[3,768,128]{2,1,0:T(8,128)(2,1)S(1)}, bf16[3,768,128]{2,1,0:T(8,128)(2,1)S(1)}, u32[]{:S(2)}, u32[]{:S(2)}) %collective-permute-start.13) | collective-permute-done | bytes 589856 | tf_op jit(solution)/shard_map/ppermute | solution.py:51
  83.8 2.4 %collective-permute-done.12 = bf16[3,768,128]{2,1,0:T(8,128)(2,1)S(1)} collective-permute-done((bf16[3,768,128]{2,1,0:T(8,128)(2,1)S(1)}, bf16[3,768,128]{2,1,0:T(8,128)(2,1)S(1)}, u32[]{:S(2)}, u32[]{:S(2)}) %collective-permute-start.12) | collective-permute-done | bytes 589856 | tf_op jit(solution)/shard_map/ppermute | solution.py:51
  86.2 12.7 %collective-permute-done.14 = bf16[3,768,128]{2,1,0:T(8,128)(2,1)S(1)} collective-permute-done((bf16[3,768,128]{2,1,0:T(8,128)(2,1)S(1)}, bf16[3,768,128]{2,1,0:T(8,128)(2,1)S(1)}, u32[]{:S(2)}, u32[]{:S(2)}) %collective-permute-start.14) | collective-permute-done | bytes 589856 | tf_op jit(solution)/shard_map/ppermute | solution.py:51
  101.2 1.8 %copy.24 = bf16[4,4,4,128,128]{4,2,3,1,0:T(4,128)(2,1)S(1)} copy(bf16[4,4,4,128,128]{4,3,2,1,0:T(8,128)(2,1)S(1)} %bitcast.151) | data formatting | bytes 4194304 | tf_op jit(solution)/shard_map/reshape | solution.py:186
  107.4 1.4 exponential_multiply_fusion
  113.1 2.4 %collective-permute-done.17 = bf16[4,64,2048]{2,1,0:T(8,128)(2,1)} collective-permute-done((bf16[4,64,2048]{2,1,0:T(8,128)(2,1)S(1)}, bf16[4,64,2048]{2,1,0:T(8,128)(2,1)}, u32[]{:S(2)}, u32[]{:S(2)}) %collective-permute-start.17) | collective-permute-done | bytes 1048608 | tf_op jit(solution)/shard_map/ppermute | solution.py:51
  115.5 1.7 %convert_add_fusion = f32[4,64,2048]{2,1,0:T(8,128)S(1)} fusion(bf16[4,64,2048]{2,1,0:T(8,128)(2,1)} %collective-permute-done.17, bf16[256,2048,1]{1,0,2:T(8,128)(2,1)S(1)} %reshape.261, s32[]{:T(128)S(6)} %select_n.349, bf16[4,2,64,128]{3,2,1,0:T(8,128)(2,1)S(1)} %bitcast.167, bf16[4,2,64,128]{3,2,1,0:T(8,128)(2,1)S(1)} %bitcast.159), kind=kOutput, calls=%fused_computation.20 | convolution fusion | flops 269746176 | bytes 4456452 | tf_op jit(solution)/shard_map/prc,cd->prd/dot_general | solution.py:265
  117.4 3.8 %collective-permute-start.20 = (bf16[64,2048]{1,0:T(8,128)(2,1)S(1)}, bf16[64,2048]{1,0:T(8,128)(2,1)S(1)}, u32[]{:S(2)}, u32[]{:S(2)}) collective-permute-start(bf16[64,2048]{1,0:T(8,128)(2,1)S(1)} %get-tuple-element.26), channel_id=1, source_target_pairs={{0,24},{8,0},{16,8},{24,16},{1,25},{9,1},{17,9},{25,17},{2,26},{10... | collective-permute-start | bytes 786440 | tf_op jit(solution)/shard_map/ppermute | solution.py:56
  121.2 7.2 %collective-permute-done.18 = bf16[64,2048]{1,0:T(8,128)(2,1)S(1)} collective-permute-done((bf16[64,2048]{1,0:T(8,128)(2,1)S(1)}, bf16[64,2048]{1,0:T(8,128)(2,1)S(1)}, u32[]{:S(2)}, u32[]{:S(2)}) %collective-permute-start.18) | collective-permute-done | bytes 262176 | tf_op jit(solution)/shard_map/ppermute | solution.py:56
  128.4 5.5 %collective-permute-done.20 = bf16[64,2048]{1,0:T(8,128)(2,1)S(1)} collective-permute-done((bf16[64,2048]{1,0:T(8,128)(2,1)S(1)}, bf16[64,2048]{1,0:T(8,128)(2,1)S(1)}, u32[]{:S(2)}, u32[]{:S(2)}) %collective-permute-start.20) | collective-permute-done | bytes 262176 | tf_op jit(solution)/shard_map/ppermute | solution.py:56
  133.8 8.6 %collective-permute-done.19 = bf16[64,2048]{1,0:T(8,128)(2,1)} collective-permute-done((bf16[64,2048]{1,0:T(8,128)(2,1)S(1)}, bf16[64,2048]{1,0:T(8,128)(2,1)}, u32[]{:S(2)}, u32[]{:S(2)}) %collective-permute-start.19) | collective-permute-done | bytes 262176 | tf_op jit(solution)/shard_map/ppermute | solution.py:56
  142.4 1.8 %fusion.36 = bf16[1,64,2048]{2,1,0:T(8,128)(2,1)} fusion(bf16[64,2048]{1,0:T(8,128)(2,1)S(1)} %collective-permute-done.20, bf16[64,2048]{1,0:T(8,128)(2,1)} %collective-permute-done.19, bf16[64,2048]{1,0:T(8,128)(2,1)S(1)} %collective-permute-done.18, f32[4,64,2048]{2,1,0:T(8,128)S(1)} %convert_add_fusion, s32[]{:T(128)S(6)} %select_n.412), kind=kLoop, calls=%fused_computation.84 | loop fusion | flops 917504 | bytes 1572868 | tf_op jit(solution)/shard_map/broadcast_in_dim | solution.py:273
  (120 shorter events, 42.2 us)
Async XLA Ops:
  0.0 19.4 %copy-start.2 = (bf16[512,512]{1,0:T(8,128)(2,1)S(1)}, bf16[512,512]{1,0:T(8,128)(2,1)}, u32[]{:S(2)}) copy-start(bf16[512,512]{1,0:T(8,128)(2,1)} %param.15) | copy-start | bytes 1572868
  3.0 64.1 %collective-permute-start.2 = (bf16[72,2048]{1,0:T(8,128)(2,1)S(1)}, bf16[72,2048]{1,0:T(8,128)(2,1)S(1)}, u32[]{:S(2)}, u32[]{:S(2)}) collective-permute-start(bf16[72,2048]{1,0:T(8,128)(2,1)S(1)} %get-tuple-element.116), channel_id=1, source_target_pairs={{0,24},{8,0},{16,8},{24,16},{1,25},{9,1},{17,9},{25,17},{2,26},{10... | collective-permute-start | bytes 884744 | tf_op jit(solution)/shard_map/ppermute | solution.py:56
  8.2 59.5 %collective-permute-start.1 = (bf16[72,2048]{1,0:T(8,128)(2,1)S(1)}, bf16[72,2048]{1,0:T(8,128)(2,1)S(1)}, u32[]{:S(2)}, u32[]{:S(2)}) collective-permute-start(bf16[72,2048]{1,0:T(8,128)(2,1)S(1)} %get-tuple-element.116), channel_id=1, source_target_pairs={{0,16},{8,24},{16,0},{24,8},{1,17},{9,25},{17,1},{25,9},{2,18},{10... | collective-permute-start | bytes 884744 | tf_op jit(solution)/shard_map/ppermute | solution.py:56
  8.2 59.6 %collective-permute-start = (bf16[72,2048]{1,0:T(8,128)(2,1)S(1)}, bf16[72,2048]{1,0:T(8,128)(2,1)S(1)}, u32[]{:S(2)}, u32[]{:S(2)}) collective-permute-start(bf16[72,2048]{1,0:T(8,128)(2,1)S(1)} %get-tuple-element.116), channel_id=1, source_target_pairs={{0,8},{8,16},{16,24},{24,0},{1,9},{9,17},{17,25},{25,1},{2,10},{10... | collective-permute-start | bytes 884744 | tf_op jit(solution)/shard_map/ppermute | solution.py:56
  10.9 35.7 %collective-permute-start.16 = (f32[3,128]{1,0:T(4,128)S(1)}, f32[3,128]{1,0:T(4,128)S(1)}, u32[]{:S(2)}, u32[]{:S(2)}) collective-permute-start(f32[3,128]{1,0:T(4,128)S(1)} %pad_maximum_fusion.7), channel_id=1, source_target_pairs={{0,1},{1,0},{2,3},{3,2},{4,5},{5,4},{6,7},{7,6},{8,9},{9,8},{10,11... | collective-permute-start | bytes 4616 | tf_op jit(solution)/shard_map/ppermute | solution.py:51
  12.4 20.8 %copy-start.3 = (bf16[512,512]{1,0:T(8,128)(2,1)S(1)}, bf16[512,512]{1,0:T(8,128)(2,1)}, u32[]{:S(2)}) copy-start(bf16[512,512]{1,0:T(8,128)(2,1)} %param.25) | copy-start | bytes 1572868
  22.8 22.9 %copy-start.4 = (bf16[2,256,256]{2,1,0:T(8,128)(2,1)S(1)}, bf16[2,256,256]{2,1,0:T(8,128)(2,1)}, u32[]{:S(2)}) copy-start(bf16[2,256,256]{2,1,0:T(8,128)(2,1)} %param.19) | copy-start | bytes 786436
  41.1 0.7 copy-start.5
  41.8 0.7 copy-start.6
  41.8 0.8 copy-start.7
  42.5 10.7 %collective-permute-start.9 = (bf16[768,128]{1,0:T(8,128)(2,1)}, bf16[768,128]{1,0:T(8,128)(2,1)S(1)}, u32[]{:S(2)}, u32[]{:S(2)}) collective-permute-start(bf16[768,128]{1,0:T(8,128)(2,1)} %get-tuple-element.44), channel_id=1, source_target_pairs={{0,1},{1,17},{8,8},{9,24},{16,9},{17,25},{24,0},{25,16},{2,3},{3,1... | collective-permute-start | bytes 589832 | tf_op jit(solution)/shard_map/ppermute | solution.py:132
  46.5 9.7 %collective-permute-start.8 = (bf16[768,128]{1,0:T(8,128)(2,1)}, bf16[768,128]{1,0:T(8,128)(2,1)S(1)}, u32[]{:S(2)}, u32[]{:S(2)}) collective-permute-start(bf16[768,128]{1,0:T(8,128)(2,1)} %copy-done.5), channel_id=1, source_target_pairs={{0,0},{1,16},{8,1},{9,17},{16,8},{17,24},{24,9},{25,25},{2,2},{3,1... | collective-permute-start | bytes 589832 | tf_op jit(solution)/shard_map/ppermute | solution.py:132
  53.3 8.2 %collective-permute-start.11 = (bf16[768,128]{1,0:T(8,128)(2,1)}, bf16[768,128]{1,0:T(8,128)(2,1)S(1)}, u32[]{:S(2)}, u32[]{:S(2)}) collective-permute-start(bf16[768,128]{1,0:T(8,128)(2,1)} %copy-done.6), channel_id=1, source_target_pairs={{0,9},{1,25},{8,0},{9,16},{16,1},{17,17},{24,8},{25,24},{2,11},{3,... | collective-permute-start | bytes 589832 | tf_op jit(solution)/shard_map/ppermute | solution.py:132
  56.2 10.7 %collective-permute-start.10 = (bf16[768,128]{1,0:T(8,128)(2,1)}, bf16[768,128]{1,0:T(8,128)(2,1)S(1)}, u32[]{:S(2)}, u32[]{:S(2)}) collective-permute-start(bf16[768,128]{1,0:T(8,128)(2,1)} %copy-done.7), channel_id=1, source_target_pairs={{0,8},{1,24},{8,9},{9,25},{16,0},{17,16},{24,1},{25,17},{2,10},{3,... | collective-permute-start | bytes 589832 | tf_op jit(solution)/shard_map/ppermute | solution.py:132
  61.5 7.0 %collective-permute-start.3 = (bf16[72,2048]{1,0:T(8,128)(2,1)S(1)}, bf16[72,2048]{1,0:T(8,128)(2,1)S(1)}, u32[]{:S(2)}, u32[]{:S(2)}) collective-permute-start(bf16[72,2048]{1,0:T(8,128)(2,1)S(1)} %get-tuple-element.116), channel_id=1, source_target_pairs={{0,1},{1,0},{2,3},{3,2},{4,5},{5,4},{6,7},{7,6},{8,9},{9,8},{10,11... | collective-permute-start | bytes 884744 | tf_op jit(solution)/shard_map/ppermute | solution.py:51
  66.9 32.5 %collective-permute-start.7 = (bf16[3328,128]{1,0:T(8,128)(2,1)}, bf16[3328,128]{1,0:T(8,128)(2,1)S(1)}, u32[]{:S(2)}, u32[]{:S(2)}) collective-permute-start(bf16[3328,128]{1,0:T(8,128)(2,1)} %get-tuple-element.118), channel_id=1, source_target_pairs={{0,1},{1,0},{2,3},{3,2},{4,5},{5,4},{6,7},{7,6},{8,9},{9,8},{10,11... | collective-permute-start | bytes 2555912 | tf_op jit(solution)/shard_map/ppermute | solution.py:51
  67.1 2.9 %collective-permute-start.6 = (bf16[72,2048]{1,0:T(8,128)(2,1)S(1)}, bf16[72,2048]{1,0:T(8,128)(2,1)S(1)}, u32[]{:S(2)}, u32[]{:S(2)}) collective-permute-start(bf16[72,2048]{1,0:T(8,128)(2,1)S(1)} %collective-permute-done.2), channel_id=1, source_target_pairs={{0,1},{1,0},{2,3},{3,2},{4,5},{5,4},{6,7},{7,6},{8,9},{9,8},{10,11... | collective-permute-start | bytes 884744 | tf_op jit(solution)/shard_map/ppermute | solution.py:51
  67.7 4.0 %collective-permute-start.5 = (bf16[72,2048]{1,0:T(8,128)(2,1)S(1)}, bf16[72,2048]{1,0:T(8,128)(2,1)S(1)}, u32[]{:S(2)}, u32[]{:S(2)}) collective-permute-start(bf16[72,2048]{1,0:T(8,128)(2,1)S(1)} %collective-permute-done.1), channel_id=1, source_target_pairs={{0,1},{1,0},{2,3},{3,2},{4,5},{5,4},{6,7},{7,6},{8,9},{9,8},{10,11... | collective-permute-start | bytes 884744 | tf_op jit(solution)/shard_map/ppermute | solution.py:51
  67.8 5.2 %collective-permute-start.4 = (bf16[72,2048]{1,0:T(8,128)(2,1)S(1)}, bf16[72,2048]{1,0:T(8,128)(2,1)S(1)}, u32[]{:S(2)}, u32[]{:S(2)}) collective-permute-start(bf16[72,2048]{1,0:T(8,128)(2,1)S(1)} %collective-permute-done), channel_id=1, source_target_pairs={{0,1},{1,0},{2,3},{3,2},{4,5},{5,4},{6,7},{7,6},{8,9},{9,8},{10,11... | collective-permute-start | bytes 884744 | tf_op jit(solution)/shard_map/ppermute | solution.py:51
  68.4 15.4 %collective-permute-start.13 = (bf16[3,768,128]{2,1,0:T(8,128)(2,1)S(1)}, bf16[3,768,128]{2,1,0:T(8,128)(2,1)S(1)}, u32[]{:S(2)}, u32[]{:S(2)}) collective-permute-start(bf16[3,768,128]{2,1,0:T(8,128)(2,1)S(1)} %get-tuple-element.32), channel_id=1, source_target_pairs={{0,4},{2,6},{4,0},{6,2},{1,5},{3,7},{5,1},{7,3},{8,12},{10,14},{12... | collective-permute-start | bytes 1769480 | tf_op jit(solution)/shard_map/ppermute | solution.py:51
  70.0 16.2 %collective-permute-start.12 = (bf16[3,768,128]{2,1,0:T(8,128)(2,1)S(1)}, bf16[3,768,128]{2,1,0:T(8,128)(2,1)S(1)}, u32[]{:S(2)}, u32[]{:S(2)}) collective-permute-start(bf16[3,768,128]{2,1,0:T(8,128)(2,1)S(1)} %get-tuple-element.32), channel_id=1, source_target_pairs={{0,2},{2,0},{4,6},{6,4},{1,3},{3,1},{5,7},{7,5},{8,10},{10,8},{12,... | collective-permute-start | bytes 1769480 | tf_op jit(solution)/shard_map/ppermute | solution.py:51
  71.7 27.2 %collective-permute-start.14 = (bf16[3,768,128]{2,1,0:T(8,128)(2,1)S(1)}, bf16[3,768,128]{2,1,0:T(8,128)(2,1)S(1)}, u32[]{:S(2)}, u32[]{:S(2)}) collective-permute-start(bf16[3,768,128]{2,1,0:T(8,128)(2,1)S(1)} %get-tuple-element.32), channel_id=1, source_target_pairs={{0,6},{2,4},{4,2},{6,0},{1,7},{3,5},{5,3},{7,1},{8,14},{10,12},{12... | collective-permute-start | bytes 1769480 | tf_op jit(solution)/shard_map/ppermute | solution.py:51
  74.5 1.4 copy-start
  101.2 1.8 %slice-start = ((bf16[4,2,72,2048]{3,2,1,0:T(8,128)(2,1)}), bf16[4,2,64,2048]{3,2,1,0:T(8,128)(2,1)S(1)}, s32[]{:S(2)}) async-start(bf16[4,2,72,2048]{3,2,1,0:T(8,128)(2,1)} %copy-done), calls=%async_computation | async-start | bytes 4194304 | tf_op jit(solution)/shard_map/slice | solution.py:201
  107.3 3.0 %copy-start.1 = (f32[8,128,128]{2,1,0:T(8,128)S(1)}, f32[8,128,128]{2,1,0:T(8,128)}, u32[]{:S(2)}) copy-start(f32[8,128,128]{2,1,0:T(8,128)} %constant_dynamic-update-slice_fusion.81) | copy-start | bytes 1572868
  107.4 4.5 %collective-permute-start.15 = (bf16[512,128]{1,0:T(8,128)(2,1)S(1)}, bf16[512,128]{1,0:T(8,128)(2,1)S(1)}, u32[]{:S(2)}, u32[]{:S(2)}) collective-permute-start(bf16[512,128]{1,0:T(8,128)(2,1)S(1)} %get-tuple-element.40), channel_id=1, source_target_pairs={{0,1},{1,0},{2,3},{3,2},{4,5},{5,4},{6,7},{7,6},{8,9},{9,8},{10,11... | collective-permute-start | bytes 393224 | tf_op jit(solution)/shard_map/ppermute | solution.py:51
  112.6 2.9 %collective-permute-start.17 = (bf16[4,64,2048]{2,1,0:T(8,128)(2,1)S(1)}, bf16[4,64,2048]{2,1,0:T(8,128)(2,1)}, u32[]{:S(2)}, u32[]{:S(2)}) collective-permute-start(bf16[4,64,2048]{2,1,0:T(8,128)(2,1)S(1)} %convolution_convert_fusion), channel_id=1, source_target_pairs={{0,1},{1,0},{2,3},{3,2},{4,5},{5,4},{6,7},{7,6},{8,9},{9,8},{10,11... | collective-permute-start | bytes 3145736 | tf_op jit(solution)/shard_map/ppermute | solution.py:51
  117.3 11.1 %collective-permute-start.18 = (bf16[64,2048]{1,0:T(8,128)(2,1)S(1)}, bf16[64,2048]{1,0:T(8,128)(2,1)S(1)}, u32[]{:S(2)}, u32[]{:S(2)}) collective-permute-start(bf16[64,2048]{1,0:T(8,128)(2,1)S(1)} %get-tuple-element.25), channel_id=1, source_target_pairs={{0,8},{8,16},{16,24},{24,0},{1,9},{9,17},{17,25},{25,1},{2,10},{10... | collective-permute-start | bytes 786440 | tf_op jit(solution)/shard_map/ppermute | solution.py:56
  117.4 16.5 %collective-permute-start.20 = (bf16[64,2048]{1,0:T(8,128)(2,1)S(1)}, bf16[64,2048]{1,0:T(8,128)(2,1)S(1)}, u32[]{:S(2)}, u32[]{:S(2)}) collective-permute-start(bf16[64,2048]{1,0:T(8,128)(2,1)S(1)} %get-tuple-element.26), channel_id=1, source_target_pairs={{0,24},{8,0},{16,8},{24,16},{1,25},{9,1},{17,9},{25,17},{2,26},{10... | collective-permute-start | bytes 786440 | tf_op jit(solution)/shard_map/ppermute | solution.py:56
  121.2 21.3 %collective-permute-start.19 = (bf16[64,2048]{1,0:T(8,128)(2,1)S(1)}, bf16[64,2048]{1,0:T(8,128)(2,1)}, u32[]{:S(2)}, u32[]{:S(2)}) collective-permute-start(bf16[64,2048]{1,0:T(8,128)(2,1)S(1)} %get-tuple-element.27), channel_id=1, source_target_pairs={{0,16},{8,24},{16,0},{24,8},{1,17},{9,25},{17,1},{25,9},{2,18},{10... | collective-permute-start | bytes 786440 | tf_op jit(solution)/shard_map/ppermute | solution.py:56

commit v2 on v0

--- a/solution.py
+++ b/solution.py
@@ -1,6 +1,8 @@
 import jax
 import jax.numpy as jnp
 from jax import lax
+from jax.experimental import pallas as pl
+from jax.experimental.pallas import tpu as pltpu
 from jax.sharding import PartitionSpec as P
 
 BLOCK = 64
@@ -46,7 +48,406 @@
     return (decay_one * decay_two, decay_two[..., None] * state_one + state_two)
 
 
-def body(
+def swapped(value, axis, bits):
+    count = lax.axis_size(axis)
+    return lax.ppermute(value, axis, [(source, source ^ bits) for source in range(count)])
+
+
+def turned(value, axis, steps):
+    count = lax.axis_size(axis)
+    return lax.ppermute(value, axis, [(source, (source + steps) % count) for source in range(count)])
+
+
+def picked(stack, place):
+    return lax.dynamic_index_in_dim(stack, place, 0, False)
+
+
+def heads_divide(tokens, query_weight, pooling_input_weight, pooling_group_maps, decay_spike, out_weight):
+    planes, members, cores = (lax.axis_size(axis) for axis in ("sp", "fs", "tp"))
+    heads = decay_spike.shape[2]
+    width = query_weight.shape[1] // heads
+    return (
+        cores == 2
+        and members & (members - 1) == 0
+        and heads == planes
+        and width % 128 == 0
+        and pooling_group_maps.shape[0] * cores == heads
+        and pooling_input_weight.shape[1] == query_weight.shape[1]
+        and tokens.shape[0] == 1
+        and tokens.shape[1] % BLOCK == 0
+        and decay_spike.shape[1] == cores * tokens.shape[1] == width
+        and query_weight.shape[0] == members * width
+        and out_weight.shape[1] == members * width
+    )
+
+
+def pack_kernel(planes, members, width, rows_each, *refs):
+    tokens, gain, spikes, maps, scale = refs[:5]
+    inputs, outputs = refs[5:9], refs[9:11]
+    messages, block, own, rows_out = refs[11 : 11 + planes], *refs[11 + planes : 14 + planes]
+    pooling_rows = refs[14 + planes]
+    plane, member, core = (lax.axis_index(axis) for axis in ("sp", "fs", "tp"))
+    half = width // 2
+    heads = spikes.shape[1]
+    own_column = lax.rem(2 * plane + core, heads)
+    partner_column = lax.rem(2 * plane + 1 - core, heads)
+    values = tokens[...].astype(jnp.float32)
+    rows_out[pl.ds(0, rows_each), :] = rms_scale(values, gain[...]).astype(jnp.bfloat16)
+    rows_out[pl.ds(rows_each, 8), :] = jnp.zeros((8, rows_out.shape[1]), jnp.bfloat16)
+    lines = [
+        jnp.broadcast_to(spikes[:, n : n + 1], (width, width)).T[:1] for n in range(heads)
+    ]
+    upper = [line.astype(jnp.bfloat16) for line in lines]
+    lower = [
+        (line - high.astype(jnp.float32)).astype(jnp.bfloat16) for line, high in zip(lines, upper)
+    ]
+    rows_out[pl.ds(rows_each, 8), pl.ds(0, width)] = jnp.concatenate(upper + lower, axis=0)
+    groups, size = maps.shape[:2]
+    for g in range(groups):
+        span = pl.ds(g * size, size)
+        scaled = maps[g].astype(jnp.float32) * scale[:, span]
+        upper = scaled.astype(jnp.bfloat16)
+        rest = (scaled - upper.astype(jnp.float32)).astype(jnp.bfloat16)
+        rows = outputs[0][span, :]
+        pooling_rows[span, :] = (
+            jnp.dot(upper, rows, preferred_element_type=jnp.float32)
+            + jnp.dot(rest, rows, preferred_element_type=jnp.float32)
+        ).astype(jnp.bfloat16)
+    outputs = (pooling_rows, outputs[1])
+    row = pl.multiple_of(member * width, width)
+    for step in range(planes):
+        column = pl.multiple_of(lax.rem(plane + step, heads) * width, width)
+        for n, w in enumerate(inputs):
+            messages[step][pl.ds(0, width), pl.ds(n * width, width)] = w[
+                pl.ds(row, width), pl.ds(column, width)
+            ]
+        for n in range(4):
+            top = pl.multiple_of(column + (n % 2) * half, half)
+            messages[step][pl.ds(width, half), pl.ds(n * width, width)] = outputs[n // 2][
+                pl.ds(top, half), pl.ds(row, width)
+            ]
+    rows = members * width
+    for place, target in ((partner_column, block), (own_column, own)):
+        column = pl.multiple_of(place * width, width)
+        for n, w in enumerate(inputs):
+            target[pl.ds(0, rows), pl.ds(n * width, width)] = w[:, pl.ds(column, width)]
+        for n, w in enumerate(outputs):
+            target[pl.ds(rows + n * width, width), :] = w[pl.ds(column, width), :]
+
+
+def down(values, steps):
+    rows = lax.broadcasted_iota(jnp.int32, values.shape, 0)
+    return jnp.where(rows >= steps, pltpu.roll(values, steps, 0), 0.0)
+
+
+def layer_kernel(planes, members, cores, width, rows_each, *refs):
+    own_vectors, partner_vectors = refs[0], refs[1]
+    position = 2
+    tokens = [refs[position + n * planes : position + (n + 1) * planes] for n in range(cores)]
+    position += cores * planes
+    pieces = refs[position : position + members]
+    position += members
+    blocks = refs[position : position + 2]
+    sent, kept = refs[position + 2 : position + 4]
+    token_all, weight_in, weight_out, spikes, mixed, sems = refs[position + 4 :]
+    plane, member, core = (lax.axis_index(axis) for axis in ("sp", "fs", "tp"))
+    column = lax.rem(cores * plane + core, planes)
+    owner = lax.div(cores * plane + core, planes)
+    owns = owner == core
+    length = planes * cores * rows_each
+    half = width // 2
+    plane_rows = members * width
+    copies = []
+    for step in range(planes):
+        source = lax.rem(plane - step + planes, planes)
+        for side in range(cores):
+            origin = core if side == 0 else 1 - core
+            top = pl.multiple_of((source * cores + origin) * rows_each, rows_each)
+            copies.append(
+                (
+                    tokens[side][step].at[pl.ds(0, rows_each), :],
+                    token_all.at[pl.ds(top, rows_each), :],
+                )
+            )
+            copies.append(
+                (
+                    tokens[side][step].at[pl.ds(rows_each, 8), pl.ds(0, width)],
+                    spikes.at[source * cores + origin],
+                )
+            )
+    copy_list = [
+        pltpu.make_async_copy(source, target, sems.at[n]) for n, (source, target) in enumerate(copies)
+    ]
+    for copy in copy_list:
+        copy.start()
+    used = len(copies)
+    own_copies = []
+    block_copies = []
+    for own_block in blocks:
+        block_copies.append(
+            [
+                pltpu.make_async_copy(
+                    own_block.at[pl.ds(0, plane_rows), :],
+                    weight_in.at[
+                        pl.ds(pl.multiple_of(plane * plane_rows, plane_rows), plane_rows), :
+                    ],
+                    sems.at[used],
+                ),
+                pltpu.make_async_copy(
+                    own_block.at[pl.ds(plane_rows, 2 * width), :],
+                    weight_out.at[
+                        :, pl.ds(pl.multiple_of(plane * plane_rows, plane_rows), plane_rows)
+                    ],
+                    sems.at[used + 1],
+                ),
+            ]
+        )
+
+    @pl.when(owns)
+    def _():
+        for copy in block_copies[0]:
+            copy.start()
+
+    @pl.when(jnp.logical_not(owns))
+    def _():
+        for copy in block_copies[1]:
+            copy.start()
+
+    used += 2
+    for bits in range(members):
+        for k in range(1, planes):
+            source = lax.rem(plane + k, planes)
+            place = pl.multiple_of((source * members + (member ^ bits)) * width, width)
+            piece = pieces[bits].at[k - 1]
+            own_copies.append(
+                pltpu.make_async_copy(
+                    piece.at[pl.ds(0, width), :], weight_in.at[pl.ds(place, width), :], sems.at[used]
+                )
+            )
+            used += 1
+            for n in range(4):
+                own_copies.append(
+                    pltpu.make_async_copy(
+                        piece.at[pl.ds(width, half), pl.ds(n * width, width)],
+                        weight_out.at[pl.ds(n * half, half), pl.ds(place, width)],
+                        sems.at[used],
+                    )
+                )
+                used += 1
+    for copy in own_copies:
+        copy.start()
+    for copy in copy_list + block_copies[0] + own_copies:
+        copy.wait()
+
+    lower_bound, head_gain = (
+        jnp.where(owns, own_vectors[pl.ds(n, 1), :], partner_vectors[pl.ds(n, 1), :])
+        for n in range(2)
+    )
+    projected = jnp.dot(token_all[...], weight_in[...], preferred_element_type=jnp.float32)
+    projected = projected.astype(jnp.bfloat16).astype(jnp.float32)
+    pool_input, query, forget_logit, value = (
+        projected[:, n * width : (n + 1) * width] for n in range(4)
+    )
+
+    window = jnp.left_shift(jnp.int32(2), plane)
+    window_sum = pool_input
+    chosen = jnp.zeros_like(pool_input)
+    for group in range(planes):
+        window_sum = window_sum + down(window_sum, 2**group)
+        chosen = jnp.where(plane == group, window_sum, chosen)
+    at = lax.broadcasted_iota(jnp.int32, pool_input.shape, 0)
+    counts = jnp.minimum(at + 1, window).astype(jnp.float32)
+    mixed[:, pl.ds(0, width)] = (chosen / counts - pool_input).astype(jnp.bfloat16)
+
+    spike_row = lax.broadcasted_iota(jnp.int32, (8, width), 0)
+    wanted_row = jnp.logical_or(spike_row == column, spike_row == column + planes)
+    spike_columns = []
+    for source in range(planes):
+        parts = spikes[source * cores + owner].astype(jnp.float32)
+        line = jnp.sum(jnp.where(wanted_row, parts, 0.0), axis=0, keepdims=True)
+        spike_columns.append(jnp.broadcast_to(line, (width, width)).T)
+    spike = jnp.concatenate(spike_columns, axis=0)
+
+    reader = query * jax.nn.sigmoid(query)
+    key_gate = jax.nn.sigmoid(-lower_bound) * jax.nn.sigmoid(-forget_logit)
+    log_decay = jnp.log1p(-key_gate) + spike
+    t_at = lax.broadcasted_iota(jnp.int32, (BLOCK, BLOCK), 0)
+    s_at = lax.broadcasted_iota(jnp.int32, (BLOCK, BLOCK), 1)
+    causal = t_at >= s_at
+    lower = causal.astype(jnp.float32)
+    state = jnp.zeros((width, width), jnp.float32)
+    for n in range(length // BLOCK):
+        rows = slice(n * BLOCK, (n + 1) * BLOCK)
+        inner_log = jnp.dot(
+            lower, log_decay[rows], preferred_element_type=jnp.float32, precision=HIGHEST
+        )
+        keys = key_gate[rows]
+        values = value[rows].astype(jnp.bfloat16)
+        read_scaled = (reader[rows] * jnp.exp(inner_log)).astype(jnp.bfloat16)
+        key_scaled = (keys * jnp.exp(-inner_log)).astype(jnp.bfloat16)
+        scores = lax.dot_general(
+            read_scaled, key_scaled, (((1,), (1,)), ((), ())), preferred_element_type=jnp.float32
+        )
+        scores = jnp.where(causal, scores, 0.0).astype(jnp.bfloat16)
+        read = jnp.dot(scores, values, preferred_element_type=jnp.float32)
+        read = read + jnp.dot(
+            read_scaled, state.astype(jnp.bfloat16), preferred_element_type=jnp.float32
+        )
+        closing = inner_log[BLOCK - 1 : BLOCK]
+        key_tail = (keys * jnp.exp(closing - inner_log)).astype(jnp.bfloat16)
+        added = lax.dot_general(
+            key_tail, values, (((0,), (0,)), ((), ())), preferred_element_type=jnp.float32
+        )
+        kept_share = jnp.broadcast_to(jnp.exp(closing), (width, width)).T
+        state = kept_share * state + added
+        mixed[pl.ds(n * BLOCK, BLOCK), pl.ds(width, width)] = (
+            rms_scale(read, 1.0) * head_gain
+        ).astype(jnp.bfloat16)
+    for p in range(planes):
+        for target, side in ((sent, 1 - core), (kept, core)):
+            top = pl.multiple_of((p * cores + side) * rows_each, rows_each)
+            target[p] = jnp.dot(
+                mixed[pl.ds(top, rows_each), :], weight_out[...], preferred_element_type=jnp.float32
+            ).astype(jnp.bfloat16)
+
+
+def by_heads(
+    tokens,
+    input_norm_gain,
+    pooling_input_weight,
+    query_weight,
+    forget_weight,
+    value_weight,
+    pooling_group_maps,
+    pooling_scale,
+    lower_bound_logits,
+    decay_spike,
+    head_norm_gain,
+    pooling_output_weight,
+    recurrent_output_weight,
+):
+    planes, members, cores = (lax.axis_size(axis) for axis in ("sp", "fs", "tp"))
+    plane, _, core = (lax.axis_index(axis) for axis in ("sp", "fs", "tp"))
+    heads = decay_spike.shape[2]
+    head = cores * plane + core
+    column = head % heads
+    partner_column = (cores * plane + 1 - core) % heads
+    width = query_weight.shape[1] // heads
+    features = tokens.shape[2]
+    rows_each = tokens.shape[1]
+    inputs = (pooling_input_weight, query_weight, forget_weight, value_weight)
+    outputs = (pooling_output_weight, recurrent_output_weight)
+    message = jax.ShapeDtypeStruct((width + width // 2, 4 * width), jnp.bfloat16)
+    block = jax.ShapeDtypeStruct(((members + 2) * width, 4 * width), jnp.bfloat16)
+    hbm = pl.BlockSpec(memory_space=pl.ANY)
+    vmem = pl.BlockSpec(memory_space=pltpu.VMEM)
+
+    def pack(*refs):
+        pack_kernel(planes, members, width, rows_each, *refs)
+
+    *messages, partner_block, own_local, own_message = pl.pallas_call(
+        pack,
+        out_shape=[message] * planes
+        + [block] * 2
+        + [jax.ShapeDtypeStruct((rows_each + 8, features), jnp.bfloat16)],
+        in_specs=[vmem] * 11,
+        out_specs=[vmem] * (planes + 3),
+        scratch_shapes=[pltpu.VMEM(pooling_output_weight.shape, jnp.bfloat16)],
+        name="pack",
+    )(
+        tokens[0],
+        input_norm_gain[None],
+        decay_spike[0],
+        pooling_group_maps,
+        pooling_scale[None],
+        *inputs,
+        *outputs,
+    )
+
+    arrived = []
+    for step in range(planes):
+        pairs = [
+            (p * cores + c, heads * c + (p + step) % heads)
+            for p in range(planes)
+            for c in range(cores)
+        ]
+        arrived.append(lax.ppermute(messages[step], ("sp", "tp"), pairs))
+    gathered = jnp.stack(arrived)
+    others = jnp.stack(
+        [picked(gathered, (column - plane - k) % planes) for k in range(1, planes)]
+    )
+    pieces = [others]
+    for bits in range(1, members):
+        pieces.append(swapped(others, "fs", bits))
+    partner_local = swapped(partner_block, "tp", 1)
+
+    def own_vectors(place):
+        return jnp.stack(
+            [
+                lax.dynamic_slice_in_dim(v, place * width, width, 0)
+                for v in (lower_bound_logits, head_norm_gain)
+            ]
+        )
+
+    received_vectors = swapped(own_vectors(partner_column), "tp", 1)
+
+    own_rows = [own_message]
+    for step in range(1, planes):
+        own_rows.append(turned(own_message, "sp", step))
+    partner_rows = []
+    for step in range(planes):
+        partner_rows.append(swapped(own_rows[step], "tp", 1))
+
+    length = planes * cores * rows_each
+
+    def layer(*refs):
+        layer_kernel(planes, members, cores, width, rows_each, *refs)
+
+    half_shape = jax.ShapeDtypeStruct((planes, rows_each, features), jnp.bfloat16)
+    sent, kept = pl.pallas_call(
+        layer,
+        out_shape=[half_shape, half_shape],
+        in_specs=[vmem] * 2 + [hbm] * (cores * planes + members + 2),
+        out_specs=[vmem, vmem],
+        scratch_shapes=[
+            pltpu.VMEM((length, features), jnp.bfloat16),
+            pltpu.VMEM((features, 4 * width), jnp.bfloat16),
+            pltpu.VMEM((2 * width, planes * members * width), jnp.bfloat16),
+            pltpu.VMEM((planes * cores, 8, width), jnp.bfloat16),
+            pltpu.VMEM((length, 2 * width), jnp.bfloat16),
+            pltpu.SemaphoreType.DMA((2 * cores * planes + 2 + 5 * planes * members,)),
+        ],
+        name="layer",
+    )(
+        own_vectors(column),
+        received_vectors,
+        *own_rows,
+        *partner_rows,
+        *pieces,
+        own_local,
+        partner_local,
+    )
+
+    from_partner = swapped(sent, "tp", 1)
+
+    def joined(p):
+        return picked(kept, p).astype(jnp.float32) + picked(from_partner, p).astype(jnp.float32)
+
+    total = joined(plane)
+    for step in range(1, planes):
+        portion = joined((plane + step) % planes).astype(jnp.bfloat16)
+        total = total + turned(portion, "sp", step).astype(jnp.float32)
+    return total.astype(jnp.bfloat16)[None]
+
+
+def body(*arrays):
+    tokens, _, pool_in, query_in, _, _, maps, _, _, spike, _, pool_out, _ = arrays
+    if heads_divide(tokens, query_in, pool_in, maps, spike, pool_out):
+        return by_heads(*arrays)
+    return by_positions(*arrays)
+
+
+def by_positions(
     tokens,
     input_norm_gain,
     pooling_input_weight,

time: 247 us -> 123 us (0.50)
  the two profiles are of different devices: /device:TPU:0 before, /device:TPU:13 now
where the time goes in v2:
time: 123 us
  waiting for transfers between devices  74.7 us (61%)
  starting transfers between devices  25.1 us (20%)
  Pallas kernels  13.7 us (11%)
  local copies, waits for them, and re-layouts  4.84 us (4%)
  other arithmetic  3.93 us (3%)
    ppermute x10, waiting for transfers between devices, swapped(): lax.ppermute(value, axis, [(source, source ^ bits) for source in range(co...  26.1 us
    ppermute x4, waiting for transfers between devices, by_heads(): arrived.append(lax.ppermute(messages[step], ('sp', 'tp'), pairs))  25.2 us
    ppermute x6, waiting for transfers between devices, turned(): lax.ppermute(value, axis, [(source, (source + steps) % count) for source...  23.4 us
    ppermute x4, starting transfers between devices, by_heads(): arrived.append(lax.ppermute(messages[step], ('sp', 'tp'), pairs))  10.8 us
    pallas_call x1, Pallas kernels, by_heads(): pl.pallas_call(layer, out_shape=[half_shape, half_shape], in_specs=[vmem]...  9.61 us
    ppermute x6, starting transfers between devices, turned(): lax.ppermute(value, axis, [(source, (source + steps) % count) for source...  7.57 us
    ppermute x10, starting transfers between devices, swapped(): lax.ppermute(value, axis, [(source, source ^ bits) for source in range(co...  6.73 us
    unnamed x29, local copies, waits for them, and re-layouts  4.72 us
  transfers between devices with their start and end apart: 20, of which 13 were waited for; matrix products, arithmetic and copies ran while one was open for 1% of the time, Pallas kernels for 0%

profile of v2, /device:TPU:13, one launch (start us, length us, event | category | flops | bytes accessed | tf_op | source)
XLA Modules:
  0.0 122.6 jit_solution(18225166977963338489)
XLA Ops:
  0.0 1.4 %copy.14 = f32[1,128,4]{2,1,0:T(8,128)} copy(f32[1,128,4]{1,2,0:T(4,128)} %param.22) | data formatting | bytes 4096 | tf_op args[9]
  1.4 4.1 %pack.1 = (bf16[192,512]{1,0:T(8,128)(2,1)}, bf16[192,512]{1,0:T(8,128)(2,1)}, bf16[192,512]{1,0:T(8,128)(2,1)}, bf16[192,512]{1,0:T(8,128)(2,1)}, bf16[768,512]...) custom-call(bf16[64,2048]{1,0:T(8,128)(2,1)} %bitcast.35, f32[1,2048]{1,0:T(1,128)} %bitcast.40, ...), custom_call_target="tpu_custom_call" | custom-call | tf_op jit(solution)/shard_map/pack/pallas_call | solution.py:348
  5.5 1.3 %collective-permute-start.1 = (bf16[72,2048]{1,0:T(8,128)(2,1)}, bf16[72,2048]{1,0:T(8,128)(2,1)S(1)}, u32[]{:S(2)}, u32[]{:S(2)}) collective-permute-start(bf16[72,2048]{1,0:T(8,128)(2,1)} %get-tuple-element.14.refs_2_), channel_id=1, source_target_pairs={{0,8},{8,16},{16,24},{24,0},{1,9},{9,17},{17,25},{25,1},{2,10},{10... | collective-permute-start | bytes 884744 | tf_op jit(solution)/shard_map/ppermute | solution.py:58
  6.8 1.1 collective-permute-start.10
  7.9 3.3 %collective-permute-start.11 = (bf16[192,512]{1,0:T(8,128)(2,1)}, bf16[192,512]{1,0:T(8,128)(2,1)S(1)}, u32[]{:S(2)}, u32[]{:S(2)}) collective-permute-start(bf16[192,512]{1,0:T(8,128)(2,1)} %get-tuple-element.18), channel_id=1, source_target_pairs={{0,9},{1,25},{8,0},{9,16},{16,1},{17,17},{24,8},{25,24},{2,11},{3,... | collective-permute-start | bytes 589832 | tf_op jit(solution)/shard_map/ppermute | solution.py:374
  11.2 1.9 %collective-permute-start.8 = (bf16[192,512]{1,0:T(8,128)(2,1)}, bf16[192,512]{1,0:T(8,128)(2,1)S(1)}, u32[]{:S(2)}, u32[]{:S(2)}) collective-permute-start(bf16[192,512]{1,0:T(8,128)(2,1)} %get-tuple-element.15), channel_id=1, source_target_pairs={{0,0},{1,16},{8,1},{9,17},{16,8},{17,24},{24,9},{25,25},{2,2},{3,1... | collective-permute-start | bytes 589832 | tf_op jit(solution)/shard_map/ppermute | solution.py:374
  13.1 4.5 %collective-permute-start.9 = (bf16[192,512]{1,0:T(8,128)(2,1)}, bf16[192,512]{1,0:T(8,128)(2,1)S(1)}, u32[]{:S(2)}, u32[]{:S(2)}) collective-permute-start(bf16[192,512]{1,0:T(8,128)(2,1)} %get-tuple-element.16), channel_id=1, source_target_pairs={{0,1},{1,17},{8,8},{9,24},{16,9},{17,25},{24,0},{25,16},{2,3},{3,1... | collective-permute-start | bytes 589832 | tf_op jit(solution)/shard_map/ppermute | solution.py:374
  17.8 0.7 copy-done.11
  18.5 0.7 collective-permute-done.10
  19.3 2.8 %collective-permute-start.2 = (bf16[72,2048]{1,0:T(8,128)(2,1)}, bf16[72,2048]{1,0:T(8,128)(2,1)S(1)}, u32[]{:S(2)}, u32[]{:S(2)}) collective-permute-start(bf16[72,2048]{1,0:T(8,128)(2,1)} %get-tuple-element.14.refs_2_), channel_id=1, source_target_pairs={{0,16},{8,24},{16,0},{24,8},{1,17},{9,25},{17,1},{25,9},{2,18},{10... | collective-permute-start | bytes 884744 | tf_op jit(solution)/shard_map/ppermute | solution.py:58
  22.1 18.1 %collective-permute-done.11 = bf16[192,512]{1,0:T(8,128)(2,1)S(1)} collective-permute-done((bf16[192,512]{1,0:T(8,128)(2,1)}, bf16[192,512]{1,0:T(8,128)(2,1)S(1)}, u32[]{:S(2)}, u32[]{:S(2)}) %collective-permute-start.11) | collective-permute-done | bytes 196640 | tf_op jit(solution)/shard_map/ppermute | solution.py:374
  40.2 4.2 %collective-permute-done.8 = bf16[192,512]{1,0:T(8,128)(2,1)S(1)} collective-permute-done((bf16[192,512]{1,0:T(8,128)(2,1)}, bf16[192,512]{1,0:T(8,128)(2,1)S(1)}, u32[]{:S(2)}, u32[]{:S(2)}) %collective-permute-start.8) | collective-permute-done | bytes 196640 | tf_op jit(solution)/shard_map/ppermute | solution.py:374
  44.4 2.1 %collective-permute-done.9 = bf16[192,512]{1,0:T(8,128)(2,1)S(1)} collective-permute-done((bf16[192,512]{1,0:T(8,128)(2,1)}, bf16[192,512]{1,0:T(8,128)(2,1)S(1)}, u32[]{:S(2)}, u32[]{:S(2)}) %collective-permute-start.9) | collective-permute-done | bytes 196640 | tf_op jit(solution)/shard_map/ppermute | solution.py:374
  48.5 1.2 %collective-permute-done.2.refs_4_ = bf16[72,2048]{1,0:T(8,128)(2,1)S(1)} collective-permute-done((bf16[72,2048]{1,0:T(8,128)(2,1)}, bf16[72,2048]{1,0:T(8,128)(2,1)S(1)}, u32[]{:S(2)}, u32[]{:S(2)}) %collective-permute-start.2) | collective-permute-done | bytes 294944 | tf_op jit(solution)/shard_map/ppermute | solution.py:58
  49.8 1.2 collective-permute-start.12
  51.0 0.9 collective-permute-start.6
  52.1 2.2 %collective-permute-start.14 = (bf16[3,192,512]{2,1,0:T(8,128)(2,1)S(1)}, bf16[3,192,512]{2,1,0:T(8,128)(2,1)S(1)}, u32[]{:S(2)}, u32[]{:S(2)}) collective-permute-start(bf16[3,192,512]{2,1,0:T(8,128)(2,1)S(1)} %pad_maximum_fusion.1.refs_10_), channel_id=1, source_target_pairs={{0,6},{2,4},{4,2},{6,0},{1,7},{3,5},{5,3},{7,1},{8,14},{10,12},{12... | collective-permute-start | bytes 1769480 | tf_op jit(solution)/shard_map/ppermute | solution.py:53
  54.2 0.7 copy-done.8
  56.2 0.6 collective-permute-done.7.refs_9_
  56.8 8.3 %collective-permute-done.12.refs_11_ = bf16[3,192,512]{2,1,0:T(8,128)(2,1)S(1)} collective-permute-done((bf16[3,192,512]{2,1,0:T(8,128)(2,1)S(1)}, bf16[3,192,512]{2,1,0:T(8,128)(2,1)S(1)}, u32[]{:S(2)}, u32[]{:S(2)}) %collective-permute-start.12) | collective-permute-done | bytes 589856 | tf_op jit(solution)/shard_map/ppermute | solution.py:53
  65.1 14.2 %collective-permute-done.13.refs_12_ = bf16[3,192,512]{2,1,0:T(8,128)(2,1)S(1)} collective-permute-done((bf16[3,192,512]{2,1,0:T(8,128)(2,1)S(1)}, bf16[3,192,512]{2,1,0:T(8,128)(2,1)S(1)}, u32[]{:S(2)}, u32[]{:S(2)}) %collective-permute-start.13) | collective-permute-done | bytes 589856 | tf_op jit(solution)/shard_map/ppermute | solution.py:53
  79.4 0.8 copy-done.3
  80.6 9.6 %layer.1 = (bf16[4,64,2048]{2,1,0:T(8,128)(2,1)}, bf16[4,64,2048]{2,1,0:T(8,128)(2,1)}) custom-call(f32[2,128]{1,0:T(2,128)} %pad_maximum_fusion.2.refs_0_, f32[2,128]{1,0:T(2,128)} %copy-done.10, bf16[72,2048]{1,0:T(8,128)(2,1)} %get-tuple-element.14.refs_2_, bf16[72,2048]{1,0:T(8,128)(2,1)} %copy-done.5, bf16[72,2048]{1,0:T(8,128)(2,1)} %copy-done.6, ...), custom_call_target="tpu_custom_call" | custom-call | tf_op jit(solution)/shard_map/layer/pallas_call | solution.py:407
  90.3 1.0 collective-permute-start.16
  91.2 2.5 %collective-permute-done.16 = bf16[4,64,2048]{2,1,0:T(8,128)(2,1)S(1)} collective-permute-done((bf16[4,64,2048]{2,1,0:T(8,128)(2,1)}, bf16[4,64,2048]{2,1,0:T(8,128)(2,1)S(1)}, u32[]{:S(2)}, u32[]{:S(2)}) %collective-permute-start.16) | collective-permute-done | bytes 1048608 | tf_op jit(solution)/shard_map/ppermute | solution.py:53
  93.7 1.4 %fusion.3 = (bf16[64,2048]{1,0:T(8,128)(2,1)S(1)}, bf16[64,2048]{1,0:T(8,128)(2,1)S(1)}, bf16[64,2048]{1,0:T(8,128)(2,1)S(1)}) fusion(bf16[4,64,2048]{2,1,0:T(8,128)(2,1)S(1)} %collective-permute-done.16, s32[]{:T(128)S(6)} %select_n.82, bf16[4,64,2048]{2,1,0:T(8,128)(2,1)} %get-tuple-element.21, s32[]{:T(128)S(6)} %select_n.86, s32[]{:T(128)S(6)} %select_n.84), kind=kLoop, calls=%fused_computation.9 | loop fusion | flops 1572864 | bytes 2359308 | tf_op jit(solution)/shard_map/convert_element_type | solution.py:438
  95.2 2.0 %collective-permute-start.18 = (bf16[64,2048]{1,0:T(8,128)(2,1)S(1)}, bf16[64,2048]{1,0:T(8,128)(2,1)S(1)}, u32[]{:S(2)}, u32[]{:S(2)}) collective-permute-start(bf16[64,2048]{1,0:T(8,128)(2,1)S(1)} %get-tuple-element.25), channel_id=1, source_target_pairs={{0,16},{8,24},{16,0},{24,8},{1,17},{9,25},{17,1},{25,9},{2,18},{10... | collective-permute-start | bytes 786440 | tf_op jit(solution)/shard_map/ppermute | solution.py:58
  97.2 1.4 %collective-permute-start.19 = (bf16[64,2048]{1,0:T(8,128)(2,1)S(1)}, bf16[64,2048]{1,0:T(8,128)(2,1)S(1)}, u32[]{:S(2)}, u32[]{:S(2)}) collective-permute-start(bf16[64,2048]{1,0:T(8,128)(2,1)S(1)} %get-tuple-element.24), channel_id=1, source_target_pairs={{0,24},{8,0},{16,8},{24,16},{1,25},{9,1},{17,9},{25,17},{2,26},{10... | collective-permute-start | bytes 786440 | tf_op jit(solution)/shard_map/ppermute | solution.py:58
  98.5 4.1 %collective-permute-done.17 = bf16[64,2048]{1,0:T(8,128)(2,1)S(1)} collective-permute-done((bf16[64,2048]{1,0:T(8,128)(2,1)S(1)}, bf16[64,2048]{1,0:T(8,128)(2,1)S(1)}, u32[]{:S(2)}, u32[]{:S(2)}) %collective-permute-start.17) | collective-permute-done | bytes 262176 | tf_op jit(solution)/shard_map/ppermute | solution.py:58
  102.7 14.9 %collective-permute-done.18 = bf16[64,2048]{1,0:T(8,128)(2,1)S(1)} collective-permute-done((bf16[64,2048]{1,0:T(8,128)(2,1)S(1)}, bf16[64,2048]{1,0:T(8,128)(2,1)S(1)}, u32[]{:S(2)}, u32[]{:S(2)}) %collective-permute-start.18) | collective-permute-done | bytes 262176 | tf_op jit(solution)/shard_map/ppermute | solution.py:58
  117.6 3.1 %collective-permute-done.19 = bf16[64,2048]{1,0:T(8,128)(2,1)S(1)} collective-permute-done((bf16[64,2048]{1,0:T(8,128)(2,1)S(1)}, bf16[64,2048]{1,0:T(8,128)(2,1)S(1)}, u32[]{:S(2)}, u32[]{:S(2)}) %collective-permute-start.19) | collective-permute-done | bytes 262176 | tf_op jit(solution)/shard_map/ppermute | solution.py:58
  120.7 1.8 %fusion.6 = bf16[1,64,2048]{2,1,0:T(8,128)(2,1)} fusion(bf16[64,2048]{1,0:T(8,128)(2,1)S(1)} %collective-permute-done.19, bf16[64,2048]{1,0:T(8,128)(2,1)S(1)} %collective-permute-done.18, bf16[64,2048]{1,0:T(8,128)(2,1)S(1)} %collective-permute-done.17, bf16[4,64,2048]{2,1,0:T(8,128)(2,1)S(1)} %collective-permute-done.16, s32[]{:T(128)S(6)} %select_n.80, ...), kind=kLoop, calls=%fused_computation.12 | loop fusion | flops 1310720 | bytes 1572868 | tf_op jit(solution)/shard_map/broadcast_in_dim | solution.py:440
  (47 shorter events, 4.0 us)
Async XLA Ops:
  5.5 41.1 %collective-permute-start.1 = (bf16[72,2048]{1,0:T(8,128)(2,1)}, bf16[72,2048]{1,0:T(8,128)(2,1)S(1)}, u32[]{:S(2)}, u32[]{:S(2)}) collective-permute-start(bf16[72,2048]{1,0:T(8,128)(2,1)} %get-tuple-element.14.refs_2_), channel_id=1, source_target_pairs={{0,8},{8,16},{16,24},{24,0},{1,9},{9,17},{17,25},{25,1},{2,10},{10... | collective-permute-start | bytes 884744 | tf_op jit(solution)/shard_map/ppermute | solution.py:58
  6.8 12.5 %collective-permute-start.10 = (bf16[192,512]{1,0:T(8,128)(2,1)}, bf16[192,512]{1,0:T(8,128)(2,1)S(1)}, u32[]{:S(2)}, u32[]{:S(2)}) collective-permute-start(bf16[192,512]{1,0:T(8,128)(2,1)} %get-tuple-element.17), channel_id=1, source_target_pairs={{0,8},{1,24},{8,9},{9,25},{16,0},{17,16},{24,1},{25,17},{2,10},{3,... | collective-permute-start | bytes 589832 | tf_op jit(solution)/shard_map/ppermute | solution.py:374
  7.9 32.4 %collective-permute-start.11 = (bf16[192,512]{1,0:T(8,128)(2,1)}, bf16[192,512]{1,0:T(8,128)(2,1)S(1)}, u32[]{:S(2)}, u32[]{:S(2)}) collective-permute-start(bf16[192,512]{1,0:T(8,128)(2,1)} %get-tuple-element.18), channel_id=1, source_target_pairs={{0,9},{1,25},{8,0},{9,16},{16,1},{17,17},{24,8},{25,24},{2,11},{3,... | collective-permute-start | bytes 589832 | tf_op jit(solution)/shard_map/ppermute | solution.py:374
  11.2 33.3 %collective-permute-start.8 = (bf16[192,512]{1,0:T(8,128)(2,1)}, bf16[192,512]{1,0:T(8,128)(2,1)S(1)}, u32[]{:S(2)}, u32[]{:S(2)}) collective-permute-start(bf16[192,512]{1,0:T(8,128)(2,1)} %get-tuple-element.15), channel_id=1, source_target_pairs={{0,0},{1,16},{8,1},{9,17},{16,8},{17,24},{24,9},{25,25},{2,2},{3,1... | collective-permute-start | bytes 589832 | tf_op jit(solution)/shard_map/ppermute | solution.py:374
  13.1 33.5 %collective-permute-start.9 = (bf16[192,512]{1,0:T(8,128)(2,1)}, bf16[192,512]{1,0:T(8,128)(2,1)S(1)}, u32[]{:S(2)}, u32[]{:S(2)}) collective-permute-start(bf16[192,512]{1,0:T(8,128)(2,1)} %get-tuple-element.16), channel_id=1, source_target_pairs={{0,1},{1,17},{8,8},{9,24},{16,9},{17,25},{24,0},{25,16},{2,3},{3,1... | collective-permute-start | bytes 589832 | tf_op jit(solution)/shard_map/ppermute | solution.py:374
  17.8 0.7 copy-start.12
  19.3 30.5 %collective-permute-start.2 = (bf16[72,2048]{1,0:T(8,128)(2,1)}, bf16[72,2048]{1,0:T(8,128)(2,1)S(1)}, u32[]{:S(2)}, u32[]{:S(2)}) collective-permute-start(bf16[72,2048]{1,0:T(8,128)(2,1)} %get-tuple-element.14.refs_2_), channel_id=1, source_target_pairs={{0,16},{8,24},{16,0},{24,8},{1,17},{9,25},{17,1},{25,9},{2,18},{10... | collective-permute-start | bytes 884744 | tf_op jit(solution)/shard_map/ppermute | solution.py:58
  40.2 10.7 %collective-permute-start.3 = (bf16[72,2048]{1,0:T(8,128)(2,1)}, bf16[72,2048]{1,0:T(8,128)(2,1)S(1)}, u32[]{:S(2)}, u32[]{:S(2)}) collective-permute-start(bf16[72,2048]{1,0:T(8,128)(2,1)} %get-tuple-element.14.refs_2_), channel_id=1, source_target_pairs={{0,24},{8,0},{16,8},{24,16},{1,25},{9,1},{17,9},{25,17},{2,26},{10... | collective-permute-start | bytes 884744 | tf_op jit(solution)/shard_map/ppermute | solution.py:58
  44.4 7.4 %collective-permute-start.4 = (bf16[72,2048]{1,0:T(8,128)(2,1)}, bf16[72,2048]{1,0:T(8,128)(2,1)}, u32[]{:S(2)}, u32[]{:S(2)}) collective-permute-start(bf16[72,2048]{1,0:T(8,128)(2,1)} %get-tuple-element.14.refs_2_), channel_id=1, source_target_pairs={{0,1},{1,0},{2,3},{3,2},{4,5},{5,4},{6,7},{7,6},{8,9},{9,8},{10,11... | collective-permute-start | bytes 884744 | tf_op jit(solution)/shard_map/ppermute | solution.py:53
  46.6 1.2 collective-permute-start
  46.6 0.7 copy-start.5
  46.6 5.5 %collective-permute-start.5 = (bf16[72,2048]{1,0:T(8,128)(2,1)S(1)}, bf16[72,2048]{1,0:T(8,128)(2,1)}, u32[]{:S(2)}, u32[]{:S(2)}) collective-permute-start(bf16[72,2048]{1,0:T(8,128)(2,1)S(1)} %collective-permute-done.1.refs_3_), channel_id=1, source_target_pairs={{0,1},{1,0},{2,3},{3,2},{4,5},{5,4},{6,7},{7,6},{8,9},{9,8},{10,11... | collective-permute-start | bytes 884744 | tf_op jit(solution)/shard_map/ppermute | solution.py:53
  47.1 1.1 copy-start.13
  48.2 31.1 %collective-permute-start.15 = (bf16[768,512]{1,0:T(8,128)(2,1)S(1)}, bf16[768,512]{1,0:T(8,128)(2,1)S(1)}, u32[]{:S(2)}, u32[]{:S(2)}) collective-permute-start(bf16[768,512]{1,0:T(8,128)(2,1)S(1)} %copy-done.13), channel_id=1, source_target_pairs={{0,1},{1,0},{2,3},{3,2},{4,5},{5,4},{6,7},{7,6},{8,9},{9,8},{10,11... | collective-permute-start | bytes 2359304 | tf_op jit(solution)/shard_map/ppermute | solution.py:53
  48.5 30.8 %copy-start = (bf16[3,192,512]{2,1,0:T(8,128)(2,1)}, bf16[3,192,512]{2,1,0:T(8,128)(2,1)S(1)}, u32[]{:S(2)}) copy-start(bf16[3,192,512]{2,1,0:T(8,128)(2,1)S(1)} %pad_maximum_fusion.1.refs_10_) | copy-start | bytes 1769476
  49.7 29.6 %copy-start.6 = (bf16[72,2048]{1,0:T(8,128)(2,1)}, bf16[72,2048]{1,0:T(8,128)(2,1)S(1)}, u32[]{:S(2)}) copy-start(bf16[72,2048]{1,0:T(8,128)(2,1)S(1)} %collective-permute-done.2.refs_4_) | copy-start | bytes 884740
  49.8 15.3 %collective-permute-start.12 = (bf16[3,192,512]{2,1,0:T(8,128)(2,1)S(1)}, bf16[3,192,512]{2,1,0:T(8,128)(2,1)S(1)}, u32[]{:S(2)}, u32[]{:S(2)}) collective-permute-start(bf16[3,192,512]{2,1,0:T(8,128)(2,1)S(1)} %pad_maximum_fusion.1.refs_10_), channel_id=1, source_target_pairs={{0,2},{2,0},{4,6},{6,4},{1,3},{3,1},{5,7},{7,5},{8,10},{10,8},{12,... | collective-permute-start | bytes 1769480 | tf_op jit(solution)/shard_map/ppermute | solution.py:53
  51.0 28.3 %copy-start.7 = (bf16[72,2048]{1,0:T(8,128)(2,1)}, bf16[72,2048]{1,0:T(8,128)(2,1)S(1)}, u32[]{:S(2)}) copy-start(bf16[72,2048]{1,0:T(8,128)(2,1)S(1)} %collective-permute-done.3.refs_5_) | copy-start | bytes 884740
  51.0 3.3 %collective-permute-start.6 = (bf16[72,2048]{1,0:T(8,128)(2,1)S(1)}, bf16[72,2048]{1,0:T(8,128)(2,1)S(1)}, u32[]{:S(2)}, u32[]{:S(2)}) collective-permute-start(bf16[72,2048]{1,0:T(8,128)(2,1)S(1)} %collective-permute-done.2.refs_4_), channel_id=1, source_target_pairs={{0,1},{1,0},{2,3},{3,2},{4,5},{5,4},{6,7},{7,6},{8,9},{9,8},{10,11... | collective-permute-start | bytes 884744 | tf_op jit(solution)/shard_map/ppermute | solution.py:53
  51.8 27.5 %collective-permute-start.13 = (bf16[3,192,512]{2,1,0:T(8,128)(2,1)S(1)}, bf16[3,192,512]{2,1,0:T(8,128)(2,1)S(1)}, u32[]{:S(2)}, u32[]{:S(2)}) collective-permute-start(bf16[3,192,512]{2,1,0:T(8,128)(2,1)S(1)} %pad_maximum_fusion.1.refs_10_), channel_id=1, source_target_pairs={{0,4},{2,6},{4,0},{6,2},{1,5},{3,7},{5,1},{7,3},{8,12},{10,14},{12... | collective-permute-start | bytes 1769480 | tf_op jit(solution)/shard_map/ppermute | solution.py:53
  52.1 27.2 %collective-permute-start.14 = (bf16[3,192,512]{2,1,0:T(8,128)(2,1)S(1)}, bf16[3,192,512]{2,1,0:T(8,128)(2,1)S(1)}, u32[]{:S(2)}, u32[]{:S(2)}) collective-permute-start(bf16[3,192,512]{2,1,0:T(8,128)(2,1)S(1)} %pad_maximum_fusion.1.refs_10_), channel_id=1, source_target_pairs={{0,6},{2,4},{4,2},{6,0},{1,7},{3,5},{5,3},{7,1},{8,14},{10,12},{12... | collective-permute-start | bytes 1769480 | tf_op jit(solution)/shard_map/ppermute | solution.py:53
  54.2 0.7 copy-start.8
  55.0 1.8 %collective-permute-start.7 = (bf16[72,2048]{1,0:T(8,128)(2,1)S(1)}, bf16[72,2048]{1,0:T(8,128)(2,1)S(1)}, u32[]{:S(2)}, u32[]{:S(2)}) collective-permute-start(bf16[72,2048]{1,0:T(8,128)(2,1)S(1)} %collective-permute-done.3.refs_5_), channel_id=1, source_target_pairs={{0,1},{1,0},{2,3},{3,2},{4,5},{5,4},{6,7},{7,6},{8,9},{9,8},{10,11... | collective-permute-start | bytes 884744 | tf_op jit(solution)/shard_map/ppermute | solution.py:53
  56.8 22.5 %copy-start.9 = (bf16[72,2048]{1,0:T(8,128)(2,1)}, bf16[72,2048]{1,0:T(8,128)(2,1)S(1)}, u32[]{:S(2)}) copy-start(bf16[72,2048]{1,0:T(8,128)(2,1)S(1)} %collective-permute-done.7.refs_9_) | copy-start | bytes 884740
  65.1 14.3 %copy-start.2 = (bf16[3,192,512]{2,1,0:T(8,128)(2,1)}, bf16[3,192,512]{2,1,0:T(8,128)(2,1)S(1)}, u32[]{:S(2)}) copy-start(bf16[3,192,512]{2,1,0:T(8,128)(2,1)S(1)} %collective-permute-done.12.refs_11_) | copy-start | bytes 1769476
  79.3 0.8 copy-start.3
  79.3 1.1 copy-start.4
  79.3 1.3 %copy-start.1 = (bf16[768,512]{1,0:T(8,128)(2,1)}, bf16[768,512]{1,0:T(8,128)(2,1)S(1)}, u32[]{:S(2)}) copy-start(bf16[768,512]{1,0:T(8,128)(2,1)S(1)} %collective-permute-done.15.refs_15_) | copy-start | bytes 2359300
  90.3 3.5 %collective-permute-start.16 = (bf16[4,64,2048]{2,1,0:T(8,128)(2,1)}, bf16[4,64,2048]{2,1,0:T(8,128)(2,1)S(1)}, u32[]{:S(2)}, u32[]{:S(2)}) collective-permute-start(bf16[4,64,2048]{2,1,0:T(8,128)(2,1)} %get-tuple-element.22), channel_id=1, source_target_pairs={{0,1},{1,0},{2,3},{3,2},{4,5},{5,4},{6,7},{7,6},{8,9},{9,8},{10,11... | collective-permute-start | bytes 3145736 | tf_op jit(solution)/shard_map/ppermute | solution.py:53
  95.1 7.5 %collective-permute-start.17 = (bf16[64,2048]{1,0:T(8,128)(2,1)S(1)}, bf16[64,2048]{1,0:T(8,128)(2,1)S(1)}, u32[]{:S(2)}, u32[]{:S(2)}) collective-permute-start(bf16[64,2048]{1,0:T(8,128)(2,1)S(1)} %get-tuple-element.23), channel_id=1, source_target_pairs={{0,8},{8,16},{16,24},{24,0},{1,9},{9,17},{17,25},{25,1},{2,10},{10... | collective-permute-start | bytes 786440 | tf_op jit(solution)/shard_map/ppermute | solution.py:58
  95.2 22.4 %collective-permute-start.18 = (bf16[64,2048]{1,0:T(8,128)(2,1)S(1)}, bf16[64,2048]{1,0:T(8,128)(2,1)S(1)}, u32[]{:S(2)}, u32[]{:S(2)}) collective-permute-start(bf16[64,2048]{1,0:T(8,128)(2,1)S(1)} %get-tuple-element.25), channel_id=1, source_target_pairs={{0,16},{8,24},{16,0},{24,8},{1,17},{9,25},{17,1},{25,9},{2,18},{10... | collective-permute-start | bytes 786440 | tf_op jit(solution)/shard_map/ppermute | solution.py:58
  97.2 23.6 %collective-permute-start.19 = (bf16[64,2048]{1,0:T(8,128)(2,1)S(1)}, bf16[64,2048]{1,0:T(8,128)(2,1)S(1)}, u32[]{:S(2)}, u32[]{:S(2)}) collective-permute-start(bf16[64,2048]{1,0:T(8,128)(2,1)S(1)} %get-tuple-element.24), channel_id=1, source_target_pairs={{0,24},{8,0},{16,8},{24,16},{1,25},{9,1},{17,9},{25,17},{2,26},{10... | collective-permute-start | bytes 786440 | tf_op jit(solution)/shard_map/ppermute | solution.py:58
  (2 other events, 1.3 us)

commit v3 on v0

--- a/solution.py
+++ b/solution.py
@@ -1,6 +1,8 @@
 import jax
 import jax.numpy as jnp
 from jax import lax
+from jax.experimental import pallas as pl
+from jax.experimental.pallas import tpu as pltpu
 from jax.sharding import PartitionSpec as P
 
 BLOCK = 64
@@ -46,7 +48,541 @@
     return (decay_one * decay_two, decay_two[..., None] * state_one + state_two)
 
 
-def body(
+def swapped(value, axis, bits):
+    count = lax.axis_size(axis)
+    return lax.ppermute(value, axis, [(source, source ^ bits) for source in range(count)])
+
+
+def picked(stack, place, axis=0):
+    return lax.dynamic_index_in_dim(stack, place, axis, False)
+
+
+def halves_divide(tokens, query_weight, pooling_input_weight, pooling_group_maps, decay_spike, out_weight):
+    planes, members, cores = (lax.axis_size(axis) for axis in ("sp", "fs", "tp"))
+    heads = decay_spike.shape[2]
+    width = query_weight.shape[1] // heads
+    return (
+        cores == 2
+        and planes == 2 * cores
+        and members == 2 * cores
+        and heads == 2 * cores
+        and width % 128 == 0
+        and pooling_group_maps.shape[0] * 2 == heads
+        and pooling_input_weight.shape[1] == query_weight.shape[1]
+        and tokens.shape[0] == 1
+        and tokens.shape[1] % BLOCK == 0
+        and decay_spike.shape[1] == cores * tokens.shape[1] == width
+        and query_weight.shape[0] == heads * width
+        and out_weight.shape[1] == heads * width
+        and 2 ** (2 * pooling_group_maps.shape[0]) <= HALO
+    )
+
+
+HALO = 16
+
+
+def places():
+    plane, member, core = (lax.axis_index(axis) for axis in ("sp", "fs", "tp"))
+    late, half = lax.div(plane, 2), lax.rem(plane, 2)
+    row, side = lax.div(member, 2), lax.rem(member, 2)
+    return plane, late, half, row, side, core
+
+
+def first_kernel(width, rows_each, *refs):
+    tokens, gain, spikes = refs[:3]
+    inputs, messages, rows_out, sems = refs[3:7], refs[7:9], refs[9], refs[10]
+    _, _, half, row, side, core = places()
+    part = inputs[0].shape[0] // 2
+    top = pl.multiple_of(side * part, part)
+    first = jnp.where(core == half, 0, 1)
+    copies = []
+    for n in range(2):
+        place = 2 * row + jnp.where(n == 0, first, 1 - first)
+        column = pl.multiple_of(place * width, width)
+        for m, w in enumerate(inputs):
+            copies.append(
+                pltpu.make_async_copy(
+                    w.at[pl.ds(top, part), pl.ds(column, width)],
+                    messages[n].at[:, pl.ds(m * width, width)],
+                    sems.at[n * 4 + m],
+                )
+            )
+    for copy in copies:
+        copy.start()
+    values = tokens[...].astype(jnp.float32)
+    rows_out[pl.ds(0, rows_each), :] = rms_scale(values, gain[...]).astype(jnp.bfloat16)
+    rows_out[pl.ds(rows_each, 8), :] = jnp.zeros((8, rows_out.shape[1]), jnp.bfloat16)
+    upper = spikes[...].astype(jnp.bfloat16)
+    lower = (spikes[...] - upper.astype(jnp.float32)).astype(jnp.bfloat16)
+    rows_out[pl.ds(rows_each, 8), pl.ds(0, width)] = jnp.concatenate([upper, lower], axis=0)
+    for copy in copies:
+        copy.wait()
+
+
+def pack_kernel(width, *refs):
+    maps, scale, bound, head_gain = refs[:4]
+    inputs, outputs = refs[4:8], refs[8:10]
+    out_messages, block, own, own_vectors, partner_vectors, pooling_rows, sems = (
+        refs[10:12],
+        *refs[12:],
+    )
+    _, _, half, row, side, core = places()
+    part = inputs[0].shape[0] // 2
+    rows = 2 * part
+    ends = ((2 * row + 1 - core, block), (2 * row + core, own))
+    copies = []
+    for n, (place, target) in enumerate(ends):
+        column = pl.multiple_of(place * width, width)
+        for m, w in enumerate(inputs):
+            copies.append(
+                pltpu.make_async_copy(
+                    w.at[:, pl.ds(column, width)],
+                    target.at[pl.ds(0, rows), pl.ds(m * width, width)],
+                    sems.at[n * 4 + m],
+                )
+            )
+    for copy in copies:
+        copy.start()
+    for place, target in ((2 * row + core, own_vectors), (2 * row + 1 - core, partner_vectors)):
+        column = pl.ds(pl.multiple_of(place * width, width), width)
+        for n, vector in enumerate((bound, head_gain)):
+            target[pl.ds(n, 1), :] = vector[:, column]
+    groups, size = maps.shape[:2]
+    for g in range(groups):
+        span = pl.ds(g * size, size)
+        scaled = maps[g].astype(jnp.float32) * scale[:, span]
+        high = scaled.astype(jnp.bfloat16)
+        rest = (scaled - high.astype(jnp.float32)).astype(jnp.bfloat16)
+        pooled = outputs[0][span, :]
+        pooling_rows[span, :] = (
+            jnp.dot(high, pooled, preferred_element_type=jnp.float32)
+            + jnp.dot(rest, pooled, preferred_element_type=jnp.float32)
+        ).astype(jnp.bfloat16)
+    outputs = (pooling_rows, outputs[1])
+    top = pl.multiple_of(side * part, part)
+    first = jnp.where(core == half, 0, 1)
+    for n in range(2):
+        place = 2 * row + jnp.where(n == 0, first, 1 - first)
+        column = pl.multiple_of(place * width, width)
+        for m, w in enumerate(outputs):
+            out_messages[n][pl.ds(m * width, width), :] = w[pl.ds(column, width), pl.ds(top, part)]
+    for place, target in ends:
+        column = pl.multiple_of(place * width, width)
+        for m, w in enumerate(outputs):
+            target[pl.ds(rows + m * width, width), :] = w[pl.ds(column, width), :]
+    for copy in copies:
+        copy.wait()
+
+
+def down(values, steps):
+    rows = lax.broadcasted_iota(jnp.int32, values.shape, 0)
+    return jnp.where(rows >= steps, pltpu.roll(values, steps, 0), 0.0)
+
+
+def piece_sources(pieces, plane, core):
+    planes = lax.axis_size("sp")
+    near, far, third = pieces[0:2], pieces[2:4], (pieces[4:6], pieces[6:8])
+    always = [(near, lax.rem(plane + 2 - core, planes)), (far, lax.rem(plane + 1 + core, planes))]
+    last = lax.rem(plane + 3, planes)
+    return always, third, last
+
+
+def start_pieces(pieces, blocks, sems, used, plane, side, core, owns, piece_target, block_target):
+    always, third, last = piece_sources(pieces, plane, core)
+    waits = []
+
+    def copies(pair, source, slot):
+        return [
+            pltpu.make_async_copy(
+                pair[n], piece_target(source, side if n == 0 else 1 - side), sems.at[slot + n]
+            )
+            for n in range(2)
+        ]
+
+    for pair, source in always:
+        group = copies(pair, source, used)
+        for copy in group:
+            copy.start()
+        waits += group
+        used += 2
+    choices = [copies(pair, last, used) for pair in third]
+    for n in range(2):
+
+        @pl.when(core == n)
+        def _(n=n):
+            for copy in choices[n]:
+                copy.start()
+
+    waits += choices[0]
+    used += 2
+    own = [pltpu.make_async_copy(block_target(b)[0], block_target(b)[1], sems.at[used]) for b in blocks]
+    for n in range(2):
+
+        @pl.when(owns if n == 0 else jnp.logical_not(owns))
+        def _(n=n):
+            own[n].start()
+
+    waits.append(own[0])
+    return waits, used + 1
+
+
+def state_kernel(width, rows_each, *refs):
+    own_vectors, partner_vectors = refs[:2]
+    tokens, pieces, blocks = refs[2:10], refs[10:18], refs[18:20]
+    read_local, read_full, pool_rows, carry = refs[20:24]
+    token_all, weight_in, spikes, sems = refs[24:]
+    plane, _, half, row, side, core = places()
+    owns = core == half
+    column = 2 * row + core
+    plane_rows = 4 * width
+    part = plane_rows // 2
+    waits = []
+    used = 0
+    for a in range(2):
+        for b in range(2):
+            for c in range(2):
+                piece = tokens[(a * 2 + b) * 2 + c]
+                order = ((row ^ b) * 2 + (half ^ a)) * 2 + (core ^ c)
+                top = pl.multiple_of(order * rows_each, rows_each)
+                waits.append(
+                    pltpu.make_async_copy(
+                        piece.at[pl.ds(0, rows_each), :],
+                        token_all.at[pl.ds(top, rows_each), :],
+                        sems.at[used],
+                    )
+                )
+                waits.append(
+                    pltpu.make_async_copy(
+                        piece.at[pl.ds(rows_each, 8), pl.ds(0, width)],
+                        spikes.at[order],
+                        sems.at[used + 1],
+                    )
+                )
+                used += 2
+    for copy in waits:
+        copy.start()
+
+    def piece_target(source, x):
+        return weight_in.at[pl.ds(pl.multiple_of(source * plane_rows + x * part, part), part), :]
+
+    def block_target(block):
+        return (
+            block.at[pl.ds(0, plane_rows), :],
+            weight_in.at[pl.ds(pl.multiple_of(plane * plane_rows, plane_rows), plane_rows), :],
+        )
+
+    more, used = start_pieces(
+        pieces, blocks, sems, used, plane, side, core, owns, piece_target, block_target
+    )
+    for copy in waits + more:
+        copy.wait()
+    lower_bound = jnp.where(owns, own_vectors[pl.ds(0, 1), :], partner_vectors[pl.ds(0, 1), :])
+    projected = jnp.dot(token_all[...], weight_in[...], preferred_element_type=jnp.float32)
+    projected = projected.astype(jnp.bfloat16)
+    pool_rows[...] = projected[:, :width]
+    query, forget_logit, value = (
+        projected[:, n * width : (n + 1) * width].astype(jnp.float32) for n in range(1, 4)
+    )
+    spike_row = lax.broadcasted_iota(jnp.int32, (8, width), 0)
+    wanted_row = jnp.logical_or(spike_row == column, spike_row == column + 4)
+    spike_columns = []
+    for n in range(4):
+        parts = spikes[2 * n + half].astype(jnp.float32)
+        line = jnp.sum(jnp.where(wanted_row, parts, 0.0), axis=0, keepdims=True)
+        spike_columns.append(jnp.broadcast_to(line, (width, width)).T)
+    spike = jnp.concatenate(spike_columns, axis=0)
+    reader = query * jax.nn.sigmoid(query)
+    key_gate = jax.nn.sigmoid(-lower_bound) * jax.nn.sigmoid(-forget_logit)
+    log_decay = jnp.log1p(-key_gate) + spike
+    t_at = lax.broadcasted_iota(jnp.int32, (BLOCK, BLOCK), 0)
+    s_at = lax.broadcasted_iota(jnp.int32, (BLOCK, BLOCK), 1)
+    causal = t_at >= s_at
+    lower = causal.astype(jnp.float32)
+    length = 4 * rows_each
+    states = [jnp.zeros((width, width), jnp.float32)] * 2
+    before = [jnp.zeros((1, width), jnp.float32)] * 2
+    for n in range(length // BLOCK):
+        for seq in range(2):
+            begin = seq * length + n * BLOCK
+            rows = slice(begin, begin + BLOCK)
+            inner_log = jnp.dot(
+                lower, log_decay[rows], preferred_element_type=jnp.float32, precision=HIGHEST
+            )
+            keys = key_gate[rows]
+            values = value[rows].astype(jnp.bfloat16)
+            grown = reader[rows] * jnp.exp(inner_log)
+            read_scaled = grown.astype(jnp.bfloat16)
+            key_scaled = (keys * jnp.exp(-inner_log)).astype(jnp.bfloat16)
+            scores = lax.dot_general(
+                read_scaled, key_scaled, (((1,), (1,)), ((), ())), preferred_element_type=jnp.float32
+            )
+            scores = jnp.where(causal, scores, 0.0).astype(jnp.bfloat16)
+            read = jnp.dot(scores, values, preferred_element_type=jnp.float32)
+            if n > 0:
+                read = read + jnp.dot(
+                    read_scaled,
+                    states[seq].astype(jnp.bfloat16),
+                    preferred_element_type=jnp.float32,
+                )
+            closing = inner_log[BLOCK - 1 : BLOCK]
+            key_tail = (keys * jnp.exp(closing - inner_log)).astype(jnp.bfloat16)
+            added = lax.dot_general(
+                key_tail, values, (((0,), (0,)), ((), ())), preferred_element_type=jnp.float32
+            )
+            share = jnp.broadcast_to(jnp.exp(closing), (width, width)).T
+            states[seq] = share * states[seq] + added
+            read_local[pl.ds(begin, BLOCK), :] = read
+            read_full[pl.ds(begin, BLOCK), :] = (grown * jnp.exp(before[seq])).astype(jnp.bfloat16)
+            before[seq] = before[seq] + closing
+    for seq in range(2):
+        top = seq * (width + HALO)
+        carry[pl.ds(top, width), :] = states[seq].astype(jnp.bfloat16)
+        carry[pl.ds(top + width, HALO), :] = projected[
+            (seq + 1) * length - HALO : (seq + 1) * length, :width
+        ]
+
+
+def output_kernel(width, rows_each, *refs):
+    own_vectors, partner_vectors, read_local, read_full, pool_rows, carry = refs[:6]
+    pieces, blocks = refs[6:14], refs[14:16]
+    sent, kept = refs[16:18]
+    weight_out, mixed, sems = refs[18:]
+    plane, late, half, row, side, core = places()
+    owns = core == half
+    plane_rows = 4 * width
+    part = plane_rows // 2
+    length = 4 * rows_each
+
+    def piece_target(source, x):
+        return weight_out.at[:, pl.ds(pl.multiple_of(source * plane_rows + x * part, part), part)]
+
+    def block_target(block):
+        return (
+            block.at[pl.ds(plane_rows, 2 * width), :],
+            weight_out.at[:, pl.ds(pl.multiple_of(plane * plane_rows, plane_rows), plane_rows)],
+        )
+
+    waits, _ = start_pieces(
+        pieces, blocks, sems, 0, plane, side, core, owns, piece_target, block_target
+    )
+    head_gain = jnp.where(owns, own_vectors[pl.ds(1, 1), :], partner_vectors[pl.ds(1, 1), :])
+    group = 2 * half + row
+    window = jnp.left_shift(jnp.int32(2), group)
+    for seq in range(2):
+        top = seq * (width + HALO)
+        rows = pl.ds(seq * length, length)
+        extended = jnp.concatenate(
+            [carry[pl.ds(top + width, HALO), :], pool_rows[rows, :]], axis=0
+        ).astype(jnp.float32)
+        window_sum = extended
+        chosen = jnp.zeros_like(extended)
+        for g in range(4):
+            window_sum = window_sum + down(window_sum, 2**g)
+            chosen = jnp.where(group == g, window_sum, chosen)
+        at = lax.broadcasted_iota(jnp.int32, (length, width), 0) + late * length
+        counts = jnp.minimum(at + 1, window).astype(jnp.float32)
+        mixed[rows, pl.ds(0, width)] = (chosen[HALO:] / counts - extended[HALO:]).astype(
+            jnp.bfloat16
+        )
+        read = read_local[rows, :] + jnp.dot(
+            read_full[rows, :], carry[pl.ds(top, width), :], preferred_element_type=jnp.float32
+        )
+        mixed[rows, pl.ds(width, width)] = (rms_scale(read, 1.0) * head_gain).astype(jnp.bfloat16)
+    for copy in waits:
+        copy.wait()
+    for target, c in ((sent, 1 - core), (kept, core)):
+        for n in range(4):
+            top = pl.multiple_of((n * 2 + c) * rows_each, rows_each)
+            target[n // 2, n % 2] = jnp.dot(
+                mixed[pl.ds(top, rows_each), :], weight_out[...], preferred_element_type=jnp.float32
+            ).astype(jnp.bfloat16)
+
+
+def by_halves(
+    tokens,
+    input_norm_gain,
+    pooling_input_weight,
+    query_weight,
+    forget_weight,
+    value_weight,
+    pooling_group_maps,
+    pooling_scale,
+    lower_bound_logits,
+    decay_spike,
+    head_norm_gain,
+    pooling_output_weight,
+    recurrent_output_weight,
+):
+    planes, members, cores = (lax.axis_size(axis) for axis in ("sp", "fs", "tp"))
+    _, _, half, row, _, _ = places()
+    heads = decay_spike.shape[2]
+    width = query_weight.shape[1] // heads
+    features = tokens.shape[2]
+    rows_each = tokens.shape[1]
+    part = query_weight.shape[0] // 2
+    hbm = pl.BlockSpec(memory_space=pl.ANY)
+    vmem = pl.BlockSpec(memory_space=pltpu.VMEM)
+
+    def made(*shape, kind=jnp.bfloat16):
+        return jax.ShapeDtypeStruct(shape, kind)
+
+    def pack(*refs):
+        pack_kernel(width, *refs)
+
+    weights_in = (pooling_input_weight, query_weight, forget_weight, value_weight)
+
+    def first(*refs):
+        first_kernel(width, rows_each, *refs)
+
+    *messages, own_rows = pl.pallas_call(
+        first,
+        out_shape=[made(part, 4 * width)] * 2 + [made(rows_each + 8, features)],
+        in_specs=[vmem] * 3 + [hbm] * 4,
+        out_specs=[vmem] * 3,
+        scratch_shapes=[pltpu.SemaphoreType.DMA((8,))],
+        name="first",
+    )(tokens[0], input_norm_gain[None], decay_spike[0].T, *weights_in)
+    block = made(2 * part + 2 * width, 4 * width)
+    *out_messages, partner_block, own_local, vectors, partner_vectors = pl.pallas_call(
+        pack,
+        out_shape=[made(2 * width, part)] * 2
+        + [block] * 2
+        + [made(2, width, kind=jnp.float32)] * 2,
+        in_specs=[vmem] * 4 + [hbm] * 4 + [vmem] * 2,
+        out_specs=[vmem] * 6,
+        scratch_shapes=[
+            pltpu.VMEM(pooling_output_weight.shape, jnp.bfloat16),
+            pltpu.SemaphoreType.DMA((8,)),
+        ],
+        name="pack",
+    )(
+        pooling_group_maps,
+        pooling_scale[None],
+        lower_bound_logits[None],
+        head_norm_gain[None],
+        *weights_in,
+        pooling_output_weight,
+        recurrent_output_weight,
+    )
+
+    def hops(wanted):
+        return [
+            (((p + k) % planes) * cores + p % cores, p * cores + c)
+            for p in range(planes)
+            for k, c in wanted
+        ]
+
+    rounds = (
+        (0, hops([(2, 0), (1, 1)])),
+        (1, hops([(2, 1), (1, 0)])),
+        (1, hops([(3, 0)])),
+        (0, hops([(3, 1)])),
+    )
+
+    def shared(pair):
+        pieces = []
+        for n, (which, pairs) in enumerate(rounds):
+            arrived = lax.ppermute(pair[which], ("sp", "tp"), pairs)
+            pieces.append(arrived)
+            used = range(cores) if n < 2 else (n - 2,)
+            across = [(f * cores + c, (f ^ 1) * cores + c) for f in range(members) for c in used]
+            pieces.append(lax.ppermute(arrived, ("fs", "tp"), across))
+        return pieces
+
+    input_pieces = shared(messages)
+    output_pieces = shared(out_messages)
+    partner_local = swapped(partner_block, "tp", 1)
+
+    received_vectors = swapped(partner_vectors, "tp", 1)
+    other_rows = swapped(own_rows, "sp", 1)
+    chip_rows = []
+    for rows in (own_rows, other_rows):
+        chip_rows += [rows, swapped(rows, "fs", 2)]
+    token_pieces = []
+    for rows in chip_rows:
+        token_pieces += [rows, swapped(rows, "tp", 1)]
+
+    length = 8 * rows_each
+    carry_shape = made(2 * (width + HALO), width)
+
+    def state(*refs):
+        state_kernel(width, rows_each, *refs)
+
+    read_local, read_full, pool_rows, carry = pl.pallas_call(
+        state,
+        out_shape=[
+            made(length, width, kind=jnp.float32),
+            made(length, width),
+            made(length, width),
+            carry_shape,
+        ],
+        in_specs=[vmem] * 2 + [hbm] * 18,
+        out_specs=[vmem] * 4,
+        scratch_shapes=[
+            pltpu.VMEM((length, features), jnp.bfloat16),
+            pltpu.VMEM((features, 4 * width), jnp.bfloat16),
+            pltpu.VMEM((8, 8, width), jnp.bfloat16),
+            pltpu.SemaphoreType.DMA((23,)),
+        ],
+        name="state",
+    )(vectors, received_vectors, *token_pieces, *input_pieces, own_local, partner_local)
+    entering_carry = lax.ppermute(carry, "sp", [(p, p + 2) for p in range(planes - 2)])
+
+    def output(*refs):
+        output_kernel(width, rows_each, *refs)
+
+    half_shape = made(2, 2, rows_each, features)
+    sent, kept = pl.pallas_call(
+        output,
+        out_shape=[half_shape] * 2,
+        in_specs=[vmem] * 6 + [hbm] * 10,
+        out_specs=[vmem] * 2,
+        scratch_shapes=[
+            pltpu.VMEM((2 * width, features), jnp.bfloat16),
+            pltpu.VMEM((length, 2 * width), jnp.bfloat16),
+            pltpu.SemaphoreType.DMA((7,)),
+        ],
+        name="output",
+    )(
+        vectors,
+        received_vectors,
+        read_local,
+        read_full,
+        pool_rows,
+        entering_carry,
+        *output_pieces,
+        own_local,
+        partner_local,
+    )
+    from_partner = swapped(sent, "tp", 1)
+    middle = features // 2
+
+    def joined(place, axis, columns):
+        return sum(
+            picked(v[..., columns], place, axis).astype(jnp.float32) for v in (kept, from_partner)
+        )
+
+    left, right = slice(0, middle), slice(middle, features)
+    left_in = swapped(joined(1 - row, 0, left).astype(jnp.bfloat16), "fs", 2)
+    right_in = swapped(joined(1 - half, 1, right).astype(jnp.bfloat16), "sp", 1)
+    left_sum = joined(row, 0, left) + left_in.astype(jnp.float32)
+    right_sum = joined(half, 1, right) + right_in.astype(jnp.float32)
+    left_last = swapped(picked(left_sum, 1 - half).astype(jnp.bfloat16), "sp", 1)
+    right_last = swapped(picked(right_sum, 1 - row).astype(jnp.bfloat16), "fs", 2)
+    left_total = picked(left_sum, half) + left_last.astype(jnp.float32)
+    right_total = picked(right_sum, row) + right_last.astype(jnp.float32)
+    total = jnp.concatenate([left_total, right_total], axis=1)
+    return total.astype(jnp.bfloat16)[None]
+
+
+def body(*arrays):
+    tokens, _, pool_in, query_in, _, _, maps, _, _, spike, _, pool_out, _ = arrays
+    if halves_divide(tokens, query_in, pool_in, maps, spike, pool_out):
+        return by_halves(*arrays)
+    return by_positions(*arrays)
+
+
+def by_positions(
     tokens,
     input_norm_gain,
     pooling_input_weight,

time: 247 us -> 116 us (0.47)
  waiting for transfers between devices: 185 us -> 50.3 us
  starting transfers between devices: 3.58 us -> 42.2 us
  blocking collectives: 26.1 us -> 0 us
  Pallas kernels: 0 us -> 19.2 us
  between operations: 13.5 us -> 0.45 us
  matrix products: 11.1 us -> 0 us
  other arithmetic: 5.86 us -> 1.12 us
    all_gather x4 -> x0, waiting for transfers between devices: 177 us -> none  [the longest x1 88.5 us: body(): full_input = lax.all_gather(column_part, 'fs', axis=1, tiled=True)]
    ppermute x1 -> x31, waiting for transfers between devices: 0.01 us -> 50.3 us  [the longest x8 21.2 us: shared(): arrived = lax.ppermute(pair[which], ('sp', 'tp'), pairs)]
    ppermute x1 -> x31, starting transfers between devices: 3.39 us -> 42.2 us  [the longest x14 13 us: swapped(): lax.ppermute(value, axis, [(source, source ^ bits) for source in range(co...]
    all_gather x3 -> x0, blocking collectives: 26.1 us -> none  [the longest x2 23.9 us: entering(): lax.all_gather(a.astype(kind), axis)]
    pallas_call x0 -> x4, Pallas kernels: none -> 19.2 us  [the longest x1 6.59 us: by_halves(): pl.pallas_call(state, out_shape=[made(length, width, kind=jnp.float32), m...]
    dot_general x7 -> x0, matrix products: 11.1 us -> none  [the longest x1 4.68 us: body(): projected = jnp.dot(normed, full_input, preferred_element_type=jnp.float32)]
    reduce_scatter x1 -> x0, waiting for transfers between devices: 8.08 us -> none  [body(): lax.psum_scatter(jnp.dot(mixed_rows, out_full, preferred_element_type=jnp...]
    concatenate x2 -> x3, other arithmetic: 4.15 us -> 0.78 us  [by_halves(): total = jnp.concatenate([left_total, right_total], axis=1)]
  transfers between devices with their start and end apart: 6 -> 31, of which waited for: 5 -> 11; matrix products, arithmetic and copies ran while one was open for 5% -> 1% of each run, Pallas kernels for 0% -> 8%
where the time goes in v3:
time: 116 us
  waiting for transfers between devices  50.3 us (43%)
  starting transfers between devices  42.2 us (36%)
  Pallas kernels  19.2 us (17%)
  local copies, waits for them, and re-layouts  2.74 us (2%)
    ppermute x8, waiting for transfers between devices, shared(): arrived = lax.ppermute(pair[which], ('sp', 'tp'), pairs)  21.2 us
    ppermute x8, waiting for transfers between devices, shared(): pieces.append(lax.ppermute(arrived, ('fs', 'tp'), across))  13.8 us
    ppermute x14, waiting for transfers between devices, swapped(): lax.ppermute(value, axis, [(source, source ^ bits) for source in range(co...  13.1 us
    ppermute x14, starting transfers between devices, swapped(): lax.ppermute(value, axis, [(source, source ^ bits) for source in range(co...  13 us
    ppermute x8, starting transfers between devices, shared(): pieces.append(lax.ppermute(arrived, ('fs', 'tp'), across))  12.9 us
    ppermute x8, starting transfers between devices, shared(): arrived = lax.ppermute(pair[which], ('sp', 'tp'), pairs)  11.9 us
    pallas_call x1, Pallas kernels, by_halves(): pl.pallas_call(state, out_shape=[made(length, width, kind=jnp.float32), m...  6.59 us
    pallas_call x1, Pallas kernels, by_halves(): pl.pallas_call(output, out_shape=[half_shape] * 2, in_specs=[vmem] * 6 +...  5.34 us
  transfers between devices with their start and end apart: 31, of which 11 were waited for; matrix products, arithmetic and copies ran while one was open for 1% of the time, Pallas kernels for 8%

profile of v3, /device:TPU:0, one launch (start us, length us, event | category | flops | bytes accessed | tf_op | source)
XLA Modules:
  0.0 115.9 jit_solution(2555320348251556068)
XLA Ops:
  0.0 4.2 %pack.1 = (bf16[256,256]{1,0:T(8,128)(2,1)}, bf16[256,256]{1,0:T(8,128)(2,1)}, bf16[768,512]{1,0:T(8,128)(2,1)}, bf16[768,512]{1,0:T(8,128)(2,1)}, f32[2,128]{1,0:T(2,128)}, /*index=5*/f32[2,128]{1,0:T(2,128)}) custom-call(bf16[2,256,256]{2,1,0:T(8,128)(2,1)} %refs_0_.1, f32[1,512]{1,0:T(1,128)} %bitcast.38, f32[1,512]{1,0:T(1,128)} %bitcast.39, ...), custom_call_target="tpu_custom_call" | custom-call | tf_op jit(solution)/shard_map/pack/pallas_call | solution.py:446
  4.2 4.1 %collective-permute-start.18 = (bf16[256,256]{1,0:T(8,128)(2,1)}, bf16[256,256]{1,0:T(8,128)(2,1)S(1)}, u32[]{:S(2)}, u32[]{:S(2)}) collective-permute-start(bf16[256,256]{1,0:T(8,128)(2,1)} %get-tuple-element.31), channel_id=1, source_target_pairs={{16,0},{8,1},{25,8},{17,9},{0,16},{24,17},{9,24},{1,25},{18,2},{10... | collective-permute-start | bytes 393224 | tf_op jit(solution)/shard_map/ppermute | solution.py:485
  8.3 3.1 %first.1 = (bf16[256,512]{1,0:T(8,128)(2,1)}, bf16[256,512]{1,0:T(8,128)(2,1)}, bf16[72,2048]{1,0:T(8,128)(2,1)}) custom-call(bf16[64,2048]{1,0:T(8,128)(2,1)} %bitcast.36, f32[1,2048]{1,0:T(1,128)} %bitcast.37, f32[4,128]{1,0:T(4,128)} %bitcast.41, bf16[512,512]{1,0:T(8,128)(2,1)} %refs_3_.1, bf16[512,512]{1,0:T(8,128)(2,1)} %refs_4_.3, ...), custom_call_target="tpu_custom_call" | custom-call | tf_op jit(solution)/shard_map/first/pallas_call | solution.py:437
  11.7 1.3 %collective-permute-start.12 = (bf16[256,512]{1,0:T(8,128)(2,1)}, bf16[256,512]{1,0:T(8,128)(2,1)S(1)}, u32[]{:S(2)}, u32[]{:S(2)}) collective-permute-start(bf16[256,512]{1,0:T(8,128)(2,1)} %get-tuple-element.24), channel_id=1, source_target_pairs={{24,0},{1,8},{8,16},{17,24},{26,2},{3,10},{10,18},{19,26},{28,4},{... | collective-permute-start | bytes 786440 | tf_op jit(solution)/shard_map/ppermute | solution.py:485
  13.0 2.6 %collective-permute-start = (f32[2,128]{1,0:T(2,128)S(1)}, f32[2,128]{1,0:T(2,128)S(1)}, u32[]{:S(2)}, u32[]{:S(2)}) collective-permute-start(f32[2,128]{1,0:T(2,128)S(1)} %copy-done.20), channel_id=1, source_target_pairs={{0,1},{1,0},{2,3},{3,2},{4,5},{5,4},{6,7},{7,6},{8,9},{9,8},{10,11... | collective-permute-start | bytes 3080 | tf_op jit(solution)/shard_map/ppermute | solution.py:53
  17.2 1.3 %collective-permute-start.22 = (bf16[256,256]{1,0:T(8,128)(2,1)S(1)}, bf16[256,256]{1,0:T(8,128)(2,1)}, u32[]{:S(2)}, u32[]{:S(2)}) collective-permute-start(bf16[256,256]{1,0:T(8,128)(2,1)S(1)} %copy-done.19), channel_id=1, source_target_pairs={{24,0},{1,8},{8,16},{17,24},{26,2},{3,10},{10,18},{19,26},{28,4},{... | collective-permute-start | bytes 393224 | tf_op jit(solution)/shard_map/ppermute | solution.py:485
  18.5 1.3 %collective-permute-start.24 = (bf16[256,256]{1,0:T(8,128)(2,1)S(1)}, bf16[256,256]{1,0:T(8,128)(2,1)}, u32[]{:S(2)}, u32[]{:S(2)}) collective-permute-start(bf16[256,256]{1,0:T(8,128)(2,1)S(1)} %copy-done.18), channel_id=1, source_target_pairs={{24,1},{1,9},{8,17},{17,25},{26,3},{3,11},{10,19},{19,27},{28,5},{... | collective-permute-start | bytes 393224 | tf_op jit(solution)/shard_map/ppermute | solution.py:485
  19.8 12.3 %collective-permute-done.22.refs_10_ = bf16[256,256]{1,0:T(8,128)(2,1)} collective-permute-done((bf16[256,256]{1,0:T(8,128)(2,1)S(1)}, bf16[256,256]{1,0:T(8,128)(2,1)}, u32[]{:S(2)}, u32[]{:S(2)}) %collective-permute-start.22) | collective-permute-done | bytes 131104 | tf_op jit(solution)/shard_map/ppermute | solution.py:485
  32.1 2.4 %collective-permute-start.4 = (bf16[72,2048]{1,0:T(8,128)(2,1)}, bf16[72,2048]{1,0:T(8,128)(2,1)S(1)}, u32[]{:S(2)}, u32[]{:S(2)}) collective-permute-start(bf16[72,2048]{1,0:T(8,128)(2,1)} %get-tuple-element.22.refs_2_), channel_id=1, source_target_pairs={{0,8},{8,0},{16,24},{24,16},{1,9},{9,1},{17,25},{25,17},{2,10},{10... | collective-permute-start | bytes 884744 | tf_op jit(solution)/shard_map/ppermute | solution.py:53
  34.5 1.5 %collective-permute-start.2 = (bf16[72,2048]{1,0:T(8,128)(2,1)}, bf16[72,2048]{1,0:T(8,128)(2,1)S(1)}, u32[]{:S(2)}, u32[]{:S(2)}) collective-permute-start(bf16[72,2048]{1,0:T(8,128)(2,1)} %get-tuple-element.22.refs_2_), channel_id=1, source_target_pairs={{0,4},{2,6},{4,0},{6,2},{1,5},{3,7},{5,1},{7,3},{8,12},{10,14},{12... | collective-permute-start | bytes 884744 | tf_op jit(solution)/shard_map/ppermute | solution.py:53
  36.1 2.9 %collective-permute-start.8 = (bf16[256,512]{1,0:T(8,128)(2,1)}, bf16[256,512]{1,0:T(8,128)(2,1)S(1)}, u32[]{:S(2)}, u32[]{:S(2)}) collective-permute-start(bf16[256,512]{1,0:T(8,128)(2,1)} %get-tuple-element.23), channel_id=1, source_target_pairs={{16,0},{8,1},{25,8},{17,9},{0,16},{24,17},{9,24},{1,25},{18,2},{10... | collective-permute-start | bytes 786440 | tf_op jit(solution)/shard_map/ppermute | solution.py:485
  39.8 8.8 %collective-permute-done.8.refs_10_ = bf16[256,512]{1,0:T(8,128)(2,1)S(1)} collective-permute-done((bf16[256,512]{1,0:T(8,128)(2,1)}, bf16[256,512]{1,0:T(8,128)(2,1)S(1)}, u32[]{:S(2)}, u32[]{:S(2)}) %collective-permute-start.8) | collective-permute-done | bytes 262176 | tf_op jit(solution)/shard_map/ppermute | solution.py:485
  48.6 1.5 %collective-permute-start.11 = (bf16[256,512]{1,0:T(8,128)(2,1)S(1)}, bf16[256,512]{1,0:T(8,128)(2,1)}, u32[]{:S(2)}, u32[]{:S(2)}) collective-permute-start(bf16[256,512]{1,0:T(8,128)(2,1)S(1)} %collective-permute-done.10.refs_12_), channel_id=1, source_target_pairs={{0,2},{1,3},{2,0},{3,1},{4,6},{5,7},{6,4},{7,5},{8,10},{9,11},{10,... | collective-permute-start | bytes 786440 | tf_op jit(solution)/shard_map/ppermute | solution.py:489
  50.1 2.4 %collective-permute-start.13 = (bf16[256,512]{1,0:T(8,128)(2,1)S(1)}, bf16[256,512]{1,0:T(8,128)(2,1)}, u32[]{:S(2)}, u32[]{:S(2)}) collective-permute-start(bf16[256,512]{1,0:T(8,128)(2,1)S(1)} %collective-permute-done.12.refs_14_), channel_id=1, source_target_pairs={{0,2},{2,0},{4,6},{6,4},{8,10},{10,8},{12,14},{14,12},{16,18},{18,... | collective-permute-start | bytes 786440 | tf_op jit(solution)/shard_map/ppermute | solution.py:489
  53.8 2.7 %collective-permute-done.11.refs_13_ = bf16[256,512]{1,0:T(8,128)(2,1)} collective-permute-done((bf16[256,512]{1,0:T(8,128)(2,1)S(1)}, bf16[256,512]{1,0:T(8,128)(2,1)}, u32[]{:S(2)}, u32[]{:S(2)}) %collective-permute-start.11) | collective-permute-done | bytes 262176 | tf_op jit(solution)/shard_map/ppermute | solution.py:489
  56.6 4.1 %collective-permute-done.13.refs_15_ = bf16[256,512]{1,0:T(8,128)(2,1)} collective-permute-done((bf16[256,512]{1,0:T(8,128)(2,1)S(1)}, bf16[256,512]{1,0:T(8,128)(2,1)}, u32[]{:S(2)}, u32[]{:S(2)}) %collective-permute-start.13) | collective-permute-done | bytes 262176 | tf_op jit(solution)/shard_map/ppermute | solution.py:489
  60.7 1.6 %collective-permute-start.9 = (bf16[256,512]{1,0:T(8,128)(2,1)S(1)}, bf16[256,512]{1,0:T(8,128)(2,1)S(1)}, u32[]{:S(2)}, u32[]{:S(2)}) collective-permute-start(bf16[256,512]{1,0:T(8,128)(2,1)S(1)} %collective-permute-done.8.refs_10_), channel_id=1, source_target_pairs={{0,2},{1,3},{2,0},{3,1},{4,6},{5,7},{6,4},{7,5},{8,10},{9,11},{10,... | collective-permute-start | bytes 786440 | tf_op jit(solution)/shard_map/ppermute | solution.py:489
  62.5 6.9 %collective-permute-done.9.refs_11_ = bf16[256,512]{1,0:T(8,128)(2,1)S(1)} collective-permute-done((bf16[256,512]{1,0:T(8,128)(2,1)S(1)}, bf16[256,512]{1,0:T(8,128)(2,1)S(1)}, u32[]{:S(2)}, u32[]{:S(2)}) %collective-permute-start.9) | collective-permute-done | bytes 262176 | tf_op jit(solution)/shard_map/ppermute | solution.py:489
  69.4 1.5 %collective-permute-start.19 = (bf16[256,256]{1,0:T(8,128)(2,1)S(1)}, bf16[256,256]{1,0:T(8,128)(2,1)}, u32[]{:S(2)}, u32[]{:S(2)}) collective-permute-start(bf16[256,256]{1,0:T(8,128)(2,1)S(1)} %collective-permute-done.18.refs_6_), channel_id=1, source_target_pairs={{0,2},{1,3},{2,0},{3,1},{4,6},{5,7},{6,4},{7,5},{8,10},{9,11},{10,... | collective-permute-start | bytes 393224 | tf_op jit(solution)/shard_map/ppermute | solution.py:489
  71.5 3.4 %collective-permute-start.23 = (bf16[256,256]{1,0:T(8,128)(2,1)}, bf16[256,256]{1,0:T(8,128)(2,1)}, u32[]{:S(2)}, u32[]{:S(2)}) collective-permute-start(bf16[256,256]{1,0:T(8,128)(2,1)} %collective-permute-done.22.refs_10_), channel_id=1, source_target_pairs={{0,2},{2,0},{4,6},{6,4},{8,10},{10,8},{12,14},{14,12},{16,18},{18,... | collective-permute-start | bytes 393224 | tf_op jit(solution)/shard_map/ppermute | solution.py:489
  74.9 1.3 %collective-permute-start.25 = (bf16[256,256]{1,0:T(8,128)(2,1)}, bf16[256,256]{1,0:T(8,128)(2,1)}, u32[]{:S(2)}, u32[]{:S(2)}) collective-permute-start(bf16[256,256]{1,0:T(8,128)(2,1)} %collective-permute-done.24.refs_12_), channel_id=1, source_target_pairs={{1,3},{3,1},{5,7},{7,5},{9,11},{11,9},{13,15},{15,13},{17,19},{19,... | collective-permute-start | bytes 393224 | tf_op jit(solution)/shard_map/ppermute | solution.py:489
  76.9 6.6 %state.1 = (f32[512,128]{1,0:T(8,128)}, bf16[512,128]{1,0:T(8,128)(2,1)}, bf16[512,128]{1,0:T(8,128)(2,1)}, bf16[288,128]{1,0:T(8,128)(2,1)}) custom-call(f32[2,128]{1,0:T(2,128)} %get-tuple-element.20.refs_0_, f32[2,128]{1,0:T(2,128)} %copy-done.17, bf16[72,2048]{1,0:T(8,128)(2,1)} %get-tuple-element.22.refs_2_, bf16[72,2048]{1,0:T(8,128)(2,1)} %copy-done.3, ...), custom_call_target="tpu_custom_call" | custom-call | tf_op jit(solution)/shard_map/state/pallas_call | solution.py:511
  83.5 4.3 %collective-permute-start.17 = (bf16[288,128]{1,0:T(8,128)(2,1)}, bf16[288,128]{1,0:T(8,128)(2,1)S(1)}, u32[]{:S(2)}, u32[]{:S(2)}) collective-permute-start(bf16[288,128]{1,0:T(8,128)(2,1)} %get-tuple-element.30), channel_id=1, source_target_pairs={{0,16},{8,24},{1,17},{9,25},{2,18},{10,26},{3,19},{11,27},{4,20},{... | collective-permute-start | bytes 221192 | tf_op jit(solution)/shard_map/ppermute | solution.py:529
  87.9 2.2 %collective-permute-done.17.refs_5_ = bf16[288,128]{1,0:T(8,128)(2,1)S(1)} collective-permute-done((bf16[288,128]{1,0:T(8,128)(2,1)}, bf16[288,128]{1,0:T(8,128)(2,1)S(1)}, u32[]{:S(2)}, u32[]{:S(2)}) %collective-permute-start.17) | collective-permute-done | bytes 73760 | tf_op jit(solution)/shard_map/ppermute | solution.py:529
  90.8 5.3 %output.1 = (bf16[2,2,64,2048]{3,2,1,0:T(8,128)(2,1)}, bf16[2,2,64,2048]{3,2,1,0:T(8,128)(2,1)}) custom-call(f32[2,128]{1,0:T(2,128)} %get-tuple-element.20.refs_0_, f32[2,128]{1,0:T(2,128)} %copy-done.17, f32[512,128]{1,0:T(8,128)} %get-tuple-element.27.refs_2_, bf16[512,128]{1,0:T(8,128)(2,1)} %get-tuple-element.28.refs_3_, ...), custom_call_target="tpu_custom_call" | custom-call | tf_op jit(solution)/shard_map/output/pallas_call | solution.py:535
  96.2 1.3 %fusion.8 = (bf16[2,2,64,1024]{3,2,1,0:T(8,128)(2,1)S(1)}, bf16[2,2,64,1024]{3,2,1,0:T(8,128)(2,1)S(1)}) fusion(bf16[2,2,64,2048]{3,2,1,0:T(8,128)(2,1)} %get-tuple-element.33), kind=kLoop, calls=%fused_computation.17 | loop fusion | bytes 2097152 | tf_op jit(solution)/shard_map/slice | solution.py:562
  97.5 1.5 %collective-permute-done.26 = bf16[2,2,64,2048]{3,2,1,0:T(8,128)(2,1)S(1)} collective-permute-done((bf16[2,2,64,2048]{3,2,1,0:T(8,128)(2,1)}, bf16[2,2,64,2048]{3,2,1,0:T(8,128)(2,1)S(1)}, u32[]{:S(2)}, u32[]{:S(2)}) %collective-permute-start.26) | collective-permute-done | bytes 1048608 | tf_op jit(solution)/shard_map/ppermute | solution.py:53
  99.2 1.3 %collective-permute-start.27 = (bf16[2,64,1024]{2,1,0:T(8,128)(2,1)S(1)}, bf16[2,64,1024]{2,1,0:T(8,128)(2,1)S(1)}, u32[]{:S(2)}, u32[]{:S(2)}) collective-permute-start(bf16[2,64,1024]{2,1,0:T(8,128)(2,1)S(1)} %fusion), channel_id=1, source_target_pairs={{0,4},{2,6},{4,0},{6,2},{1,5},{3,7},{5,1},{7,3},{8,12},{10,14},{12... | collective-permute-start | bytes 786440 | tf_op jit(solution)/shard_map/ppermute | solution.py:53
  101.6 6.0 %collective-permute-done.27 = bf16[2,64,1024]{2,1,0:T(8,128)(2,1)S(1)} collective-permute-done((bf16[2,64,1024]{2,1,0:T(8,128)(2,1)S(1)}, bf16[2,64,1024]{2,1,0:T(8,128)(2,1)S(1)}, u32[]{:S(2)}, u32[]{:S(2)}) %collective-permute-start.27) | collective-permute-done | bytes 262176 | tf_op jit(solution)/shard_map/ppermute | solution.py:53
  107.8 2.2 %collective-permute-start.28 = (bf16[64,1024]{1,0:T(8,128)(2,1)S(1)}, bf16[64,1024]{1,0:T(8,128)(2,1)S(1)}, u32[]{:S(2)}, u32[]{:S(2)}) collective-permute-start(bf16[64,1024]{1,0:T(8,128)(2,1)S(1)} %fusion.4), channel_id=1, source_target_pairs={{0,8},{8,0},{16,24},{24,16},{1,9},{9,1},{17,25},{25,17},{2,10},{10... | collective-permute-start | bytes 393224 | tf_op jit(solution)/shard_map/ppermute | solution.py:53
  110.5 2.5 %collective-permute-done.28 = bf16[64,1024]{1,0:T(8,128)(2,1)S(1)} collective-permute-done((bf16[64,1024]{1,0:T(8,128)(2,1)S(1)}, bf16[64,1024]{1,0:T(8,128)(2,1)S(1)}, u32[]{:S(2)}, u32[]{:S(2)}) %collective-permute-start.28) | collective-permute-done | bytes 131104 | tf_op jit(solution)/shard_map/ppermute | solution.py:53
  113.0 2.2 %collective-permute-done.30 = bf16[64,1024]{1,0:T(8,128)(2,1)S(1)} collective-permute-done((bf16[64,1024]{1,0:T(8,128)(2,1)S(1)}, bf16[64,1024]{1,0:T(8,128)(2,1)S(1)}, u32[]{:S(2)}, u32[]{:S(2)}) %collective-permute-start.30) | collective-permute-done | bytes 131104 | tf_op jit(solution)/shard_map/ppermute | solution.py:53
  (87 shorter events, 8.6 us)
Async XLA Ops:
  4.2 12.9 %collective-permute-start.18 = (bf16[256,256]{1,0:T(8,128)(2,1)}, bf16[256,256]{1,0:T(8,128)(2,1)S(1)}, u32[]{:S(2)}, u32[]{:S(2)}) collective-permute-start(bf16[256,256]{1,0:T(8,128)(2,1)} %get-tuple-element.31), channel_id=1, source_target_pairs={{16,0},{8,1},{25,8},{17,9},{0,16},{24,17},{9,24},{1,25},{18,2},{10... | collective-permute-start | bytes 393224 | tf_op jit(solution)/shard_map/ppermute | solution.py:485
  8.3 10.1 %collective-permute-start.20 = (bf16[256,256]{1,0:T(8,128)(2,1)}, bf16[256,256]{1,0:T(8,128)(2,1)S(1)}, u32[]{:S(2)}, u32[]{:S(2)}) collective-permute-start(bf16[256,256]{1,0:T(8,128)(2,1)} %get-tuple-element.32), channel_id=1, source_target_pairs={{16,1},{8,0},{25,9},{17,8},{0,17},{24,16},{9,25},{1,24},{18,3},{10... | collective-permute-start | bytes 393224 | tf_op jit(solution)/shard_map/ppermute | solution.py:485
  11.4 24.6 %collective-permute-start.10 = (bf16[256,512]{1,0:T(8,128)(2,1)}, bf16[256,512]{1,0:T(8,128)(2,1)S(1)}, u32[]{:S(2)}, u32[]{:S(2)}) collective-permute-start(bf16[256,512]{1,0:T(8,128)(2,1)} %get-tuple-element.24), channel_id=1, source_target_pairs={{16,1},{8,0},{25,9},{17,8},{0,17},{24,16},{9,25},{1,24},{18,3},{10... | collective-permute-start | bytes 786440 | tf_op jit(solution)/shard_map/ppermute | solution.py:485
  11.7 24.3 %collective-permute-start.12 = (bf16[256,512]{1,0:T(8,128)(2,1)}, bf16[256,512]{1,0:T(8,128)(2,1)S(1)}, u32[]{:S(2)}, u32[]{:S(2)}) collective-permute-start(bf16[256,512]{1,0:T(8,128)(2,1)} %get-tuple-element.24), channel_id=1, source_target_pairs={{24,0},{1,8},{8,16},{17,24},{26,2},{3,10},{10,18},{19,26},{28,4},{... | collective-permute-start | bytes 786440 | tf_op jit(solution)/shard_map/ppermute | solution.py:485
  13.0 3.4 %collective-permute-start = (f32[2,128]{1,0:T(2,128)S(1)}, f32[2,128]{1,0:T(2,128)S(1)}, u32[]{:S(2)}, u32[]{:S(2)}) collective-permute-start(f32[2,128]{1,0:T(2,128)S(1)} %copy-done.20), channel_id=1, source_target_pairs={{0,1},{1,0},{2,3},{3,2},{4,5},{5,4},{6,7},{7,6},{8,9},{9,8},{10,11... | collective-permute-start | bytes 3080 | tf_op jit(solution)/shard_map/ppermute | solution.py:53
  16.5 22.5 %collective-permute-start.14 = (bf16[256,512]{1,0:T(8,128)(2,1)}, bf16[256,512]{1,0:T(8,128)(2,1)S(1)}, u32[]{:S(2)}, u32[]{:S(2)}) collective-permute-start(bf16[256,512]{1,0:T(8,128)(2,1)} %get-tuple-element.23), channel_id=1, source_target_pairs={{24,1},{1,9},{8,17},{17,25},{26,3},{3,11},{10,19},{19,27},{28,5},{... | collective-permute-start | bytes 786440 | tf_op jit(solution)/shard_map/ppermute | solution.py:485
  17.2 66.4 %copy-start.14 = (bf16[256,256]{1,0:T(8,128)(2,1)}, bf16[256,256]{1,0:T(8,128)(2,1)S(1)}, u32[]{:S(2)}) copy-start(bf16[256,256]{1,0:T(8,128)(2,1)S(1)} %collective-permute-done.18.refs_6_) | copy-start | bytes 393220
  17.2 14.9 %collective-permute-start.22 = (bf16[256,256]{1,0:T(8,128)(2,1)S(1)}, bf16[256,256]{1,0:T(8,128)(2,1)}, u32[]{:S(2)}, u32[]{:S(2)}) collective-permute-start(bf16[256,256]{1,0:T(8,128)(2,1)S(1)} %copy-done.19), channel_id=1, source_target_pairs={{24,0},{1,8},{8,16},{17,24},{26,2},{3,10},{10,18},{19,26},{28,4},{... | collective-permute-start | bytes 393224 | tf_op jit(solution)/shard_map/ppermute | solution.py:485
  18.5 16.0 %collective-permute-start.24 = (bf16[256,256]{1,0:T(8,128)(2,1)S(1)}, bf16[256,256]{1,0:T(8,128)(2,1)}, u32[]{:S(2)}, u32[]{:S(2)}) collective-permute-start(bf16[256,256]{1,0:T(8,128)(2,1)S(1)} %copy-done.18), channel_id=1, source_target_pairs={{24,1},{1,9},{8,17},{17,25},{26,3},{3,11},{10,19},{19,27},{28,5},{... | collective-permute-start | bytes 393224 | tf_op jit(solution)/shard_map/ppermute | solution.py:485
  32.1 18.0 %collective-permute-start.4 = (bf16[72,2048]{1,0:T(8,128)(2,1)}, bf16[72,2048]{1,0:T(8,128)(2,1)S(1)}, u32[]{:S(2)}, u32[]{:S(2)}) collective-permute-start(bf16[72,2048]{1,0:T(8,128)(2,1)} %get-tuple-element.22.refs_2_), channel_id=1, source_target_pairs={{0,8},{8,0},{16,24},{24,16},{1,9},{9,1},{17,25},{25,17},{2,10},{10... | collective-permute-start | bytes 884744 | tf_op jit(solution)/shard_map/ppermute | solution.py:53
  34.5 18.0 %collective-permute-start.2 = (bf16[72,2048]{1,0:T(8,128)(2,1)}, bf16[72,2048]{1,0:T(8,128)(2,1)S(1)}, u32[]{:S(2)}, u32[]{:S(2)}) collective-permute-start(bf16[72,2048]{1,0:T(8,128)(2,1)} %get-tuple-element.22.refs_2_), channel_id=1, source_target_pairs={{0,4},{2,6},{4,0},{6,2},{1,5},{3,7},{5,1},{7,3},{8,12},{10,14},{12... | collective-permute-start | bytes 884744 | tf_op jit(solution)/shard_map/ppermute | solution.py:53
  36.0 17.1 %collective-permute-start.1 = (bf16[72,2048]{1,0:T(8,128)(2,1)}, bf16[72,2048]{1,0:T(8,128)(2,1)S(1)}, u32[]{:S(2)}, u32[]{:S(2)}) collective-permute-start(bf16[72,2048]{1,0:T(8,128)(2,1)} %get-tuple-element.22.refs_2_), channel_id=1, source_target_pairs={{0,1},{1,0},{2,3},{3,2},{4,5},{5,4},{6,7},{7,6},{8,9},{9,8},{10,11... | collective-permute-start | bytes 884744 | tf_op jit(solution)/shard_map/ppermute | solution.py:53
  36.1 12.6 %collective-permute-start.8 = (bf16[256,512]{1,0:T(8,128)(2,1)}, bf16[256,512]{1,0:T(8,128)(2,1)S(1)}, u32[]{:S(2)}, u32[]{:S(2)}) collective-permute-start(bf16[256,512]{1,0:T(8,128)(2,1)} %get-tuple-element.23), channel_id=1, source_target_pairs={{16,0},{8,1},{25,8},{17,9},{0,16},{24,17},{9,24},{1,25},{18,2},{10... | collective-permute-start | bytes 786440 | tf_op jit(solution)/shard_map/ppermute | solution.py:485
  39.0 35.9 %collective-permute-start.16 = (bf16[768,512]{1,0:T(8,128)(2,1)}, bf16[768,512]{1,0:T(8,128)(2,1)S(1)}, u32[]{:S(2)}, u32[]{:S(2)}) collective-permute-start(bf16[768,512]{1,0:T(8,128)(2,1)} %get-tuple-element.26), channel_id=1, source_target_pairs={{0,1},{1,0},{2,3},{3,2},{4,5},{5,4},{6,7},{7,6},{8,9},{9,8},{10,11... | collective-permute-start | bytes 2359304 | tf_op jit(solution)/shard_map/ppermute | solution.py:53
  48.6 8.0 %collective-permute-start.11 = (bf16[256,512]{1,0:T(8,128)(2,1)S(1)}, bf16[256,512]{1,0:T(8,128)(2,1)}, u32[]{:S(2)}, u32[]{:S(2)}) collective-permute-start(bf16[256,512]{1,0:T(8,128)(2,1)S(1)} %collective-permute-done.10.refs_12_), channel_id=1, source_target_pairs={{0,2},{1,3},{2,0},{3,1},{4,6},{5,7},{6,4},{7,5},{8,10},{9,11},{10,... | collective-permute-start | bytes 786440 | tf_op jit(solution)/shard_map/ppermute | solution.py:489
  50.1 10.6 %collective-permute-start.13 = (bf16[256,512]{1,0:T(8,128)(2,1)S(1)}, bf16[256,512]{1,0:T(8,128)(2,1)}, u32[]{:S(2)}, u32[]{:S(2)}) collective-permute-start(bf16[256,512]{1,0:T(8,128)(2,1)S(1)} %collective-permute-done.12.refs_14_), channel_id=1, source_target_pairs={{0,2},{2,0},{4,6},{6,4},{8,10},{10,8},{12,14},{14,12},{16,18},{18,... | collective-permute-start | bytes 786440 | tf_op jit(solution)/shard_map/ppermute | solution.py:489
  52.6 9.7 %collective-permute-start.6 = (bf16[72,2048]{1,0:T(8,128)(2,1)S(1)}, bf16[72,2048]{1,0:T(8,128)(2,1)S(1)}, u32[]{:S(2)}, u32[]{:S(2)}) collective-permute-start(bf16[72,2048]{1,0:T(8,128)(2,1)S(1)} %collective-permute-done.4.refs_6_), channel_id=1, source_target_pairs={{0,4},{2,6},{4,0},{6,2},{1,5},{3,7},{5,1},{7,3},{8,12},{10,14},{12... | collective-permute-start | bytes 884744 | tf_op jit(solution)/shard_map/ppermute | solution.py:53
  53.2 7.6 %collective-permute-start.15 = (bf16[256,512]{1,0:T(8,128)(2,1)S(1)}, bf16[256,512]{1,0:T(8,128)(2,1)S(1)}, u32[]{:S(2)}, u32[]{:S(2)}) collective-permute-start(bf16[256,512]{1,0:T(8,128)(2,1)S(1)} %collective-permute-done.14.refs_16_), channel_id=1, source_target_pairs={{1,3},{3,1},{5,7},{7,5},{9,11},{11,9},{13,15},{15,13},{17,19},{19,... | collective-permute-start | bytes 786440 | tf_op jit(solution)/shard_map/ppermute | solution.py:489
  56.6 14.4 %collective-permute-start.5 = (bf16[72,2048]{1,0:T(8,128)(2,1)S(1)}, bf16[72,2048]{1,0:T(8,128)(2,1)S(1)}, u32[]{:S(2)}, u32[]{:S(2)}) collective-permute-start(bf16[72,2048]{1,0:T(8,128)(2,1)S(1)} %collective-permute-done.4.refs_6_), channel_id=1, source_target_pairs={{0,1},{1,0},{2,3},{3,2},{4,5},{5,4},{6,7},{7,6},{8,9},{9,8},{10,11... | collective-permute-start | bytes 884744 | tf_op jit(solution)/shard_map/ppermute | solution.py:53
  60.7 10.8 %collective-permute-start.3 = (bf16[72,2048]{1,0:T(8,128)(2,1)S(1)}, bf16[72,2048]{1,0:T(8,128)(2,1)S(1)}, u32[]{:S(2)}, u32[]{:S(2)}) collective-permute-start(bf16[72,2048]{1,0:T(8,128)(2,1)S(1)} %collective-permute-done.2.refs_4_), channel_id=1, source_target_pairs={{0,1},{1,0},{2,3},{3,2},{4,5},{5,4},{6,7},{7,6},{8,9},{9,8},{10,11... | collective-permute-start | bytes 884744 | tf_op jit(solution)/shard_map/ppermute | solution.py:53
  60.7 8.7 %collective-permute-start.9 = (bf16[256,512]{1,0:T(8,128)(2,1)S(1)}, bf16[256,512]{1,0:T(8,128)(2,1)S(1)}, u32[]{:S(2)}, u32[]{:S(2)}) collective-permute-start(bf16[256,512]{1,0:T(8,128)(2,1)S(1)} %collective-permute-done.8.refs_10_), channel_id=1, source_target_pairs={{0,2},{1,3},{2,0},{3,1},{4,6},{5,7},{6,4},{7,5},{8,10},{9,11},{10,... | collective-permute-start | bytes 786440 | tf_op jit(solution)/shard_map/ppermute | solution.py:489
  62.3 13.9 %collective-permute-start.7 = (bf16[72,2048]{1,0:T(8,128)(2,1)S(1)}, bf16[72,2048]{1,0:T(8,128)(2,1)S(1)}, u32[]{:S(2)}, u32[]{:S(2)}) collective-permute-start(bf16[72,2048]{1,0:T(8,128)(2,1)S(1)} %collective-permute-done.6.refs_8_), channel_id=1, source_target_pairs={{0,1},{1,0},{2,3},{3,2},{4,5},{5,4},{6,7},{7,6},{8,9},{9,8},{10,11... | collective-permute-start | bytes 884744 | tf_op jit(solution)/shard_map/ppermute | solution.py:53
  69.4 18.4 %collective-permute-start.19 = (bf16[256,256]{1,0:T(8,128)(2,1)S(1)}, bf16[256,256]{1,0:T(8,128)(2,1)}, u32[]{:S(2)}, u32[]{:S(2)}) collective-permute-start(bf16[256,256]{1,0:T(8,128)(2,1)S(1)} %collective-permute-done.18.refs_6_), channel_id=1, source_target_pairs={{0,2},{1,3},{2,0},{3,1},{4,6},{5,7},{6,4},{7,5},{8,10},{9,11},{10,... | collective-permute-start | bytes 393224 | tf_op jit(solution)/shard_map/ppermute | solution.py:489
  70.9 17.0 %collective-permute-start.21 = (bf16[256,256]{1,0:T(8,128)(2,1)}, bf16[256,256]{1,0:T(8,128)(2,1)}, u32[]{:S(2)}, u32[]{:S(2)}) collective-permute-start(bf16[256,256]{1,0:T(8,128)(2,1)} %copy-done.15), channel_id=1, source_target_pairs={{0,2},{1,3},{2,0},{3,1},{4,6},{5,7},{6,4},{7,5},{8,10},{9,11},{10,... | collective-permute-start | bytes 393224 | tf_op jit(solution)/shard_map/ppermute | solution.py:489
  71.5 16.4 %collective-permute-start.23 = (bf16[256,256]{1,0:T(8,128)(2,1)}, bf16[256,256]{1,0:T(8,128)(2,1)}, u32[]{:S(2)}, u32[]{:S(2)}) collective-permute-start(bf16[256,256]{1,0:T(8,128)(2,1)} %collective-permute-done.22.refs_10_), channel_id=1, source_target_pairs={{0,2},{2,0},{4,6},{6,4},{8,10},{10,8},{12,14},{14,12},{16,18},{18,... | collective-permute-start | bytes 393224 | tf_op jit(solution)/shard_map/ppermute | solution.py:489
  74.9 13.0 %collective-permute-start.25 = (bf16[256,256]{1,0:T(8,128)(2,1)}, bf16[256,256]{1,0:T(8,128)(2,1)}, u32[]{:S(2)}, u32[]{:S(2)}) collective-permute-start(bf16[256,256]{1,0:T(8,128)(2,1)} %collective-permute-done.24.refs_12_), channel_id=1, source_target_pairs={{1,3},{3,1},{5,7},{7,5},{9,11},{11,9},{13,15},{15,13},{17,19},{19,... | collective-permute-start | bytes 393224 | tf_op jit(solution)/shard_map/ppermute | solution.py:489
  83.5 6.6 %collective-permute-start.17 = (bf16[288,128]{1,0:T(8,128)(2,1)}, bf16[288,128]{1,0:T(8,128)(2,1)S(1)}, u32[]{:S(2)}, u32[]{:S(2)}) collective-permute-start(bf16[288,128]{1,0:T(8,128)(2,1)} %get-tuple-element.30), channel_id=1, source_target_pairs={{0,16},{8,24},{1,17},{9,25},{2,18},{10,26},{3,19},{11,27},{4,20},{... | collective-permute-start | bytes 221192 | tf_op jit(solution)/shard_map/ppermute | solution.py:529
  96.1 2.9 %collective-permute-start.26 = (bf16[2,2,64,2048]{3,2,1,0:T(8,128)(2,1)}, bf16[2,2,64,2048]{3,2,1,0:T(8,128)(2,1)S(1)}, u32[]{:S(2)}, u32[]{:S(2)}) collective-permute-start(bf16[2,2,64,2048]{3,2,1,0:T(8,128)(2,1)} %get-tuple-element.34), channel_id=1, source_target_pairs={{0,1},{1,0},{2,3},{3,2},{4,5},{5,4},{6,7},{7,6},{8,9},{9,8},{10,11... | collective-permute-start | bytes 3145736 | tf_op jit(solution)/shard_map/ppermute | solution.py:53
  99.2 8.4 %collective-permute-start.27 = (bf16[2,64,1024]{2,1,0:T(8,128)(2,1)S(1)}, bf16[2,64,1024]{2,1,0:T(8,128)(2,1)S(1)}, u32[]{:S(2)}, u32[]{:S(2)}) collective-permute-start(bf16[2,64,1024]{2,1,0:T(8,128)(2,1)S(1)} %fusion), channel_id=1, source_target_pairs={{0,4},{2,6},{4,0},{6,2},{1,5},{3,7},{5,1},{7,3},{8,12},{10,14},{12... | collective-permute-start | bytes 786440 | tf_op jit(solution)/shard_map/ppermute | solution.py:53
  100.6 9.4 %collective-permute-start.29 = (bf16[2,64,1024]{2,1,0:T(8,128)(2,1)S(1)}, bf16[2,64,1024]{2,1,0:T(8,128)(2,1)S(1)}, u32[]{:S(2)}, u32[]{:S(2)}) collective-permute-start(bf16[2,64,1024]{2,1,0:T(8,128)(2,1)S(1)} %fusion.1), channel_id=1, source_target_pairs={{0,8},{8,0},{16,24},{24,16},{1,9},{9,1},{17,25},{25,17},{2,10},{10... | collective-permute-start | bytes 786440 | tf_op jit(solution)/shard_map/ppermute | solution.py:53
  107.8 5.2 %collective-permute-start.28 = (bf16[64,1024]{1,0:T(8,128)(2,1)S(1)}, bf16[64,1024]{1,0:T(8,128)(2,1)S(1)}, u32[]{:S(2)}, u32[]{:S(2)}) collective-permute-start(bf16[64,1024]{1,0:T(8,128)(2,1)S(1)} %fusion.4), channel_id=1, source_target_pairs={{0,8},{8,0},{16,24},{24,16},{1,9},{9,1},{17,25},{25,17},{2,10},{10... | collective-permute-start | bytes 393224 | tf_op jit(solution)/shard_map/ppermute | solution.py:53
  110.1 5.0 %collective-permute-start.30 = (bf16[64,1024]{1,0:T(8,128)(2,1)S(1)}, bf16[64,1024]{1,0:T(8,128)(2,1)S(1)}, u32[]{:S(2)}, u32[]{:S(2)}) collective-permute-start(bf16[64,1024]{1,0:T(8,128)(2,1)S(1)} %fusion.5), channel_id=1, source_target_pairs={{0,4},{2,6},{4,0},{6,2},{1,5},{3,7},{5,1},{7,3},{8,12},{10,14},{12... | collective-permute-start | bytes 393224 | tf_op jit(solution)/shard_map/ppermute | solution.py:53
  (20 other events, 303.4 us)

commit v4 on v3

--- a/solution.py
+++ b/solution.py
@@ -74,11 +74,13 @@
         and decay_spike.shape[1] == cores * tokens.shape[1] == width
         and query_weight.shape[0] == heads * width
         and out_weight.shape[1] == heads * width
+        and pooling_group_maps.shape[1] == 2 * width
         and 2 ** (2 * pooling_group_maps.shape[0]) <= HALO
     )
 
 
 HALO = 16
+MEBI = 2**20
 
 
 def places():
@@ -89,9 +91,16 @@
 
 
 def first_kernel(width, rows_each, *refs):
-    tokens, gain, spikes = refs[:3]
-    inputs, messages, rows_out, sems = refs[3:7], refs[7:9], refs[9], refs[10]
+    sources, inputs, messages, rows_out = refs[:3], refs[3:7], refs[7:9], refs[9]
+    locals_in, sems = refs[10:13], refs[13]
+    tokens, gain, spikes = locals_in
     _, _, half, row, side, core = places()
+    loads = [
+        pltpu.make_async_copy(source, target, sems.at[8 + n])
+        for n, (source, target) in enumerate(zip(sources, locals_in))
+    ]
+    for copy in loads:
+        copy.start()
     part = inputs[0].shape[0] // 2
     top = pl.multiple_of(side * part, part)
     first = jnp.where(core == half, 0, 1)
@@ -109,6 +118,8 @@
             )
     for copy in copies:
         copy.start()
+    for copy in loads:
+        copy.wait()
     values = tokens[...].astype(jnp.float32)
     rows_out[pl.ds(0, rows_each), :] = rms_scale(values, gain[...]).astype(jnp.bfloat16)
     rows_out[pl.ds(rows_each, 8), :] = jnp.zeros((8, rows_out.shape[1]), jnp.bfloat16)
@@ -120,56 +131,64 @@
 
 
 def pack_kernel(width, *refs):
-    maps, scale, bound, head_gain = refs[:4]
-    inputs, outputs = refs[4:8], refs[8:10]
-    out_messages, block, own, own_vectors, partner_vectors, pooling_rows, sems = (
-        refs[10:12],
-        *refs[12:],
-    )
-    _, _, half, row, side, core = places()
-    part = inputs[0].shape[0] // 2
-    rows = 2 * part
-    ends = ((2 * row + 1 - core, block), (2 * row + core, own))
+    sources = refs[:3]
+    inputs, maps, pool_weight, rec_weight = refs[3:7], refs[7], refs[8], refs[9]
+    messages, blocks, own_vectors, partner_vectors, pooled = refs[10:12], refs[12:14], *refs[14:17]
+    group_map, group_rows, scale, bound, head_gain, sems = refs[17:]
+    _, _, half, row, _, core = places()
+    rows = inputs[0].shape[0]
+    size = maps.shape[1]
+    begin = pl.multiple_of(row * size, size)
+    first = jnp.where(core == half, 0, 1)
+    group_copies = [
+        pltpu.make_async_copy(maps.at[row], group_map, sems.at[0]),
+        pltpu.make_async_copy(pool_weight.at[pl.ds(begin, size), :], group_rows, sems.at[1]),
+    ]
+    group_copies += [
+        pltpu.make_async_copy(source, target, sems.at[14 + n])
+        for n, (source, target) in enumerate(zip(sources, (scale, bound, head_gain)))
+    ]
     copies = []
-    for n, (place, target) in enumerate(ends):
-        column = pl.multiple_of(place * width, width)
-        for m, w in enumerate(inputs):
-            copies.append(
-                pltpu.make_async_copy(
-                    w.at[:, pl.ds(column, width)],
-                    target.at[pl.ds(0, rows), pl.ds(m * width, width)],
-                    sems.at[n * 4 + m],
-                )
+    targets = []
+    for n, place in enumerate((1 - core, core)):
+        column = pl.multiple_of((2 * row + place) * width, width)
+        copies += [
+            pltpu.make_async_copy(
+                w.at[:, pl.ds(column, width)],
+                blocks[n].at[pl.ds(0, rows), pl.ds(m * width, width)],
+                sems.at[2 + 4 * n + m],
             )
-    for copy in copies:
+            for m, w in enumerate(inputs)
+        ]
+        targets.append((place, blocks[n].at[pl.ds(rows + width, width), :]))
+    for n in range(2):
+        place = jnp.where(n == 0, first, 1 - first)
+        targets.append((place, messages[n].at[pl.ds(width, width), :]))
+    for n, (place, target) in enumerate(targets):
+        at = pl.ds(pl.multiple_of((2 * row + place) * width, width), width)
+        copies.append(pltpu.make_async_copy(rec_weight.at[at, :], target, sems.at[10 + n]))
+    for copy in group_copies + copies:
         copy.start()
+    for copy in group_copies:
+        copy.wait()
     for place, target in ((2 * row + core, own_vectors), (2 * row + 1 - core, partner_vectors)):
-        column = pl.ds(pl.multiple_of(place * width, width), width)
+        at = pl.ds(pl.multiple_of(place * width, width), width)
         for n, vector in enumerate((bound, head_gain)):
-            target[pl.ds(n, 1), :] = vector[:, column]
-    groups, size = maps.shape[:2]
-    for g in range(groups):
-        span = pl.ds(g * size, size)
-        scaled = maps[g].astype(jnp.float32) * scale[:, span]
-        high = scaled.astype(jnp.bfloat16)
-        rest = (scaled - high.astype(jnp.float32)).astype(jnp.bfloat16)
-        pooled = outputs[0][span, :]
-        pooling_rows[span, :] = (
-            jnp.dot(high, pooled, preferred_element_type=jnp.float32)
-            + jnp.dot(rest, pooled, preferred_element_type=jnp.float32)
-        ).astype(jnp.bfloat16)
-    outputs = (pooling_rows, outputs[1])
-    top = pl.multiple_of(side * part, part)
-    first = jnp.where(core == half, 0, 1)
+            target[pl.ds(n, 1), :] = vector[:, at]
+    scaled = group_map[...].astype(jnp.float32) * scale[:, pl.ds(begin, size)]
+    high = scaled.astype(jnp.bfloat16)
+    rest = (scaled - high.astype(jnp.float32)).astype(jnp.bfloat16)
+    pooled[...] = (
+        jnp.dot(high, group_rows[...], preferred_element_type=jnp.float32)
+        + jnp.dot(rest, group_rows[...], preferred_element_type=jnp.float32)
+    ).astype(jnp.bfloat16)
+    for block, place in zip(blocks, (1 - core, core)):
+        block[pl.ds(rows, width), :] = pooled[pl.ds(pl.multiple_of(place * width, width), width), :]
     for n in range(2):
-        place = 2 * row + jnp.where(n == 0, first, 1 - first)
-        column = pl.multiple_of(place * width, width)
-        for m, w in enumerate(outputs):
-            out_messages[n][pl.ds(m * width, width), :] = w[pl.ds(column, width), pl.ds(top, part)]
-    for place, target in ends:
-        column = pl.multiple_of(place * width, width)
-        for m, w in enumerate(outputs):
-            target[pl.ds(rows + m * width, width), :] = w[pl.ds(column, width), :]
+        place = jnp.where(n == 0, first, 1 - first)
+        messages[n][pl.ds(0, width), :] = pooled[
+            pl.ds(pl.multiple_of(place * width, width), width), :
+        ]
     for copy in copies:
         copy.wait()
 
@@ -179,33 +198,27 @@
     return jnp.where(rows >= steps, pltpu.roll(values, steps, 0), 0.0)
 
 
-def piece_sources(pieces, plane, core):
+def start_pieces(pieces, blocks, sems, plane, core, owns, put):
     planes = lax.axis_size("sp")
-    near, far, third = pieces[0:2], pieces[2:4], (pieces[4:6], pieces[6:8])
-    always = [(near, lax.rem(plane + 2 - core, planes)), (far, lax.rem(plane + 1 + core, planes))]
-    last = lax.rem(plane + 3, planes)
-    return always, third, last
-
-
-def start_pieces(pieces, blocks, sems, used, plane, side, core, owns, piece_target, block_target):
-    always, third, last = piece_sources(pieces, plane, core)
+    near, far, last = (
+        lax.rem(plane + k, planes) for k in (2 - core, 1 + core, 3)
+    )
     waits = []
-
-    def copies(pair, source, slot):
+    used = 0
+
+    def copies(group, source, slot):
         return [
-            pltpu.make_async_copy(
-                pair[n], piece_target(source, side if n == 0 else 1 - side), sems.at[slot + n]
-            )
-            for n in range(2)
+            pltpu.make_async_copy(piece, put(source, n), sems.at[slot + n])
+            for n, piece in enumerate(group)
         ]
 
-    for pair, source in always:
-        group = copies(pair, source, used)
-        for copy in group:
+    for group, source in zip(pieces[:2], (near, far)):
+        made = copies(group, source, used)
+        for copy in made:
             copy.start()
-        waits += group
-        used += 2
-    choices = [copies(pair, last, used) for pair in third]
+        waits += made
+        used += len(group)
+    choices = [copies(group, last, used) for group in pieces[2:]]
     for n in range(2):
 
         @pl.when(core == n)
@@ -214,23 +227,25 @@
                 copy.start()
 
     waits += choices[0]
-    used += 2
-    own = [pltpu.make_async_copy(block_target(b)[0], block_target(b)[1], sems.at[used]) for b in blocks]
-    for n in range(2):
-
-        @pl.when(owns if n == 0 else jnp.logical_not(owns))
-        def _(n=n):
-            own[n].start()
-
-    waits.append(own[0])
-    return waits, used + 1
+    used += len(choices[0])
+    for n, group in enumerate(blocks):
+        for m, (source, target) in enumerate(group):
+            copy = pltpu.make_async_copy(source, target, sems.at[used + m])
+
+            @pl.when(owns if n == 0 else jnp.logical_not(owns))
+            def _(copy=copy):
+                copy.start()
+
+            if n == 0:
+                waits.append(copy)
+    return waits
 
 
 def state_kernel(width, rows_each, *refs):
     own_vectors, partner_vectors = refs[:2]
     tokens, pieces, blocks = refs[2:10], refs[10:18], refs[18:20]
     read_local, read_full, pool_rows, carry = refs[20:24]
-    token_all, weight_in, spikes, sems = refs[24:]
+    token_all, weight_in, spikes, token_sems, sems = refs[24:]
     plane, _, half, row, side, core = places()
     owns = core == half
     column = 2 * row + core
@@ -248,32 +263,28 @@
                     pltpu.make_async_copy(
                         piece.at[pl.ds(0, rows_each), :],
                         token_all.at[pl.ds(top, rows_each), :],
-                        sems.at[used],
+                        token_sems.at[used],
                     )
                 )
                 waits.append(
                     pltpu.make_async_copy(
                         piece.at[pl.ds(rows_each, 8), pl.ds(0, width)],
                         spikes.at[order],
-                        sems.at[used + 1],
+                        token_sems.at[used + 1],
                     )
                 )
                 used += 2
     for copy in waits:
         copy.start()
 
-    def piece_target(source, x):
+    def put(source, n):
+        x = side if n == 0 else 1 - side
         return weight_in.at[pl.ds(pl.multiple_of(source * plane_rows + x * part, part), part), :]
 
-    def block_target(block):
-        return (
-            block.at[pl.ds(0, plane_rows), :],
-            weight_in.at[pl.ds(pl.multiple_of(plane * plane_rows, plane_rows), plane_rows), :],
-        )
-
-    more, used = start_pieces(
-        pieces, blocks, sems, used, plane, side, core, owns, piece_target, block_target
-    )
+    begin = pl.ds(pl.multiple_of(plane * plane_rows, plane_rows), plane_rows)
+    ends = [[(block.at[pl.ds(0, plane_rows), :], weight_in.at[begin, :])] for block in blocks]
+    pairs = [pieces[2 * n : 2 * n + 2] for n in range(4)]
+    more = start_pieces(pairs, ends, sems, plane, core, owns, put)
     for copy in waits + more:
         copy.wait()
     lower_bound = jnp.where(owns, own_vectors[pl.ds(0, 1), :], partner_vectors[pl.ds(0, 1), :])
@@ -344,27 +355,20 @@
 
 def output_kernel(width, rows_each, *refs):
     own_vectors, partner_vectors, read_local, read_full, pool_rows, carry = refs[:6]
-    pieces, blocks = refs[6:14], refs[14:16]
-    sent, kept = refs[16:18]
-    weight_out, mixed, sems = refs[18:]
-    plane, late, half, row, side, core = places()
+    pieces, blocks = refs[6:10], refs[10:12]
+    sent, kept = refs[12:14]
+    weight_out, mixed, sems = refs[14:]
+    plane, late, half, row, _, core = places()
     owns = core == half
     plane_rows = 4 * width
-    part = plane_rows // 2
     length = 4 * rows_each
 
-    def piece_target(source, x):
-        return weight_out.at[:, pl.ds(pl.multiple_of(source * plane_rows + x * part, part), part)]
-
-    def block_target(block):
-        return (
-            block.at[pl.ds(plane_rows, 2 * width), :],
-            weight_out.at[:, pl.ds(pl.multiple_of(plane * plane_rows, plane_rows), plane_rows)],
-        )
-
-    waits, _ = start_pieces(
-        pieces, blocks, sems, 0, plane, side, core, owns, piece_target, block_target
-    )
+    def put(source, n):
+        return weight_out.at[source]
+
+    ends = [[(block.at[pl.ds(plane_rows, 2 * width), :], weight_out.at[plane])] for block in blocks]
+    singles = [[piece] for piece in pieces]
+    waits = start_pieces(singles, ends, sems, plane, core, owns, put)
     head_gain = jnp.where(owns, own_vectors[pl.ds(1, 1), :], partner_vectors[pl.ds(1, 1), :])
     group = 2 * half + row
     window = jnp.left_shift(jnp.int32(2), group)
@@ -393,9 +397,11 @@
     for target, c in ((sent, 1 - core), (kept, core)):
         for n in range(4):
             top = pl.multiple_of((n * 2 + c) * rows_each, rows_each)
-            target[n // 2, n % 2] = jnp.dot(
-                mixed[pl.ds(top, rows_each), :], weight_out[...], preferred_element_type=jnp.float32
-            ).astype(jnp.bfloat16)
+            rows = mixed[pl.ds(top, rows_each), :]
+            for p in range(weight_out.shape[0]):
+                target[n // 2, n % 2, :, pl.ds(p * plane_rows, plane_rows)] = jnp.dot(
+                    rows, weight_out[p], preferred_element_type=jnp.float32
+                ).astype(jnp.bfloat16)
 
 
 def by_halves(
@@ -420,16 +426,22 @@
     features = tokens.shape[2]
     rows_each = tokens.shape[1]
     part = query_weight.shape[0] // 2
-    hbm = pl.BlockSpec(memory_space=pl.ANY)
+    hbm = pl.BlockSpec(memory_space=pltpu.HBM)
     vmem = pl.BlockSpec(memory_space=pltpu.VMEM)
 
     def made(*shape, kind=jnp.bfloat16):
-        return jax.ShapeDtypeStruct(shape, kind)
+        return pltpu.VMEM(shape, kind)
+
+    def near(*values):
+        return [pltpu.with_memory_space_constraint(v, pltpu.VMEM) for v in values]
 
     def pack(*refs):
         pack_kernel(width, *refs)
 
-    weights_in = (pooling_input_weight, query_weight, forget_weight, value_weight)
+    def far(*values):
+        return [pltpu.with_memory_space_constraint(v, pltpu.HBM) for v in values]
+
+    weights_in = far(pooling_input_weight, query_weight, forget_weight, value_weight)
 
     def first(*refs):
         first_kernel(width, rows_each, *refs)
@@ -437,32 +449,39 @@
     *messages, own_rows = pl.pallas_call(
         first,
         out_shape=[made(part, 4 * width)] * 2 + [made(rows_each + 8, features)],
-        in_specs=[vmem] * 3 + [hbm] * 4,
+        in_specs=[hbm] * 7,
         out_specs=[vmem] * 3,
-        scratch_shapes=[pltpu.SemaphoreType.DMA((8,))],
+        scratch_shapes=[
+            pltpu.VMEM((rows_each, features), jnp.bfloat16),
+            pltpu.VMEM((1, features), jnp.float32),
+            pltpu.VMEM((heads, width), jnp.float32),
+            pltpu.SemaphoreType.DMA((11,)),
+        ],
+        compiler_params=pltpu.CompilerParams(vmem_limit_bytes=8 * MEBI),
         name="first",
-    )(tokens[0], input_norm_gain[None], decay_spike[0].T, *weights_in)
-    block = made(2 * part + 2 * width, 4 * width)
-    *out_messages, partner_block, own_local, vectors, partner_vectors = pl.pallas_call(
+    )(*far(tokens[0], input_norm_gain[None], decay_spike[0].T), *weights_in)
+    *out_messages, partner_block, own_block, vectors, partner_vectors, _ = pl.pallas_call(
         pack,
-        out_shape=[made(2 * width, part)] * 2
-        + [block] * 2
-        + [made(2, width, kind=jnp.float32)] * 2,
-        in_specs=[vmem] * 4 + [hbm] * 4 + [vmem] * 2,
-        out_specs=[vmem] * 6,
+        out_shape=[made(2 * width, 4 * width)] * 2
+        + [made(2 * part + 2 * width, 4 * width)] * 2
+        + [made(2, width, kind=jnp.float32)] * 2
+        + [made(2 * width, 4 * width)],
+        in_specs=[hbm] * 10,
+        out_specs=[vmem] * 7,
         scratch_shapes=[
-            pltpu.VMEM(pooling_output_weight.shape, jnp.bfloat16),
-            pltpu.SemaphoreType.DMA((8,)),
+            pltpu.VMEM(pooling_group_maps.shape[1:], jnp.bfloat16),
+            pltpu.VMEM((2 * width, 4 * width), jnp.bfloat16),
+        ]
+        + [pltpu.VMEM((1, heads * width), jnp.float32)] * 3
+        + [
+            pltpu.SemaphoreType.DMA((17,)),
         ],
+        compiler_params=pltpu.CompilerParams(vmem_limit_bytes=12 * MEBI),
         name="pack",
     )(
-        pooling_group_maps,
-        pooling_scale[None],
-        lower_bound_logits[None],
-        head_norm_gain[None],
+        *far(pooling_scale[None], lower_bound_logits[None], head_norm_gain[None]),
         *weights_in,
-        pooling_output_weight,
-        recurrent_output_weight,
+        *far(pooling_group_maps, pooling_output_weight, recurrent_output_weight),
     )
 
     def hops(wanted):
@@ -489,8 +508,10 @@
             pieces.append(lax.ppermute(arrived, ("fs", "tp"), across))
         return pieces
 
-    input_pieces = shared(messages)
-    output_pieces = shared(out_messages)
+    pieces = shared(messages)
+    output_pieces = []
+    for which, pairs in rounds:
+        output_pieces.append(lax.ppermute(out_messages[which], ("sp", "tp"), pairs))
     partner_local = swapped(partner_block, "tp", 1)
 
     received_vectors = swapped(partner_vectors, "tp", 1)
@@ -516,16 +537,20 @@
             made(length, width),
             carry_shape,
         ],
-        in_specs=[vmem] * 2 + [hbm] * 18,
+        in_specs=[vmem] * 20,
         out_specs=[vmem] * 4,
         scratch_shapes=[
             pltpu.VMEM((length, features), jnp.bfloat16),
             pltpu.VMEM((features, 4 * width), jnp.bfloat16),
             pltpu.VMEM((8, 8, width), jnp.bfloat16),
-            pltpu.SemaphoreType.DMA((23,)),
+            pltpu.SemaphoreType.DMA((16,)),
+            pltpu.SemaphoreType.DMA((7,)),
         ],
+        compiler_params=pltpu.CompilerParams(vmem_limit_bytes=24 * MEBI),
         name="state",
-    )(vectors, received_vectors, *token_pieces, *input_pieces, own_local, partner_local)
+    )(
+        *near(vectors, received_vectors, *token_pieces, *pieces, own_block, partner_local),
+    )
     entering_carry = lax.ppermute(carry, "sp", [(p, p + 2) for p in range(planes - 2)])
 
     def output(*refs):
@@ -535,24 +560,18 @@
     sent, kept = pl.pallas_call(
         output,
         out_shape=[half_shape] * 2,
-        in_specs=[vmem] * 6 + [hbm] * 10,
+        in_specs=[vmem] * 12,
         out_specs=[vmem] * 2,
         scratch_shapes=[
-            pltpu.VMEM((2 * width, features), jnp.bfloat16),
+            pltpu.VMEM((planes, 2 * width, 4 * width), jnp.bfloat16),
             pltpu.VMEM((length, 2 * width), jnp.bfloat16),
-            pltpu.SemaphoreType.DMA((7,)),
+            pltpu.SemaphoreType.DMA((4,)),
         ],
+        compiler_params=pltpu.CompilerParams(vmem_limit_bytes=20 * MEBI),
         name="output",
     )(
-        vectors,
-        received_vectors,
-        read_local,
-        read_full,
-        pool_rows,
-        entering_carry,
-        *output_pieces,
-        own_local,
-        partner_local,
+        *near(vectors, received_vectors, read_local, read_full, pool_rows, entering_carry),
+        *near(*output_pieces, own_block, partner_local),
     )
     from_partner = swapped(sent, "tp", 1)
     middle = features // 2

time: 116 us -> 99.8 us (0.86)
  Pallas kernels: 19.2 us -> 9.27 us
  waiting for transfers between devices: 50.3 us -> 45.3 us
  local copies, waits for them, and re-layouts: 2.74 us -> 1.43 us
    ppermute x8 -> x4, waiting for transfers between devices: 21.2 us -> 8.6 us  [shared(): arrived = lax.ppermute(pair[which], ('sp', 'tp'), pairs)]
    ppermute x0 -> x4, waiting for transfers between devices: none -> 10.3 us  [by_halves(): output_pieces.append(lax.ppermute(out_messages[which], ('sp', 'tp'), pairs))]
    ppermute x14, starting transfers between devices: 13 us -> 21.6 us  [swapped(): lax.ppermute(value, axis, [(source, source ^ bits) for source in range(co...]
    ppermute x8 -> x4, starting transfers between devices: 12.9 us -> 6.09 us  [shared(): pieces.append(lax.ppermute(arrived, ('fs', 'tp'), across))]
    pallas_call x2, Pallas kernels: 9.53 us -> 4.58 us  [the longest x1 2.44 us: by_halves(): pl.pallas_call(pack, out_shape=[made(2 * width, 4 * width)] * 2 + [made(2...]
    ppermute x8 -> x4, starting transfers between devices: 11.9 us -> 7.72 us  [shared(): arrived = lax.ppermute(pair[which], ('sp', 'tp'), pairs)]
    pallas_call x1, Pallas kernels: 6.59 us -> 3.44 us  [by_halves(): pl.pallas_call(state, out_shape=[made(length, width, kind=jnp.float32), m...]
    ppermute x1, waiting for transfers between devices: 2.23 us -> 0.01 us  [by_halves(): lax.ppermute(carry, 'sp', [(p, p + 2) for p in range(planes - 2)])]
  transfers between devices with their start and end apart: 31 -> 27, of which waited for: 11 -> 10; matrix products, arithmetic and copies ran while one was open for 1% -> 0% of each run, Pallas kernels for 8% -> 6%
where the time goes in v4:
time: 99.8 us; the launch traced here: 99.5 us
  waiting for transfers between devices  45.3 us (45%)
  starting transfers between devices  42.2 us (42%)
  Pallas kernels  9.27 us (9%)
  local copies, waits for them, and re-layouts  1.43 us (1%)
  other arithmetic  1.12 us (1%)
    ppermute x14, starting transfers between devices, swapped(): lax.ppermute(value, axis, [(source, source ^ bits) for source in range(co...  21.6 us
    ppermute x4, waiting for transfers between devices, shared(): pieces.append(lax.ppermute(arrived, ('fs', 'tp'), across))  14.6 us
    ppermute x14, waiting for transfers between devices, swapped(): lax.ppermute(value, axis, [(source, source ^ bits) for source in range(co...  11.8 us
    ppermute x4, waiting for transfers between devices, by_halves(): output_pieces.append(lax.ppermute(out_messages[which], ('sp', 'tp'), pairs))  10.3 us
    ppermute x4, waiting for transfers between devices, shared(): arrived = lax.ppermute(pair[which], ('sp', 'tp'), pairs)  8.6 us
    ppermute x4, starting transfers between devices, shared(): arrived = lax.ppermute(pair[which], ('sp', 'tp'), pairs)  7.72 us
    ppermute x4, starting transfers between devices, shared(): pieces.append(lax.ppermute(arrived, ('fs', 'tp'), across))  6.09 us
    ppermute x1, starting transfers between devices, by_halves(): lax.ppermute(carry, 'sp', [(p, p + 2) for p in range(planes - 2)])  4.72 us
  transfers between devices with their start and end apart: 27, of which 10 were waited for; matrix products, arithmetic and copies ran while one was open for 0% of the time, Pallas kernels for 6%

profile of v4, /device:TPU:0, one launch (start us, length us, event | category | flops | bytes accessed | tf_op | source)
XLA Modules:
  0.0 99.5 jit_solution(8904052825574066853)
XLA Ops:
  0.0 1.2 %first.1 = (bf16[256,512]{1,0:T(8,128)(2,1)S(1)}, bf16[256,512]{1,0:T(8,128)(2,1)S(1)}, bf16[72,2048]{1,0:T(8,128)(2,1)S(1)}) custom-call(bf16[64,2048]{1,0:T(8,128)(2,1)} %bitcast.36, f32[1,2048]{1,0:T(1,128)} %bitcast.37, f32[4,128]{1,0:T(4,128)} %bitcast.41, bf16[512,512]{1,0:T(8,128)(2,1)} %refs_3_.3, bf16[512,512]{1,0:T(8,128)(2,1)} %refs_4_.3, ...), custom_call_target="tpu_custom_call" | custom-call | tf_op jit(solution)/shard_map/first/pallas_call | solution.py:449
  1.3 3.6 %collective-permute-start.10 = (bf16[256,512]{1,0:T(8,128)(2,1)S(1)}, bf16[256,512]{1,0:T(8,128)(2,1)S(1)}, u32[]{:S(2)}, u32[]{:S(2)}) collective-permute-start(bf16[256,512]{1,0:T(8,128)(2,1)S(1)} %get-tuple-element.24), channel_id=1, source_target_pairs={{16,1},{8,0},{25,9},{17,8},{0,17},{24,16},{9,25},{1,24},{18,3},{10... | collective-permute-start | bytes 786440 | tf_op jit(solution)/shard_map/ppermute | solution.py:504
  4.8 1.3 %collective-permute-start.12 = (bf16[256,512]{1,0:T(8,128)(2,1)S(1)}, bf16[256,512]{1,0:T(8,128)(2,1)S(1)}, u32[]{:S(2)}, u32[]{:S(2)}) collective-permute-start(bf16[256,512]{1,0:T(8,128)(2,1)S(1)} %get-tuple-element.24), channel_id=1, source_target_pairs={{24,0},{1,8},{8,16},{17,24},{26,2},{3,10},{10,18},{19,26},{28,4},{... | collective-permute-start | bytes 786440 | tf_op jit(solution)/shard_map/ppermute | solution.py:504
  6.8 4.8 %collective-permute-start.4 = (bf16[72,2048]{1,0:T(8,128)(2,1)S(1)}, bf16[72,2048]{1,0:T(8,128)(2,1)S(1)}, u32[]{:S(2)}, u32[]{:S(2)}) collective-permute-start(bf16[72,2048]{1,0:T(8,128)(2,1)S(1)} %get-tuple-element.22.refs_2_), channel_id=1, source_target_pairs={{0,8},{8,0},{16,24},{24,16},{1,9},{9,1},{17,25},{25,17},{2,10},{10... | collective-permute-start | bytes 884744 | tf_op jit(solution)/shard_map/ppermute | solution.py:53
  11.6 2.4 %pack.1 = (bf16[256,512]{1,0:T(8,128)(2,1)S(1)}, bf16[256,512]{1,0:T(8,128)(2,1)S(1)}, bf16[768,512]{1,0:T(8,128)(2,1)S(1)}, bf16[768,512]{1,0:T(8,128)(2,1)S(1)...) custom-call(f32[1,512]{1,0:T(1,128)} %bitcast.38, f32[1,512]{1,0:T(1,128)} %bitcast.39, ...), custom_call_target="tpu_custom_call" | custom-call | tf_op jit(solution)/shard_map/pack/pallas_call | solution.py:463
  14.1 1.1 %collective-permute-done.refs_1_ = f32[2,128]{1,0:T(2,128)S(1)} collective-permute-done((f32[2,128]{1,0:T(2,128)S(1)}, f32[2,128]{1,0:T(2,128)S(1)}, u32[]{:S(2)}, u32[]{:S(2)}) %collective-permute-start) | collective-permute-done | bytes 1056 | tf_op jit(solution)/shard_map/ppermute | solution.py:53
  15.3 1.5 %collective-permute-start.2 = (bf16[72,2048]{1,0:T(8,128)(2,1)S(1)}, bf16[72,2048]{1,0:T(8,128)(2,1)S(1)}, u32[]{:S(2)}, u32[]{:S(2)}) collective-permute-start(bf16[72,2048]{1,0:T(8,128)(2,1)S(1)} %get-tuple-element.22.refs_2_), channel_id=1, source_target_pairs={{0,4},{2,6},{4,0},{6,2},{1,5},{3,7},{5,1},{7,3},{8,12},{10,14},{12... | collective-permute-start | bytes 884744 | tf_op jit(solution)/shard_map/ppermute | solution.py:53
  16.8 2.2 %collective-permute-start.8 = (bf16[256,512]{1,0:T(8,128)(2,1)S(1)}, bf16[256,512]{1,0:T(8,128)(2,1)S(1)}, u32[]{:S(2)}, u32[]{:S(2)}) collective-permute-start(bf16[256,512]{1,0:T(8,128)(2,1)S(1)} %get-tuple-element.23), channel_id=1, source_target_pairs={{16,0},{8,1},{25,8},{17,9},{0,16},{24,17},{9,24},{1,25},{18,2},{10... | collective-permute-start | bytes 786440 | tf_op jit(solution)/shard_map/ppermute | solution.py:504
  20.0 1.4 %collective-permute-start.1 = (bf16[72,2048]{1,0:T(8,128)(2,1)S(1)}, bf16[72,2048]{1,0:T(8,128)(2,1)S(1)}, u32[]{:S(2)}, u32[]{:S(2)}) collective-permute-start(bf16[72,2048]{1,0:T(8,128)(2,1)S(1)} %get-tuple-element.22.refs_2_), channel_id=1, source_target_pairs={{0,1},{1,0},{2,3},{3,2},{4,5},{5,4},{6,7},{7,6},{8,9},{9,8},{10,11... | collective-permute-start | bytes 884744 | tf_op jit(solution)/shard_map/ppermute | solution.py:53
  21.4 8.6 %collective-permute-done.8.refs_10_ = bf16[256,512]{1,0:T(8,128)(2,1)S(1)} collective-permute-done((bf16[256,512]{1,0:T(8,128)(2,1)S(1)}, bf16[256,512]{1,0:T(8,128)(2,1)S(1)}, u32[]{:S(2)}, u32[]{:S(2)}) %collective-permute-start.8) | collective-permute-done | bytes 262176 | tf_op jit(solution)/shard_map/ppermute | solution.py:504
  30.0 1.5 %collective-permute-start.11 = (bf16[256,512]{1,0:T(8,128)(2,1)S(1)}, bf16[256,512]{1,0:T(8,128)(2,1)S(1)}, u32[]{:S(2)}, u32[]{:S(2)}) collective-permute-start(bf16[256,512]{1,0:T(8,128)(2,1)S(1)} %collective-permute-done.10.refs_12_), channel_id=1, source_target_pairs={{0,2},{1,3},{2,0},{3,1},{4,6},{5,7},{6,4},{7,5},{8,10},{9,11},{10,... | collective-permute-start | bytes 786440 | tf_op jit(solution)/shard_map/ppermute | solution.py:508
  31.5 2.4 %collective-permute-start.13 = (bf16[256,512]{1,0:T(8,128)(2,1)S(1)}, bf16[256,512]{1,0:T(8,128)(2,1)S(1)}, u32[]{:S(2)}, u32[]{:S(2)}) collective-permute-start(bf16[256,512]{1,0:T(8,128)(2,1)S(1)} %collective-permute-done.12.refs_14_), channel_id=1, source_target_pairs={{0,2},{2,0},{4,6},{6,4},{8,10},{10,8},{12,14},{14,12},{16,18},{18,... | collective-permute-start | bytes 786440 | tf_op jit(solution)/shard_map/ppermute | solution.py:508
  34.6 1.6 %collective-permute-start.6 = (bf16[72,2048]{1,0:T(8,128)(2,1)S(1)}, bf16[72,2048]{1,0:T(8,128)(2,1)S(1)}, u32[]{:S(2)}, u32[]{:S(2)}) collective-permute-start(bf16[72,2048]{1,0:T(8,128)(2,1)S(1)} %collective-permute-done.4.refs_6_), channel_id=1, source_target_pairs={{0,4},{2,6},{4,0},{6,2},{1,5},{3,7},{5,1},{7,3},{8,12},{10,14},{12... | collective-permute-start | bytes 884744 | tf_op jit(solution)/shard_map/ppermute | solution.py:53
  36.2 2.7 %collective-permute-done.11.refs_13_ = bf16[256,512]{1,0:T(8,128)(2,1)S(1)} collective-permute-done((bf16[256,512]{1,0:T(8,128)(2,1)S(1)}, bf16[256,512]{1,0:T(8,128)(2,1)S(1)}, u32[]{:S(2)}, u32[]{:S(2)}) %collective-permute-start.11) | collective-permute-done | bytes 262176 | tf_op jit(solution)/shard_map/ppermute | solution.py:508
  39.6 4.9 %collective-permute-done.13.refs_15_ = bf16[256,512]{1,0:T(8,128)(2,1)S(1)} collective-permute-done((bf16[256,512]{1,0:T(8,128)(2,1)S(1)}, bf16[256,512]{1,0:T(8,128)(2,1)S(1)}, u32[]{:S(2)}, u32[]{:S(2)}) %collective-permute-start.13) | collective-permute-done | bytes 262176 | tf_op jit(solution)/shard_map/ppermute | solution.py:508
  44.5 1.5 %collective-permute-start.9 = (bf16[256,512]{1,0:T(8,128)(2,1)S(1)}, bf16[256,512]{1,0:T(8,128)(2,1)S(1)}, u32[]{:S(2)}, u32[]{:S(2)}) collective-permute-start(bf16[256,512]{1,0:T(8,128)(2,1)S(1)} %collective-permute-done.8.refs_10_), channel_id=1, source_target_pairs={{0,2},{1,3},{2,0},{3,1},{4,6},{5,7},{6,4},{7,5},{8,10},{9,11},{10,... | collective-permute-start | bytes 786440 | tf_op jit(solution)/shard_map/ppermute | solution.py:508
  46.2 7.0 %collective-permute-done.9.refs_11_ = bf16[256,512]{1,0:T(8,128)(2,1)S(1)} collective-permute-done((bf16[256,512]{1,0:T(8,128)(2,1)S(1)}, bf16[256,512]{1,0:T(8,128)(2,1)S(1)}, u32[]{:S(2)}, u32[]{:S(2)}) %collective-permute-start.9) | collective-permute-done | bytes 262176 | tf_op jit(solution)/shard_map/ppermute | solution.py:508
  53.4 1.3 %collective-permute-start.20 = (bf16[256,512]{1,0:T(8,128)(2,1)S(1)}, bf16[256,512]{1,0:T(8,128)(2,1)S(1)}, u32[]{:S(2)}, u32[]{:S(2)}) collective-permute-start(bf16[256,512]{1,0:T(8,128)(2,1)S(1)} %get-tuple-element.32), channel_id=1, source_target_pairs={{24,0},{1,8},{8,16},{17,24},{26,2},{3,10},{10,18},{19,26},{28,4},{... | collective-permute-start | bytes 786440 | tf_op jit(solution)/shard_map/ppermute | solution.py:514
  55.4 3.4 %state.1 = (f32[512,128]{1,0:T(8,128)S(1)}, bf16[512,128]{1,0:T(8,128)(2,1)S(1)}, bf16[512,128]{1,0:T(8,128)(2,1)S(1)}, bf16[288,128]{1,0:T(8,128)(2,1)S(1)}) custom-call(f32[2,128]{1,0:T(2,128)S(1)} %get-tuple-element.20.refs_0_, f32[2,128]{1,0:T(2,128)S(1)} %collective-permute-done.refs_1_, bf16[72,2048]{1,0:T(8,128)(2,1)S(1)} %get-tuple-element.22.refs_2_, ...), custom_call_target="tpu_custom_call" | custom-call | tf_op jit(solution)/shard_map/state/pallas_call | solution.py:532
  58.8 4.7 %collective-permute-start.17 = (bf16[288,128]{1,0:T(8,128)(2,1)S(1)}, bf16[288,128]{1,0:T(8,128)(2,1)S(1)}, u32[]{:S(2)}, u32[]{:S(2)}) collective-permute-start(bf16[288,128]{1,0:T(8,128)(2,1)S(1)} %get-tuple-element.30), channel_id=1, source_target_pairs={{0,16},{8,24},{1,17},{9,25},{2,18},{10,26},{3,19},{11,27},{4,20},{... | collective-permute-start | bytes 221192 | tf_op jit(solution)/shard_map/ppermute | solution.py:554
  63.5 10.3 %collective-permute-done.18.refs_6_ = bf16[256,512]{1,0:T(8,128)(2,1)S(1)} collective-permute-done((bf16[256,512]{1,0:T(8,128)(2,1)S(1)}, bf16[256,512]{1,0:T(8,128)(2,1)S(1)}, u32[]{:S(2)}, u32[]{:S(2)}) %collective-permute-start.18) | collective-permute-done | bytes 262176 | tf_op jit(solution)/shard_map/ppermute | solution.py:514
  73.8 2.1 %output.1 = (bf16[2,2,64,2048]{3,2,1,0:T(8,128)(2,1)S(1)}, bf16[2,2,64,2048]{3,2,1,0:T(8,128)(2,1)S(1)}) custom-call(f32[2,128]{1,0:T(2,128)S(1)} %get-tuple-element.20.refs_0_, f32[2,128]{1,0:T(2,128)S(1)} %collective-permute-done.refs_1_, f32[512,128]{1,0:T(8,128)S(1)} %get-tuple-element.27.refs_2_, bf16[512,128]{1,0:T(8,128)(2,1)S(1)} %get-tuple-element.28.refs_3_, ...), custom_call_target="tpu_custom_call" | custom-call | tf_op jit(solution)/shard_map/output/pallas_call | solution.py:560
  76.0 3.1 %collective-permute-start.22 = (bf16[2,2,64,2048]{3,2,1,0:T(8,128)(2,1)S(1)}, bf16[2,2,64,2048]{3,2,1,0:T(8,128)(2,1)}, u32[]{:S(2)}, u32[]{:S(2)}) collective-permute-start(bf16[2,2,64,2048]{3,2,1,0:T(8,128)(2,1)S(1)} %get-tuple-element.34), channel_id=1, source_target_pairs={{0,1},{1,0},{2,3},{3,2},{4,5},{5,4},{6,7},{7,6},{8,9},{9,8},{10,11... | collective-permute-start | bytes 3145736 | tf_op jit(solution)/shard_map/ppermute | solution.py:53
  79.2 2.3 %collective-permute-done.22 = bf16[2,2,64,2048]{3,2,1,0:T(8,128)(2,1)} collective-permute-done((bf16[2,2,64,2048]{3,2,1,0:T(8,128)(2,1)S(1)}, bf16[2,2,64,2048]{3,2,1,0:T(8,128)(2,1)}, u32[]{:S(2)}, u32[]{:S(2)}) %collective-permute-start.22) | collective-permute-done | bytes 1048608 | tf_op jit(solution)/shard_map/ppermute | solution.py:53
  81.5 1.3 %fusion.9 = (bf16[2,2,64,1024]{3,2,1,0:T(8,128)(2,1)S(1)}, bf16[2,2,64,1024]{3,2,1,0:T(8,128)(2,1)S(1)}) fusion(bf16[2,2,64,2048]{3,2,1,0:T(8,128)(2,1)} %collective-permute-done.22), kind=kLoop, calls=%fused_computation.18 | loop fusion | bytes 2097152 | tf_op jit(solution)/shard_map/slice | solution.py:581
  82.9 1.6 %collective-permute-start.23 = (bf16[2,64,1024]{2,1,0:T(8,128)(2,1)S(1)}, bf16[2,64,1024]{2,1,0:T(8,128)(2,1)S(1)}, u32[]{:S(2)}, u32[]{:S(2)}) collective-permute-start(bf16[2,64,1024]{2,1,0:T(8,128)(2,1)S(1)} %fusion), channel_id=1, source_target_pairs={{0,4},{2,6},{4,0},{6,2},{1,5},{3,7},{5,1},{7,3},{8,12},{10,14},{12... | collective-permute-start | bytes 786440 | tf_op jit(solution)/shard_map/ppermute | solution.py:53
  84.6 2.1 %collective-permute-start.25 = (bf16[2,64,1024]{2,1,0:T(8,128)(2,1)S(1)}, bf16[2,64,1024]{2,1,0:T(8,128)(2,1)S(1)}, u32[]{:S(2)}, u32[]{:S(2)}) collective-permute-start(bf16[2,64,1024]{2,1,0:T(8,128)(2,1)S(1)} %fusion.1), channel_id=1, source_target_pairs={{0,8},{8,0},{16,24},{24,16},{1,9},{9,1},{17,25},{25,17},{2,10},{10... | collective-permute-start | bytes 786440 | tf_op jit(solution)/shard_map/ppermute | solution.py:53
  86.7 4.9 %collective-permute-done.23 = bf16[2,64,1024]{2,1,0:T(8,128)(2,1)S(1)} collective-permute-done((bf16[2,64,1024]{2,1,0:T(8,128)(2,1)S(1)}, bf16[2,64,1024]{2,1,0:T(8,128)(2,1)S(1)}, u32[]{:S(2)}, u32[]{:S(2)}) %collective-permute-start.23) | collective-permute-done | bytes 262176 | tf_op jit(solution)/shard_map/ppermute | solution.py:53
  91.7 1.9 %collective-permute-start.24 = (bf16[64,1024]{1,0:T(8,128)(2,1)S(1)}, bf16[64,1024]{1,0:T(8,128)(2,1)S(1)}, u32[]{:S(2)}, u32[]{:S(2)}) collective-permute-start(bf16[64,1024]{1,0:T(8,128)(2,1)S(1)} %fusion.4), channel_id=1, source_target_pairs={{0,8},{8,0},{16,24},{24,16},{1,9},{9,1},{17,25},{25,17},{2,10},{10... | collective-permute-start | bytes 393224 | tf_op jit(solution)/shard_map/ppermute | solution.py:53
  93.7 1.6 %collective-permute-start.26 = (bf16[64,1024]{1,0:T(8,128)(2,1)S(1)}, bf16[64,1024]{1,0:T(8,128)(2,1)S(1)}, u32[]{:S(2)}, u32[]{:S(2)}) collective-permute-start(bf16[64,1024]{1,0:T(8,128)(2,1)S(1)} %fusion.5), channel_id=1, source_target_pairs={{0,4},{2,6},{4,0},{6,2},{1,5},{3,7},{5,1},{7,3},{8,12},{10,14},{12... | collective-permute-start | bytes 393224 | tf_op jit(solution)/shard_map/ppermute | solution.py:53
  95.3 1.4 %collective-permute-done.24 = bf16[64,1024]{1,0:T(8,128)(2,1)S(1)} collective-permute-done((bf16[64,1024]{1,0:T(8,128)(2,1)S(1)}, bf16[64,1024]{1,0:T(8,128)(2,1)S(1)}, u32[]{:S(2)}, u32[]{:S(2)}) %collective-permute-start.24) | collective-permute-done | bytes 131104 | tf_op jit(solution)/shard_map/ppermute | solution.py:53
  96.8 2.0 %collective-permute-done.26 = bf16[64,1024]{1,0:T(8,128)(2,1)S(1)} collective-permute-done((bf16[64,1024]{1,0:T(8,128)(2,1)S(1)}, bf16[64,1024]{1,0:T(8,128)(2,1)S(1)}, u32[]{:S(2)}, u32[]{:S(2)}) %collective-permute-start.26) | collective-permute-done | bytes 131104 | tf_op jit(solution)/shard_map/ppermute | solution.py:53
  (37 shorter events, 5.4 us)
Async XLA Ops:
  1.3 15.5 %collective-permute-start.10 = (bf16[256,512]{1,0:T(8,128)(2,1)S(1)}, bf16[256,512]{1,0:T(8,128)(2,1)S(1)}, u32[]{:S(2)}, u32[]{:S(2)}) collective-permute-start(bf16[256,512]{1,0:T(8,128)(2,1)S(1)} %get-tuple-element.24), channel_id=1, source_target_pairs={{16,1},{8,0},{25,9},{17,8},{0,17},{24,16},{9,25},{1,24},{18,3},{10... | collective-permute-start | bytes 786440 | tf_op jit(solution)/shard_map/ppermute | solution.py:504
  4.8 14.2 %collective-permute-start.12 = (bf16[256,512]{1,0:T(8,128)(2,1)S(1)}, bf16[256,512]{1,0:T(8,128)(2,1)S(1)}, u32[]{:S(2)}, u32[]{:S(2)}) collective-permute-start(bf16[256,512]{1,0:T(8,128)(2,1)S(1)} %get-tuple-element.24), channel_id=1, source_target_pairs={{24,0},{1,8},{8,16},{17,24},{26,2},{3,10},{10,18},{19,26},{28,4},{... | collective-permute-start | bytes 786440 | tf_op jit(solution)/shard_map/ppermute | solution.py:504
  6.1 13.9 %collective-permute-start.14 = (bf16[256,512]{1,0:T(8,128)(2,1)S(1)}, bf16[256,512]{1,0:T(8,128)(2,1)S(1)}, u32[]{:S(2)}, u32[]{:S(2)}) collective-permute-start(bf16[256,512]{1,0:T(8,128)(2,1)S(1)} %get-tuple-element.23), channel_id=1, source_target_pairs={{24,1},{1,9},{8,17},{17,25},{26,3},{3,11},{10,19},{19,27},{28,5},{... | collective-permute-start | bytes 786440 | tf_op jit(solution)/shard_map/ppermute | solution.py:504
  6.8 24.7 %collective-permute-start.4 = (bf16[72,2048]{1,0:T(8,128)(2,1)S(1)}, bf16[72,2048]{1,0:T(8,128)(2,1)S(1)}, u32[]{:S(2)}, u32[]{:S(2)}) collective-permute-start(bf16[72,2048]{1,0:T(8,128)(2,1)S(1)} %get-tuple-element.22.refs_2_), channel_id=1, source_target_pairs={{0,8},{8,0},{16,24},{24,16},{1,9},{9,1},{17,25},{25,17},{2,10},{10... | collective-permute-start | bytes 884744 | tf_op jit(solution)/shard_map/ppermute | solution.py:53
  14.0 1.2 %collective-permute-start = (f32[2,128]{1,0:T(2,128)S(1)}, f32[2,128]{1,0:T(2,128)S(1)}, u32[]{:S(2)}, u32[]{:S(2)}) collective-permute-start(f32[2,128]{1,0:T(2,128)S(1)} %get-tuple-element.21), channel_id=1, source_target_pairs={{0,1},{1,0},{2,3},{3,2},{4,5},{5,4},{6,7},{7,6},{8,9},{9,8},{10,11... | collective-permute-start | bytes 3080 | tf_op jit(solution)/shard_map/ppermute | solution.py:53
  15.3 18.7 %collective-permute-start.2 = (bf16[72,2048]{1,0:T(8,128)(2,1)S(1)}, bf16[72,2048]{1,0:T(8,128)(2,1)S(1)}, u32[]{:S(2)}, u32[]{:S(2)}) collective-permute-start(bf16[72,2048]{1,0:T(8,128)(2,1)S(1)} %get-tuple-element.22.refs_2_), channel_id=1, source_target_pairs={{0,4},{2,6},{4,0},{6,2},{1,5},{3,7},{5,1},{7,3},{8,12},{10,14},{12... | collective-permute-start | bytes 884744 | tf_op jit(solution)/shard_map/ppermute | solution.py:53
  16.8 13.2 %collective-permute-start.8 = (bf16[256,512]{1,0:T(8,128)(2,1)S(1)}, bf16[256,512]{1,0:T(8,128)(2,1)S(1)}, u32[]{:S(2)}, u32[]{:S(2)}) collective-permute-start(bf16[256,512]{1,0:T(8,128)(2,1)S(1)} %get-tuple-element.23), channel_id=1, source_target_pairs={{16,0},{8,1},{25,8},{17,9},{0,16},{24,17},{9,24},{1,25},{18,2},{10... | collective-permute-start | bytes 786440 | tf_op jit(solution)/shard_map/ppermute | solution.py:504
  19.0 35.7 %collective-permute-start.16 = (bf16[768,512]{1,0:T(8,128)(2,1)S(1)}, bf16[768,512]{1,0:T(8,128)(2,1)S(1)}, u32[]{:S(2)}, u32[]{:S(2)}) collective-permute-start(bf16[768,512]{1,0:T(8,128)(2,1)S(1)} %get-tuple-element.26), channel_id=1, source_target_pairs={{0,1},{1,0},{2,3},{3,2},{4,5},{5,4},{6,7},{7,6},{8,9},{9,8},{10,11... | collective-permute-start | bytes 2359304 | tf_op jit(solution)/shard_map/ppermute | solution.py:53
  20.0 14.6 %collective-permute-start.1 = (bf16[72,2048]{1,0:T(8,128)(2,1)S(1)}, bf16[72,2048]{1,0:T(8,128)(2,1)S(1)}, u32[]{:S(2)}, u32[]{:S(2)}) collective-permute-start(bf16[72,2048]{1,0:T(8,128)(2,1)S(1)} %get-tuple-element.22.refs_2_), channel_id=1, source_target_pairs={{0,1},{1,0},{2,3},{3,2},{4,5},{5,4},{6,7},{7,6},{8,9},{9,8},{10,11... | collective-permute-start | bytes 884744 | tf_op jit(solution)/shard_map/ppermute | solution.py:53
  30.0 8.9 %collective-permute-start.11 = (bf16[256,512]{1,0:T(8,128)(2,1)S(1)}, bf16[256,512]{1,0:T(8,128)(2,1)S(1)}, u32[]{:S(2)}, u32[]{:S(2)}) collective-permute-start(bf16[256,512]{1,0:T(8,128)(2,1)S(1)} %collective-permute-done.10.refs_12_), channel_id=1, source_target_pairs={{0,2},{1,3},{2,0},{3,1},{4,6},{5,7},{6,4},{7,5},{8,10},{9,11},{10,... | collective-permute-start | bytes 786440 | tf_op jit(solution)/shard_map/ppermute | solution.py:508
  31.5 13.0 %collective-permute-start.13 = (bf16[256,512]{1,0:T(8,128)(2,1)S(1)}, bf16[256,512]{1,0:T(8,128)(2,1)S(1)}, u32[]{:S(2)}, u32[]{:S(2)}) collective-permute-start(bf16[256,512]{1,0:T(8,128)(2,1)S(1)} %collective-permute-done.12.refs_14_), channel_id=1, source_target_pairs={{0,2},{2,0},{4,6},{6,4},{8,10},{10,8},{12,14},{14,12},{16,18},{18,... | collective-permute-start | bytes 786440 | tf_op jit(solution)/shard_map/ppermute | solution.py:508
  33.9 10.6 %collective-permute-start.15 = (bf16[256,512]{1,0:T(8,128)(2,1)S(1)}, bf16[256,512]{1,0:T(8,128)(2,1)S(1)}, u32[]{:S(2)}, u32[]{:S(2)}) collective-permute-start(bf16[256,512]{1,0:T(8,128)(2,1)S(1)} %collective-permute-done.14.refs_16_), channel_id=1, source_target_pairs={{1,3},{3,1},{5,7},{7,5},{9,11},{11,9},{13,15},{15,13},{17,19},{19,... | collective-permute-start | bytes 786440 | tf_op jit(solution)/shard_map/ppermute | solution.py:508
  34.6 11.4 %collective-permute-start.6 = (bf16[72,2048]{1,0:T(8,128)(2,1)S(1)}, bf16[72,2048]{1,0:T(8,128)(2,1)S(1)}, u32[]{:S(2)}, u32[]{:S(2)}) collective-permute-start(bf16[72,2048]{1,0:T(8,128)(2,1)S(1)} %collective-permute-done.4.refs_6_), channel_id=1, source_target_pairs={{0,4},{2,6},{4,0},{6,2},{1,5},{3,7},{5,1},{7,3},{8,12},{10,14},{12... | collective-permute-start | bytes 884744 | tf_op jit(solution)/shard_map/ppermute | solution.py:53
  38.9 14.3 %collective-permute-start.5 = (bf16[72,2048]{1,0:T(8,128)(2,1)S(1)}, bf16[72,2048]{1,0:T(8,128)(2,1)S(1)}, u32[]{:S(2)}, u32[]{:S(2)}) collective-permute-start(bf16[72,2048]{1,0:T(8,128)(2,1)S(1)} %collective-permute-done.4.refs_6_), channel_id=1, source_target_pairs={{0,1},{1,0},{2,3},{3,2},{4,5},{5,4},{6,7},{7,6},{8,9},{9,8},{10,11... | collective-permute-start | bytes 884744 | tf_op jit(solution)/shard_map/ppermute | solution.py:53
  44.5 8.9 %collective-permute-start.3 = (bf16[72,2048]{1,0:T(8,128)(2,1)S(1)}, bf16[72,2048]{1,0:T(8,128)(2,1)S(1)}, u32[]{:S(2)}, u32[]{:S(2)}) collective-permute-start(bf16[72,2048]{1,0:T(8,128)(2,1)S(1)} %collective-permute-done.2.refs_4_), channel_id=1, source_target_pairs={{0,1},{1,0},{2,3},{3,2},{4,5},{5,4},{6,7},{7,6},{8,9},{9,8},{10,11... | collective-permute-start | bytes 884744 | tf_op jit(solution)/shard_map/ppermute | solution.py:53
  44.5 8.7 %collective-permute-start.9 = (bf16[256,512]{1,0:T(8,128)(2,1)S(1)}, bf16[256,512]{1,0:T(8,128)(2,1)S(1)}, u32[]{:S(2)}, u32[]{:S(2)}) collective-permute-start(bf16[256,512]{1,0:T(8,128)(2,1)S(1)} %collective-permute-done.8.refs_10_), channel_id=1, source_target_pairs={{0,2},{1,3},{2,0},{3,1},{4,6},{5,7},{6,4},{7,5},{8,10},{9,11},{10,... | collective-permute-start | bytes 786440 | tf_op jit(solution)/shard_map/ppermute | solution.py:508
  46.0 9.3 %collective-permute-start.7 = (bf16[72,2048]{1,0:T(8,128)(2,1)S(1)}, bf16[72,2048]{1,0:T(8,128)(2,1)S(1)}, u32[]{:S(2)}, u32[]{:S(2)}) collective-permute-start(bf16[72,2048]{1,0:T(8,128)(2,1)S(1)} %collective-permute-done.6.refs_8_), channel_id=1, source_target_pairs={{0,1},{1,0},{2,3},{3,2},{4,5},{5,4},{6,7},{7,6},{8,9},{9,8},{10,11... | collective-permute-start | bytes 884744 | tf_op jit(solution)/shard_map/ppermute | solution.py:53
  53.2 20.6 %collective-permute-start.18 = (bf16[256,512]{1,0:T(8,128)(2,1)S(1)}, bf16[256,512]{1,0:T(8,128)(2,1)S(1)}, u32[]{:S(2)}, u32[]{:S(2)}) collective-permute-start(bf16[256,512]{1,0:T(8,128)(2,1)S(1)} %get-tuple-element.31), channel_id=1, source_target_pairs={{16,0},{8,1},{25,8},{17,9},{0,16},{24,17},{9,24},{1,25},{18,2},{10... | collective-permute-start | bytes 786440 | tf_op jit(solution)/shard_map/ppermute | solution.py:514
  53.2 20.6 %collective-permute-start.19 = (bf16[256,512]{1,0:T(8,128)(2,1)S(1)}, bf16[256,512]{1,0:T(8,128)(2,1)S(1)}, u32[]{:S(2)}, u32[]{:S(2)}) collective-permute-start(bf16[256,512]{1,0:T(8,128)(2,1)S(1)} %get-tuple-element.32), channel_id=1, source_target_pairs={{16,1},{8,0},{25,9},{17,8},{0,17},{24,16},{9,25},{1,24},{18,3},{10... | collective-permute-start | bytes 786440 | tf_op jit(solution)/shard_map/ppermute | solution.py:514
  53.4 20.5 %collective-permute-start.20 = (bf16[256,512]{1,0:T(8,128)(2,1)S(1)}, bf16[256,512]{1,0:T(8,128)(2,1)S(1)}, u32[]{:S(2)}, u32[]{:S(2)}) collective-permute-start(bf16[256,512]{1,0:T(8,128)(2,1)S(1)} %get-tuple-element.32), channel_id=1, source_target_pairs={{24,0},{1,8},{8,16},{17,24},{26,2},{3,10},{10,18},{19,26},{28,4},{... | collective-permute-start | bytes 786440 | tf_op jit(solution)/shard_map/ppermute | solution.py:514
  54.7 19.2 %collective-permute-start.21 = (bf16[256,512]{1,0:T(8,128)(2,1)S(1)}, bf16[256,512]{1,0:T(8,128)(2,1)S(1)}, u32[]{:S(2)}, u32[]{:S(2)}) collective-permute-start(bf16[256,512]{1,0:T(8,128)(2,1)S(1)} %get-tuple-element.31), channel_id=1, source_target_pairs={{24,1},{1,9},{8,17},{17,25},{26,3},{3,11},{10,19},{19,27},{28,5},{... | collective-permute-start | bytes 786440 | tf_op jit(solution)/shard_map/ppermute | solution.py:514
  58.8 15.0 %collective-permute-start.17 = (bf16[288,128]{1,0:T(8,128)(2,1)S(1)}, bf16[288,128]{1,0:T(8,128)(2,1)S(1)}, u32[]{:S(2)}, u32[]{:S(2)}) collective-permute-start(bf16[288,128]{1,0:T(8,128)(2,1)S(1)} %get-tuple-element.30), channel_id=1, source_target_pairs={{0,16},{8,24},{1,17},{9,25},{2,18},{10,26},{3,19},{11,27},{4,20},{... | collective-permute-start | bytes 221192 | tf_op jit(solution)/shard_map/ppermute | solution.py:554
  76.0 5.5 %collective-permute-start.22 = (bf16[2,2,64,2048]{3,2,1,0:T(8,128)(2,1)S(1)}, bf16[2,2,64,2048]{3,2,1,0:T(8,128)(2,1)}, u32[]{:S(2)}, u32[]{:S(2)}) collective-permute-start(bf16[2,2,64,2048]{3,2,1,0:T(8,128)(2,1)S(1)} %get-tuple-element.34), channel_id=1, source_target_pairs={{0,1},{1,0},{2,3},{3,2},{4,5},{5,4},{6,7},{7,6},{8,9},{9,8},{10,11... | collective-permute-start | bytes 3145736 | tf_op jit(solution)/shard_map/ppermute | solution.py:53
  82.9 8.7 %collective-permute-start.23 = (bf16[2,64,1024]{2,1,0:T(8,128)(2,1)S(1)}, bf16[2,64,1024]{2,1,0:T(8,128)(2,1)S(1)}, u32[]{:S(2)}, u32[]{:S(2)}) collective-permute-start(bf16[2,64,1024]{2,1,0:T(8,128)(2,1)S(1)} %fusion), channel_id=1, source_target_pairs={{0,4},{2,6},{4,0},{6,2},{1,5},{3,7},{5,1},{7,3},{8,12},{10,14},{12... | collective-permute-start | bytes 786440 | tf_op jit(solution)/shard_map/ppermute | solution.py:53
  84.6 9.0 %collective-permute-start.25 = (bf16[2,64,1024]{2,1,0:T(8,128)(2,1)S(1)}, bf16[2,64,1024]{2,1,0:T(8,128)(2,1)S(1)}, u32[]{:S(2)}, u32[]{:S(2)}) collective-permute-start(bf16[2,64,1024]{2,1,0:T(8,128)(2,1)S(1)} %fusion.1), channel_id=1, source_target_pairs={{0,8},{8,0},{16,24},{24,16},{1,9},{9,1},{17,25},{25,17},{2,10},{10... | collective-permute-start | bytes 786440 | tf_op jit(solution)/shard_map/ppermute | solution.py:53
  91.7 5.0 %collective-permute-start.24 = (bf16[64,1024]{1,0:T(8,128)(2,1)S(1)}, bf16[64,1024]{1,0:T(8,128)(2,1)S(1)}, u32[]{:S(2)}, u32[]{:S(2)}) collective-permute-start(bf16[64,1024]{1,0:T(8,128)(2,1)S(1)} %fusion.4), channel_id=1, source_target_pairs={{0,8},{8,0},{16,24},{24,16},{1,9},{9,1},{17,25},{25,17},{2,10},{10... | collective-permute-start | bytes 393224 | tf_op jit(solution)/shard_map/ppermute | solution.py:53
  93.7 5.0 %collective-permute-start.26 = (bf16[64,1024]{1,0:T(8,128)(2,1)S(1)}, bf16[64,1024]{1,0:T(8,128)(2,1)S(1)}, u32[]{:S(2)}, u32[]{:S(2)}) collective-permute-start(bf16[64,1024]{1,0:T(8,128)(2,1)S(1)} %fusion.5), channel_id=1, source_target_pairs={{0,4},{2,6},{4,0},{6,2},{1,5},{3,7},{5,1},{7,3},{8,12},{10,14},{12... | collective-permute-start | bytes 393224 | tf_op jit(solution)/shard_map/ppermute | solution.py:53

commit v5 on v4

--- a/solution.py
+++ b/solution.py
@@ -135,7 +135,7 @@
     inputs, maps, pool_weight, rec_weight = refs[3:7], refs[7], refs[8], refs[9]
     messages, blocks, own_vectors, partner_vectors, pooled = refs[10:12], refs[12:14], *refs[14:17]
     group_map, group_rows, scale, bound, head_gain, sems = refs[17:]
-    _, _, half, row, _, core = places()
+    _, _, half, row, side, core = places()
     rows = inputs[0].shape[0]
     size = maps.shape[1]
     begin = pl.multiple_of(row * size, size)
@@ -150,6 +150,7 @@
     ]
     copies = []
     targets = []
+    top = pl.ds(pl.multiple_of(side * (rows // 2), rows // 2), rows // 2)
     for n, place in enumerate((1 - core, core)):
         column = pl.multiple_of((2 * row + place) * width, width)
         copies += [
@@ -160,13 +161,13 @@
             )
             for m, w in enumerate(inputs)
         ]
-        targets.append((place, blocks[n].at[pl.ds(rows + width, width), :]))
+        targets.append((place, slice(None), blocks[n].at[pl.ds(rows + width, width), :]))
     for n in range(2):
         place = jnp.where(n == 0, first, 1 - first)
-        targets.append((place, messages[n].at[pl.ds(width, width), :]))
-    for n, (place, target) in enumerate(targets):
+        targets.append((place, top, messages[n].at[pl.ds(width, width), :]))
+    for n, (place, columns, target) in enumerate(targets):
         at = pl.ds(pl.multiple_of((2 * row + place) * width, width), width)
-        copies.append(pltpu.make_async_copy(rec_weight.at[at, :], target, sems.at[10 + n]))
+        copies.append(pltpu.make_async_copy(rec_weight.at[at, columns], target, sems.at[10 + n]))
     for copy in group_copies + copies:
         copy.start()
     for copy in group_copies:
@@ -187,7 +188,7 @@
     for n in range(2):
         place = jnp.where(n == 0, first, 1 - first)
         messages[n][pl.ds(0, width), :] = pooled[
-            pl.ds(pl.multiple_of(place * width, width), width), :
+            pl.ds(pl.multiple_of(place * width, width), width), top
         ]
     for copy in copies:
         copy.wait()
@@ -355,20 +356,22 @@
 
 def output_kernel(width, rows_each, *refs):
     own_vectors, partner_vectors, read_local, read_full, pool_rows, carry = refs[:6]
-    pieces, blocks = refs[6:10], refs[10:12]
-    sent, kept = refs[12:14]
-    weight_out, mixed, sems = refs[14:]
-    plane, late, half, row, _, core = places()
+    pieces, blocks = refs[6:14], refs[14:16]
+    sent, kept = refs[16:18]
+    weight_out, mixed, sems = refs[18:]
+    plane, late, half, row, side, core = places()
     owns = core == half
     plane_rows = 4 * width
+    part = plane_rows // 2
     length = 4 * rows_each
 
     def put(source, n):
-        return weight_out.at[source]
+        x = side if n == 0 else 1 - side
+        return weight_out.at[source, :, pl.ds(pl.multiple_of(x * part, part), part)]
 
     ends = [[(block.at[pl.ds(plane_rows, 2 * width), :], weight_out.at[plane])] for block in blocks]
-    singles = [[piece] for piece in pieces]
-    waits = start_pieces(singles, ends, sems, plane, core, owns, put)
+    pairs = [pieces[2 * n : 2 * n + 2] for n in range(4)]
+    waits = start_pieces(pairs, ends, sems, plane, core, owns, put)
     head_gain = jnp.where(owns, own_vectors[pl.ds(1, 1), :], partner_vectors[pl.ds(1, 1), :])
     group = 2 * half + row
     window = jnp.left_shift(jnp.int32(2), group)
@@ -404,6 +407,22 @@
                 ).astype(jnp.bfloat16)
 
 
+def join_kernel(*refs):
+    kept, received, left_send, right_send, left_keep, right_keep = refs
+    _, _, half, row, _, _ = places()
+    middle = kept.shape[-1] // 2
+    left, right = pl.ds(0, middle), pl.ds(middle, middle)
+    for n in range(2):
+        for target, at in (
+            (left_send, (1 - row, n, slice(None), left)),
+            (right_send, (n, 1 - half, slice(None), right)),
+            (left_keep, (row, n, slice(None), left)),
+            (right_keep, (n, half, slice(None), right)),
+        ):
+            total = kept[at].astype(jnp.float32) + received[at].astype(jnp.float32)
+            target[n] = total.astype(target.dtype)
+
+
 def by_halves(
     tokens,
     input_norm_gain,
@@ -462,7 +481,7 @@
     )(*far(tokens[0], input_norm_gain[None], decay_spike[0].T), *weights_in)
     *out_messages, partner_block, own_block, vectors, partner_vectors, _ = pl.pallas_call(
         pack,
-        out_shape=[made(2 * width, 4 * width)] * 2
+        out_shape=[made(2 * width, part)] * 2
         + [made(2 * part + 2 * width, 4 * width)] * 2
         + [made(2, width, kind=jnp.float32)] * 2
         + [made(2 * width, 4 * width)],
@@ -509,9 +528,7 @@
         return pieces
 
     pieces = shared(messages)
-    output_pieces = []
-    for which, pairs in rounds:
-        output_pieces.append(lax.ppermute(out_messages[which], ("sp", "tp"), pairs))
+    output_pieces = shared(out_messages)
     partner_local = swapped(partner_block, "tp", 1)
 
     received_vectors = swapped(partner_vectors, "tp", 1)
@@ -560,12 +577,12 @@
     sent, kept = pl.pallas_call(
         output,
         out_shape=[half_shape] * 2,
-        in_specs=[vmem] * 12,
+        in_specs=[vmem] * 16,
         out_specs=[vmem] * 2,
         scratch_shapes=[
             pltpu.VMEM((planes, 2 * width, 4 * width), jnp.bfloat16),
             pltpu.VMEM((length, 2 * width), jnp.bfloat16),
-            pltpu.SemaphoreType.DMA((4,)),
+            pltpu.SemaphoreType.DMA((7,)),
         ],
         compiler_params=pltpu.CompilerParams(vmem_limit_bytes=20 * MEBI),
         name="output",
@@ -576,16 +593,19 @@
     from_partner = swapped(sent, "tp", 1)
     middle = features // 2
 
-    def joined(place, axis, columns):
-        return sum(
-            picked(v[..., columns], place, axis).astype(jnp.float32) for v in (kept, from_partner)
-        )
-
-    left, right = slice(0, middle), slice(middle, features)
-    left_in = swapped(joined(1 - row, 0, left).astype(jnp.bfloat16), "fs", 2)
-    right_in = swapped(joined(1 - half, 1, right).astype(jnp.bfloat16), "sp", 1)
-    left_sum = joined(row, 0, left) + left_in.astype(jnp.float32)
-    right_sum = joined(half, 1, right) + right_in.astype(jnp.float32)
+    portion = (2, rows_each, middle)
+    left_send, right_send, left_keep, right_keep = pl.pallas_call(
+        join_kernel,
+        out_shape=[made(*portion)] * 2 + [made(*portion, kind=jnp.float32)] * 2,
+        in_specs=[vmem] * 2,
+        out_specs=[vmem] * 4,
+        compiler_params=pltpu.CompilerParams(vmem_limit_bytes=12 * MEBI),
+        name="join",
+    )(*near(kept, from_partner))
+    left_in = swapped(left_send, "fs", 2)
+    right_in = swapped(right_send, "sp", 1)
+    left_sum = left_keep + left_in.astype(jnp.float32)
+    right_sum = right_keep + right_in.astype(jnp.float32)
     left_last = swapped(picked(left_sum, 1 - half).astype(jnp.bfloat16), "sp", 1)
     right_last = swapped(picked(right_sum, 1 - row).astype(jnp.bfloat16), "fs", 2)
     left_total = picked(left_sum, half) + left_last.astype(jnp.float32)

time: 99.8 us -> 105 us (1.052)
  waiting for transfers between devices: 45.3 us -> 53.3 us
  starting transfers between devices: 42.2 us -> 40.7 us
  local copies, waits for them, and re-layouts: 1.43 us -> 0.05 us
    ppermute x4 -> x8, waiting for transfers between devices: 8.6 us -> 23.3 us  [shared(): arrived = lax.ppermute(pair[which], ('sp', 'tp'), pairs)]
    ppermute x4 -> x0, waiting for transfers between devices: 10.3 us -> none  [by_halves(): output_pieces.append(lax.ppermute(out_messages[which], ('sp', 'tp'), pairs))]
    ppermute x14, starting transfers between devices: 21.6 us -> 13.1 us  [swapped(): lax.ppermute(value, axis, [(source, source ^ bits) for source in range(co...]
    ppermute x4 -> x8, starting transfers between devices: 6.09 us -> 12.2 us  [shared(): pieces.append(lax.ppermute(arrived, ('fs', 'tp'), across))]
    ppermute x4 -> x8, starting transfers between devices: 7.72 us -> 11.2 us  [shared(): arrived = lax.ppermute(pair[which], ('sp', 'tp'), pairs)]
    ppermute x14, waiting for transfers between devices: 11.8 us -> 14.2 us  [swapped(): lax.ppermute(value, axis, [(source, source ^ bits) for source in range(co...]
    ppermute x4 -> x0, starting transfers between devices: 2.09 us -> none  [by_halves(): output_pieces.append(lax.ppermute(out_messages[which], ('sp', 'tp'), pairs))]
    ppermute x1, waiting for transfers between devices: 0.01 us -> 1.92 us  [by_halves(): lax.ppermute(carry, 'sp', [(p, p + 2) for p in range(planes - 2)])]
  transfers between devices with their start and end apart: 27 -> 31, of which waited for: 10 -> 11; matrix products, arithmetic and copies ran while one was open for 0% -> 0% of each run, Pallas kernels for 6% -> 4%
where the time goes in v5:
time: 105 us
  waiting for transfers between devices  53.3 us (51%)
  starting transfers between devices  40.7 us (39%)
  Pallas kernels  9.42 us (9%)
    ppermute x8, waiting for transfers between devices, shared(): arrived = lax.ppermute(pair[which], ('sp', 'tp'), pairs)  23.3 us
    ppermute x14, waiting for transfers between devices, swapped(): lax.ppermute(value, axis, [(source, source ^ bits) for source in range(co...  14.2 us
    ppermute x8, waiting for transfers between devices, shared(): pieces.append(lax.ppermute(arrived, ('fs', 'tp'), across))  13.8 us
    ppermute x14, starting transfers between devices, swapped(): lax.ppermute(value, axis, [(source, source ^ bits) for source in range(co...  13.1 us
    ppermute x8, starting transfers between devices, shared(): pieces.append(lax.ppermute(arrived, ('fs', 'tp'), across))  12.2 us
    ppermute x8, starting transfers between devices, shared(): arrived = lax.ppermute(pair[which], ('sp', 'tp'), pairs)  11.2 us
    ppermute x1, starting transfers between devices, by_halves(): lax.ppermute(carry, 'sp', [(p, p + 2) for p in range(planes - 2)])  4.22 us
    pallas_call x1, Pallas kernels, by_halves(): pl.pallas_call(state, out_shape=[made(length, width, kind=jnp.float32), m...  3.44 us
  transfers between devices with their start and end apart: 31, of which 11 were waited for; matrix products, arithmetic and copies ran while one was open for 0% of the time, Pallas kernels for 4%

profile of v5, /device:TPU:0, one launch (start us, length us, event | category | flops | bytes accessed | tf_op | source)
XLA Modules:
  0.0 104.6 jit_solution(11054514268759377976)
XLA Ops:
  0.0 2.4 %pack.1 = (bf16[256,256]{1,0:T(8,128)(2,1)S(1)}, bf16[256,256]{1,0:T(8,128)(2,1)S(1)}, bf16[768,512]{1,0:T(8,128)(2,1)S(1)}, bf16[768,512]{1,0:T(8,128)(2,1)S(1)...) custom-call(f32[1,512]{1,0:T(1,128)} %bitcast.30, f32[1,512]{1,0:T(1,128)} %bitcast.31, ...), custom_call_target="tpu_custom_call" | custom-call | tf_op jit(solution)/shard_map/pack/pallas_call | solution.py:482
  2.4 4.1 %collective-permute-start.18 = (bf16[256,256]{1,0:T(8,128)(2,1)S(1)}, bf16[256,256]{1,0:T(8,128)(2,1)S(1)}, u32[]{:S(2)}, u32[]{:S(2)}) collective-permute-start(bf16[256,256]{1,0:T(8,128)(2,1)S(1)} %get-tuple-element.35), channel_id=1, source_target_pairs={{16,0},{8,1},{25,8},{17,9},{0,16},{24,17},{9,24},{1,25},{18,2},{10... | collective-permute-start | bytes 393224 | tf_op jit(solution)/shard_map/ppermute | solution.py:523
  6.5 1.2 %first.1 = (bf16[256,512]{1,0:T(8,128)(2,1)S(1)}, bf16[256,512]{1,0:T(8,128)(2,1)S(1)}, bf16[72,2048]{1,0:T(8,128)(2,1)S(1)}) custom-call(bf16[64,2048]{1,0:T(8,128)(2,1)} %bitcast.28, f32[1,2048]{1,0:T(1,128)} %bitcast.29, f32[4,128]{1,0:T(4,128)} %bitcast.33, bf16[512,512]{1,0:T(8,128)(2,1)} %refs_3_.3, bf16[512,512]{1,0:T(8,128)(2,1)} %refs_4_.3, ...), custom_call_target="tpu_custom_call" | custom-call | tf_op jit(solution)/shard_map/first/pallas_call | solution.py:468
  8.1 1.3 %collective-permute-start.12 = (bf16[256,512]{1,0:T(8,128)(2,1)S(1)}, bf16[256,512]{1,0:T(8,128)(2,1)S(1)}, u32[]{:S(2)}, u32[]{:S(2)}) collective-permute-start(bf16[256,512]{1,0:T(8,128)(2,1)S(1)} %get-tuple-element.28), channel_id=1, source_target_pairs={{24,0},{1,8},{8,16},{17,24},{26,2},{3,10},{10,18},{19,26},{28,4},{... | collective-permute-start | bytes 786440 | tf_op jit(solution)/shard_map/ppermute | solution.py:523
  9.3 2.6 %collective-permute-start = (f32[2,128]{1,0:T(2,128)S(1)}, f32[2,128]{1,0:T(2,128)S(1)}, u32[]{:S(2)}, u32[]{:S(2)}) collective-permute-start(f32[2,128]{1,0:T(2,128)S(1)} %get-tuple-element.25), channel_id=1, source_target_pairs={{0,1},{1,0},{2,3},{3,2},{4,5},{5,4},{6,7},{7,6},{8,9},{9,8},{10,11... | collective-permute-start | bytes 3080 | tf_op jit(solution)/shard_map/ppermute | solution.py:53
  12.0 0.8 collective-permute-done.refs_1_
  13.5 1.3 %collective-permute-start.22 = (bf16[256,256]{1,0:T(8,128)(2,1)S(1)}, bf16[256,256]{1,0:T(8,128)(2,1)S(1)}, u32[]{:S(2)}, u32[]{:S(2)}) collective-permute-start(bf16[256,256]{1,0:T(8,128)(2,1)S(1)} %get-tuple-element.36), channel_id=1, source_target_pairs={{24,0},{1,8},{8,16},{17,24},{26,2},{3,10},{10,18},{19,26},{28,4},{... | collective-permute-start | bytes 393224 | tf_op jit(solution)/shard_map/ppermute | solution.py:523
  15.5 14.5 %collective-permute-done.22.refs_10_ = bf16[256,256]{1,0:T(8,128)(2,1)S(1)} collective-permute-done((bf16[256,256]{1,0:T(8,128)(2,1)S(1)}, bf16[256,256]{1,0:T(8,128)(2,1)S(1)}, u32[]{:S(2)}, u32[]{:S(2)}) %collective-permute-start.22) | collective-permute-done | bytes 131104 | tf_op jit(solution)/shard_map/ppermute | solution.py:523
  30.0 2.5 %collective-permute-start.4 = (bf16[72,2048]{1,0:T(8,128)(2,1)S(1)}, bf16[72,2048]{1,0:T(8,128)(2,1)S(1)}, u32[]{:S(2)}, u32[]{:S(2)}) collective-permute-start(bf16[72,2048]{1,0:T(8,128)(2,1)S(1)} %get-tuple-element.26.refs_2_), channel_id=1, source_target_pairs={{0,8},{8,0},{16,24},{24,16},{1,9},{9,1},{17,25},{25,17},{2,10},{10... | collective-permute-start | bytes 884744 | tf_op jit(solution)/shard_map/ppermute | solution.py:53
  32.5 1.5 %collective-permute-start.2 = (bf16[72,2048]{1,0:T(8,128)(2,1)S(1)}, bf16[72,2048]{1,0:T(8,128)(2,1)S(1)}, u32[]{:S(2)}, u32[]{:S(2)}) collective-permute-start(bf16[72,2048]{1,0:T(8,128)(2,1)S(1)} %get-tuple-element.26.refs_2_), channel_id=1, source_target_pairs={{0,4},{2,6},{4,0},{6,2},{1,5},{3,7},{5,1},{7,3},{8,12},{10,14},{12... | collective-permute-start | bytes 884744 | tf_op jit(solution)/shard_map/ppermute | solution.py:53
  34.0 2.9 %collective-permute-start.8 = (bf16[256,512]{1,0:T(8,128)(2,1)S(1)}, bf16[256,512]{1,0:T(8,128)(2,1)S(1)}, u32[]{:S(2)}, u32[]{:S(2)}) collective-permute-start(bf16[256,512]{1,0:T(8,128)(2,1)S(1)} %get-tuple-element.27), channel_id=1, source_target_pairs={{16,0},{8,1},{25,8},{17,9},{0,16},{24,17},{9,24},{1,25},{18,2},{10... | collective-permute-start | bytes 786440 | tf_op jit(solution)/shard_map/ppermute | solution.py:523
  36.9 0.8 collective-permute-start.16
  37.6 8.8 %collective-permute-done.8.refs_10_ = bf16[256,512]{1,0:T(8,128)(2,1)S(1)} collective-permute-done((bf16[256,512]{1,0:T(8,128)(2,1)S(1)}, bf16[256,512]{1,0:T(8,128)(2,1)S(1)}, u32[]{:S(2)}, u32[]{:S(2)}) %collective-permute-start.8) | collective-permute-done | bytes 262176 | tf_op jit(solution)/shard_map/ppermute | solution.py:523
  46.4 1.5 %collective-permute-start.11 = (bf16[256,512]{1,0:T(8,128)(2,1)S(1)}, bf16[256,512]{1,0:T(8,128)(2,1)S(1)}, u32[]{:S(2)}, u32[]{:S(2)}) collective-permute-start(bf16[256,512]{1,0:T(8,128)(2,1)S(1)} %collective-permute-done.10.refs_12_), channel_id=1, source_target_pairs={{0,2},{1,3},{2,0},{3,1},{4,6},{5,7},{6,4},{7,5},{8,10},{9,11},{10,... | collective-permute-start | bytes 786440 | tf_op jit(solution)/shard_map/ppermute | solution.py:527
  47.9 2.4 %collective-permute-start.13 = (bf16[256,512]{1,0:T(8,128)(2,1)S(1)}, bf16[256,512]{1,0:T(8,128)(2,1)S(1)}, u32[]{:S(2)}, u32[]{:S(2)}) collective-permute-start(bf16[256,512]{1,0:T(8,128)(2,1)S(1)} %collective-permute-done.12.refs_14_), channel_id=1, source_target_pairs={{0,2},{2,0},{4,6},{6,4},{8,10},{10,8},{12,14},{14,12},{16,18},{18,... | collective-permute-start | bytes 786440 | tf_op jit(solution)/shard_map/ppermute | solution.py:527
  51.6 3.0 %collective-permute-done.11.refs_13_ = bf16[256,512]{1,0:T(8,128)(2,1)S(1)} collective-permute-done((bf16[256,512]{1,0:T(8,128)(2,1)S(1)}, bf16[256,512]{1,0:T(8,128)(2,1)S(1)}, u32[]{:S(2)}, u32[]{:S(2)}) %collective-permute-start.11) | collective-permute-done | bytes 262176 | tf_op jit(solution)/shard_map/ppermute | solution.py:527
  54.6 3.8 %collective-permute-done.13.refs_15_ = bf16[256,512]{1,0:T(8,128)(2,1)S(1)} collective-permute-done((bf16[256,512]{1,0:T(8,128)(2,1)S(1)}, bf16[256,512]{1,0:T(8,128)(2,1)S(1)}, u32[]{:S(2)}, u32[]{:S(2)}) %collective-permute-start.13) | collective-permute-done | bytes 262176 | tf_op jit(solution)/shard_map/ppermute | solution.py:527
  58.4 1.5 %collective-permute-start.9 = (bf16[256,512]{1,0:T(8,128)(2,1)S(1)}, bf16[256,512]{1,0:T(8,128)(2,1)S(1)}, u32[]{:S(2)}, u32[]{:S(2)}) collective-permute-start(bf16[256,512]{1,0:T(8,128)(2,1)S(1)} %collective-permute-done.8.refs_10_), channel_id=1, source_target_pairs={{0,2},{1,3},{2,0},{3,1},{4,6},{5,7},{6,4},{7,5},{8,10},{9,11},{10,... | collective-permute-start | bytes 786440 | tf_op jit(solution)/shard_map/ppermute | solution.py:527
  60.1 7.0 %collective-permute-done.9.refs_11_ = bf16[256,512]{1,0:T(8,128)(2,1)S(1)} collective-permute-done((bf16[256,512]{1,0:T(8,128)(2,1)S(1)}, bf16[256,512]{1,0:T(8,128)(2,1)S(1)}, u32[]{:S(2)}, u32[]{:S(2)}) %collective-permute-start.9) | collective-permute-done | bytes 262176 | tf_op jit(solution)/shard_map/ppermute | solution.py:527
  67.1 1.5 %collective-permute-start.19 = (bf16[256,256]{1,0:T(8,128)(2,1)S(1)}, bf16[256,256]{1,0:T(8,128)(2,1)S(1)}, u32[]{:S(2)}, u32[]{:S(2)}) collective-permute-start(bf16[256,256]{1,0:T(8,128)(2,1)S(1)} %collective-permute-done.18.refs_6_), channel_id=1, source_target_pairs={{0,2},{1,3},{2,0},{3,1},{4,6},{5,7},{6,4},{7,5},{8,10},{9,11},{10,... | collective-permute-start | bytes 393224 | tf_op jit(solution)/shard_map/ppermute | solution.py:527
  69.1 3.4 %collective-permute-start.23 = (bf16[256,256]{1,0:T(8,128)(2,1)S(1)}, bf16[256,256]{1,0:T(8,128)(2,1)S(1)}, u32[]{:S(2)}, u32[]{:S(2)}) collective-permute-start(bf16[256,256]{1,0:T(8,128)(2,1)S(1)} %collective-permute-done.22.refs_10_), channel_id=1, source_target_pairs={{0,2},{2,0},{4,6},{6,4},{8,10},{10,8},{12,14},{14,12},{16,18},{18,... | collective-permute-start | bytes 393224 | tf_op jit(solution)/shard_map/ppermute | solution.py:527
  73.2 3.4 %state.1 = (f32[512,128]{1,0:T(8,128)S(1)}, bf16[512,128]{1,0:T(8,128)(2,1)S(1)}, bf16[512,128]{1,0:T(8,128)(2,1)S(1)}, bf16[288,128]{1,0:T(8,128)(2,1)S(1)}) custom-call(f32[2,128]{1,0:T(2,128)S(1)} %get-tuple-element.24.refs_0_, f32[2,128]{1,0:T(2,128)S(1)} %collective-permute-done.refs_1_, bf16[72,2048]{1,0:T(8,128)(2,1)S(1)} %get-tuple-element.26.refs_2_, ...), custom_call_target="tpu_custom_call" | custom-call | tf_op jit(solution)/shard_map/state/pallas_call | solution.py:549
  76.7 4.2 %collective-permute-start.17 = (bf16[288,128]{1,0:T(8,128)(2,1)S(1)}, bf16[288,128]{1,0:T(8,128)(2,1)S(1)}, u32[]{:S(2)}, u32[]{:S(2)}) collective-permute-start(bf16[288,128]{1,0:T(8,128)(2,1)S(1)} %get-tuple-element.34), channel_id=1, source_target_pairs={{0,16},{8,24},{1,17},{9,25},{2,18},{10,26},{3,19},{11,27},{4,20},{... | collective-permute-start | bytes 221192 | tf_op jit(solution)/shard_map/ppermute | solution.py:571
  80.9 1.9 %collective-permute-done.17.refs_5_ = bf16[288,128]{1,0:T(8,128)(2,1)S(1)} collective-permute-done((bf16[288,128]{1,0:T(8,128)(2,1)S(1)}, bf16[288,128]{1,0:T(8,128)(2,1)S(1)}, u32[]{:S(2)}, u32[]{:S(2)}) %collective-permute-start.17) | collective-permute-done | bytes 73760 | tf_op jit(solution)/shard_map/ppermute | solution.py:571
  82.8 2.2 %output.1 = (bf16[2,2,64,2048]{3,2,1,0:T(8,128)(2,1)S(1)}, bf16[2,2,64,2048]{3,2,1,0:T(8,128)(2,1)S(1)}) custom-call(f32[2,128]{1,0:T(2,128)S(1)} %get-tuple-element.24.refs_0_, f32[2,128]{1,0:T(2,128)S(1)} %collective-permute-done.refs_1_, f32[512,128]{1,0:T(8,128)S(1)} %get-tuple-element.31.refs_2_, bf16[512,128]{1,0:T(8,128)(2,1)S(1)} %get-tuple-element.32.refs_3_, ...), custom_call_target="tpu_custom_call" | custom-call | tf_op jit(solution)/shard_map/output/pallas_call | solution.py:577
  85.1 2.6 %collective-permute-done.26.refs_1_ = bf16[2,2,64,2048]{3,2,1,0:T(8,128)(2,1)S(1)} collective-permute-done((bf16[2,2,64,2048]{3,2,1,0:T(8,128)(2,1)S(1)}, bf16[2,2,64,2048]{3,2,1,0:T(8,128)(2,1)S(1)}, u32[]{:S(2)}, u32[]{:S(2)}) %collective-permute-start.26) | collective-permute-done | bytes 1048608 | tf_op jit(solution)/shard_map/ppermute | solution.py:53
  88.0 1.3 %collective-permute-start.27 = (bf16[2,64,1024]{2,1,0:T(8,128)(2,1)S(1)}, bf16[2,64,1024]{2,1,0:T(8,128)(2,1)S(1)}, u32[]{:S(2)}, u32[]{:S(2)}) collective-permute-start(bf16[2,64,1024]{2,1,0:T(8,128)(2,1)S(1)} %get-tuple-element.40), channel_id=1, source_target_pairs={{0,4},{2,6},{4,0},{6,2},{1,5},{3,7},{5,1},{7,3},{8,12},{10,14},{12... | collective-permute-start | bytes 786440 | tf_op jit(solution)/shard_map/ppermute | solution.py:53
  89.2 1.0 collective-permute-start.29
  90.3 6.1 %collective-permute-done.27 = bf16[2,64,1024]{2,1,0:T(8,128)(2,1)S(1)} collective-permute-done((bf16[2,64,1024]{2,1,0:T(8,128)(2,1)S(1)}, bf16[2,64,1024]{2,1,0:T(8,128)(2,1)S(1)}, u32[]{:S(2)}, u32[]{:S(2)}) %collective-permute-start.27) | collective-permute-done | bytes 262176 | tf_op jit(solution)/shard_map/ppermute | solution.py:53
  96.5 2.2 %collective-permute-start.28 = (bf16[64,1024]{1,0:T(8,128)(2,1)S(1)}, bf16[64,1024]{1,0:T(8,128)(2,1)S(1)}, u32[]{:S(2)}, u32[]{:S(2)}) collective-permute-start(bf16[64,1024]{1,0:T(8,128)(2,1)S(1)} %fusion.2), channel_id=1, source_target_pairs={{0,8},{8,0},{16,24},{24,16},{1,9},{9,1},{17,25},{25,17},{2,10},{10... | collective-permute-start | bytes 393224 | tf_op jit(solution)/shard_map/ppermute | solution.py:53
  99.1 2.5 %collective-permute-done.28 = bf16[64,1024]{1,0:T(8,128)(2,1)S(1)} collective-permute-done((bf16[64,1024]{1,0:T(8,128)(2,1)S(1)}, bf16[64,1024]{1,0:T(8,128)(2,1)S(1)}, u32[]{:S(2)}, u32[]{:S(2)}) %collective-permute-start.28) | collective-permute-done | bytes 131104 | tf_op jit(solution)/shard_map/ppermute | solution.py:53
  101.7 2.2 %collective-permute-done.30 = bf16[64,1024]{1,0:T(8,128)(2,1)S(1)} collective-permute-done((bf16[64,1024]{1,0:T(8,128)(2,1)S(1)}, bf16[64,1024]{1,0:T(8,128)(2,1)S(1)}, u32[]{:S(2)}, u32[]{:S(2)}) %collective-permute-start.30) | collective-permute-done | bytes 131104 | tf_op jit(solution)/shard_map/ppermute | solution.py:53
  (42 shorter events, 6.0 us)
Async XLA Ops:
  2.4 11.1 %collective-permute-start.18 = (bf16[256,256]{1,0:T(8,128)(2,1)S(1)}, bf16[256,256]{1,0:T(8,128)(2,1)S(1)}, u32[]{:S(2)}, u32[]{:S(2)}) collective-permute-start(bf16[256,256]{1,0:T(8,128)(2,1)S(1)} %get-tuple-element.35), channel_id=1, source_target_pairs={{16,0},{8,1},{25,8},{17,9},{0,16},{24,17},{9,24},{1,25},{18,2},{10... | collective-permute-start | bytes 393224 | tf_op jit(solution)/shard_map/ppermute | solution.py:523
  6.5 8.3 %collective-permute-start.20 = (bf16[256,256]{1,0:T(8,128)(2,1)S(1)}, bf16[256,256]{1,0:T(8,128)(2,1)S(1)}, u32[]{:S(2)}, u32[]{:S(2)}) collective-permute-start(bf16[256,256]{1,0:T(8,128)(2,1)S(1)} %get-tuple-element.36), channel_id=1, source_target_pairs={{16,1},{8,0},{25,9},{17,8},{0,17},{24,16},{9,25},{1,24},{18,3},{10... | collective-permute-start | bytes 393224 | tf_op jit(solution)/shard_map/ppermute | solution.py:523
  7.8 26.2 %collective-permute-start.10 = (bf16[256,512]{1,0:T(8,128)(2,1)S(1)}, bf16[256,512]{1,0:T(8,128)(2,1)S(1)}, u32[]{:S(2)}, u32[]{:S(2)}) collective-permute-start(bf16[256,512]{1,0:T(8,128)(2,1)S(1)} %get-tuple-element.28), channel_id=1, source_target_pairs={{16,1},{8,0},{25,9},{17,8},{0,17},{24,16},{9,25},{1,24},{18,3},{10... | collective-permute-start | bytes 786440 | tf_op jit(solution)/shard_map/ppermute | solution.py:523
  8.1 25.9 %collective-permute-start.12 = (bf16[256,512]{1,0:T(8,128)(2,1)S(1)}, bf16[256,512]{1,0:T(8,128)(2,1)S(1)}, u32[]{:S(2)}, u32[]{:S(2)}) collective-permute-start(bf16[256,512]{1,0:T(8,128)(2,1)S(1)} %get-tuple-element.28), channel_id=1, source_target_pairs={{24,0},{1,8},{8,16},{17,24},{26,2},{3,10},{10,18},{19,26},{28,4},{... | collective-permute-start | bytes 786440 | tf_op jit(solution)/shard_map/ppermute | solution.py:523
  9.3 3.4 %collective-permute-start = (f32[2,128]{1,0:T(2,128)S(1)}, f32[2,128]{1,0:T(2,128)S(1)}, u32[]{:S(2)}, u32[]{:S(2)}) collective-permute-start(f32[2,128]{1,0:T(2,128)S(1)} %get-tuple-element.25), channel_id=1, source_target_pairs={{0,1},{1,0},{2,3},{3,2},{4,5},{5,4},{6,7},{7,6},{8,9},{9,8},{10,11... | collective-permute-start | bytes 3080 | tf_op jit(solution)/shard_map/ppermute | solution.py:53
  12.8 24.1 %collective-permute-start.14 = (bf16[256,512]{1,0:T(8,128)(2,1)S(1)}, bf16[256,512]{1,0:T(8,128)(2,1)S(1)}, u32[]{:S(2)}, u32[]{:S(2)}) collective-permute-start(bf16[256,512]{1,0:T(8,128)(2,1)S(1)} %get-tuple-element.27), channel_id=1, source_target_pairs={{24,1},{1,9},{8,17},{17,25},{26,3},{3,11},{10,19},{19,27},{28,5},{... | collective-permute-start | bytes 786440 | tf_op jit(solution)/shard_map/ppermute | solution.py:523
  13.5 16.5 %collective-permute-start.22 = (bf16[256,256]{1,0:T(8,128)(2,1)S(1)}, bf16[256,256]{1,0:T(8,128)(2,1)S(1)}, u32[]{:S(2)}, u32[]{:S(2)}) collective-permute-start(bf16[256,256]{1,0:T(8,128)(2,1)S(1)} %get-tuple-element.36), channel_id=1, source_target_pairs={{24,0},{1,8},{8,16},{17,24},{26,2},{3,10},{10,18},{19,26},{28,4},{... | collective-permute-start | bytes 393224 | tf_op jit(solution)/shard_map/ppermute | solution.py:523
  14.8 17.7 %collective-permute-start.24 = (bf16[256,256]{1,0:T(8,128)(2,1)S(1)}, bf16[256,256]{1,0:T(8,128)(2,1)S(1)}, u32[]{:S(2)}, u32[]{:S(2)}) collective-permute-start(bf16[256,256]{1,0:T(8,128)(2,1)S(1)} %get-tuple-element.35), channel_id=1, source_target_pairs={{24,1},{1,9},{8,17},{17,25},{26,3},{3,11},{10,19},{19,27},{28,5},{... | collective-permute-start | bytes 393224 | tf_op jit(solution)/shard_map/ppermute | solution.py:523
  30.0 17.8 %collective-permute-start.4 = (bf16[72,2048]{1,0:T(8,128)(2,1)S(1)}, bf16[72,2048]{1,0:T(8,128)(2,1)S(1)}, u32[]{:S(2)}, u32[]{:S(2)}) collective-permute-start(bf16[72,2048]{1,0:T(8,128)(2,1)S(1)} %get-tuple-element.26.refs_2_), channel_id=1, source_target_pairs={{0,8},{8,0},{16,24},{24,16},{1,9},{9,1},{17,25},{25,17},{2,10},{10... | collective-permute-start | bytes 884744 | tf_op jit(solution)/shard_map/ppermute | solution.py:53
  32.5 17.8 %collective-permute-start.2 = (bf16[72,2048]{1,0:T(8,128)(2,1)S(1)}, bf16[72,2048]{1,0:T(8,128)(2,1)S(1)}, u32[]{:S(2)}, u32[]{:S(2)}) collective-permute-start(bf16[72,2048]{1,0:T(8,128)(2,1)S(1)} %get-tuple-element.26.refs_2_), channel_id=1, source_target_pairs={{0,4},{2,6},{4,0},{6,2},{1,5},{3,7},{5,1},{7,3},{8,12},{10,14},{12... | collective-permute-start | bytes 884744 | tf_op jit(solution)/shard_map/ppermute | solution.py:53
  34.0 16.9 %collective-permute-start.1 = (bf16[72,2048]{1,0:T(8,128)(2,1)S(1)}, bf16[72,2048]{1,0:T(8,128)(2,1)S(1)}, u32[]{:S(2)}, u32[]{:S(2)}) collective-permute-start(bf16[72,2048]{1,0:T(8,128)(2,1)S(1)} %get-tuple-element.26.refs_2_), channel_id=1, source_target_pairs={{0,1},{1,0},{2,3},{3,2},{4,5},{5,4},{6,7},{7,6},{8,9},{9,8},{10,11... | collective-permute-start | bytes 884744 | tf_op jit(solution)/shard_map/ppermute | solution.py:53
  34.0 12.4 %collective-permute-start.8 = (bf16[256,512]{1,0:T(8,128)(2,1)S(1)}, bf16[256,512]{1,0:T(8,128)(2,1)S(1)}, u32[]{:S(2)}, u32[]{:S(2)}) collective-permute-start(bf16[256,512]{1,0:T(8,128)(2,1)S(1)} %get-tuple-element.27), channel_id=1, source_target_pairs={{16,0},{8,1},{25,8},{17,9},{0,16},{24,17},{9,24},{1,25},{18,2},{10... | collective-permute-start | bytes 786440 | tf_op jit(solution)/shard_map/ppermute | solution.py:523
  36.9 35.7 %collective-permute-start.16 = (bf16[768,512]{1,0:T(8,128)(2,1)S(1)}, bf16[768,512]{1,0:T(8,128)(2,1)S(1)}, u32[]{:S(2)}, u32[]{:S(2)}) collective-permute-start(bf16[768,512]{1,0:T(8,128)(2,1)S(1)} %get-tuple-element.30), channel_id=1, source_target_pairs={{0,1},{1,0},{2,3},{3,2},{4,5},{5,4},{6,7},{7,6},{8,9},{9,8},{10,11... | collective-permute-start | bytes 2359304 | tf_op jit(solution)/shard_map/ppermute | solution.py:53
  46.4 8.2 %collective-permute-start.11 = (bf16[256,512]{1,0:T(8,128)(2,1)S(1)}, bf16[256,512]{1,0:T(8,128)(2,1)S(1)}, u32[]{:S(2)}, u32[]{:S(2)}) collective-permute-start(bf16[256,512]{1,0:T(8,128)(2,1)S(1)} %collective-permute-done.10.refs_12_), channel_id=1, source_target_pairs={{0,2},{1,3},{2,0},{3,1},{4,6},{5,7},{6,4},{7,5},{8,10},{9,11},{10,... | collective-permute-start | bytes 786440 | tf_op jit(solution)/shard_map/ppermute | solution.py:527
  47.9 10.5 %collective-permute-start.13 = (bf16[256,512]{1,0:T(8,128)(2,1)S(1)}, bf16[256,512]{1,0:T(8,128)(2,1)S(1)}, u32[]{:S(2)}, u32[]{:S(2)}) collective-permute-start(bf16[256,512]{1,0:T(8,128)(2,1)S(1)} %collective-permute-done.12.refs_14_), channel_id=1, source_target_pairs={{0,2},{2,0},{4,6},{6,4},{8,10},{10,8},{12,14},{14,12},{16,18},{18,... | collective-permute-start | bytes 786440 | tf_op jit(solution)/shard_map/ppermute | solution.py:527
  50.3 9.5 %collective-permute-start.6 = (bf16[72,2048]{1,0:T(8,128)(2,1)S(1)}, bf16[72,2048]{1,0:T(8,128)(2,1)S(1)}, u32[]{:S(2)}, u32[]{:S(2)}) collective-permute-start(bf16[72,2048]{1,0:T(8,128)(2,1)S(1)} %collective-permute-done.4.refs_6_), channel_id=1, source_target_pairs={{0,4},{2,6},{4,0},{6,2},{1,5},{3,7},{5,1},{7,3},{8,12},{10,14},{12... | collective-permute-start | bytes 884744 | tf_op jit(solution)/shard_map/ppermute | solution.py:53
  50.9 7.5 %collective-permute-start.15 = (bf16[256,512]{1,0:T(8,128)(2,1)S(1)}, bf16[256,512]{1,0:T(8,128)(2,1)S(1)}, u32[]{:S(2)}, u32[]{:S(2)}) collective-permute-start(bf16[256,512]{1,0:T(8,128)(2,1)S(1)} %collective-permute-done.14.refs_16_), channel_id=1, source_target_pairs={{1,3},{3,1},{5,7},{7,5},{9,11},{11,9},{13,15},{15,13},{17,19},{19,... | collective-permute-start | bytes 786440 | tf_op jit(solution)/shard_map/ppermute | solution.py:527
  54.6 14.0 %collective-permute-start.5 = (bf16[72,2048]{1,0:T(8,128)(2,1)S(1)}, bf16[72,2048]{1,0:T(8,128)(2,1)S(1)}, u32[]{:S(2)}, u32[]{:S(2)}) collective-permute-start(bf16[72,2048]{1,0:T(8,128)(2,1)S(1)} %collective-permute-done.4.refs_6_), channel_id=1, source_target_pairs={{0,1},{1,0},{2,3},{3,2},{4,5},{5,4},{6,7},{7,6},{8,9},{9,8},{10,11... | collective-permute-start | bytes 884744 | tf_op jit(solution)/shard_map/ppermute | solution.py:53
  58.3 10.8 %collective-permute-start.3 = (bf16[72,2048]{1,0:T(8,128)(2,1)S(1)}, bf16[72,2048]{1,0:T(8,128)(2,1)S(1)}, u32[]{:S(2)}, u32[]{:S(2)}) collective-permute-start(bf16[72,2048]{1,0:T(8,128)(2,1)S(1)} %collective-permute-done.2.refs_4_), channel_id=1, source_target_pairs={{0,1},{1,0},{2,3},{3,2},{4,5},{5,4},{6,7},{7,6},{8,9},{9,8},{10,11... | collective-permute-start | bytes 884744 | tf_op jit(solution)/shard_map/ppermute | solution.py:53
  58.4 8.7 %collective-permute-start.9 = (bf16[256,512]{1,0:T(8,128)(2,1)S(1)}, bf16[256,512]{1,0:T(8,128)(2,1)S(1)}, u32[]{:S(2)}, u32[]{:S(2)}) collective-permute-start(bf16[256,512]{1,0:T(8,128)(2,1)S(1)} %collective-permute-done.8.refs_10_), channel_id=1, source_target_pairs={{0,2},{1,3},{2,0},{3,1},{4,6},{5,7},{6,4},{7,5},{8,10},{9,11},{10,... | collective-permute-start | bytes 786440 | tf_op jit(solution)/shard_map/ppermute | solution.py:527
  59.8 13.3 %collective-permute-start.7 = (bf16[72,2048]{1,0:T(8,128)(2,1)S(1)}, bf16[72,2048]{1,0:T(8,128)(2,1)S(1)}, u32[]{:S(2)}, u32[]{:S(2)}) collective-permute-start(bf16[72,2048]{1,0:T(8,128)(2,1)S(1)} %collective-permute-done.6.refs_8_), channel_id=1, source_target_pairs={{0,1},{1,0},{2,3},{3,2},{4,5},{5,4},{6,7},{7,6},{8,9},{9,8},{10,11... | collective-permute-start | bytes 884744 | tf_op jit(solution)/shard_map/ppermute | solution.py:53
  67.1 13.8 %collective-permute-start.19 = (bf16[256,256]{1,0:T(8,128)(2,1)S(1)}, bf16[256,256]{1,0:T(8,128)(2,1)S(1)}, u32[]{:S(2)}, u32[]{:S(2)}) collective-permute-start(bf16[256,256]{1,0:T(8,128)(2,1)S(1)} %collective-permute-done.18.refs_6_), channel_id=1, source_target_pairs={{0,2},{1,3},{2,0},{3,1},{4,6},{5,7},{6,4},{7,5},{8,10},{9,11},{10,... | collective-permute-start | bytes 393224 | tf_op jit(solution)/shard_map/ppermute | solution.py:527
  68.6 12.3 %collective-permute-start.21 = (bf16[256,256]{1,0:T(8,128)(2,1)S(1)}, bf16[256,256]{1,0:T(8,128)(2,1)S(1)}, u32[]{:S(2)}, u32[]{:S(2)}) collective-permute-start(bf16[256,256]{1,0:T(8,128)(2,1)S(1)} %collective-permute-done.20.refs_8_), channel_id=1, source_target_pairs={{0,2},{1,3},{2,0},{3,1},{4,6},{5,7},{6,4},{7,5},{8,10},{9,11},{10,... | collective-permute-start | bytes 393224 | tf_op jit(solution)/shard_map/ppermute | solution.py:527
  69.1 11.8 %collective-permute-start.23 = (bf16[256,256]{1,0:T(8,128)(2,1)S(1)}, bf16[256,256]{1,0:T(8,128)(2,1)S(1)}, u32[]{:S(2)}, u32[]{:S(2)}) collective-permute-start(bf16[256,256]{1,0:T(8,128)(2,1)S(1)} %collective-permute-done.22.refs_10_), channel_id=1, source_target_pairs={{0,2},{2,0},{4,6},{6,4},{8,10},{10,8},{12,14},{14,12},{16,18},{18,... | collective-permute-start | bytes 393224 | tf_op jit(solution)/shard_map/ppermute | solution.py:527
  72.5 8.4 %collective-permute-start.25 = (bf16[256,256]{1,0:T(8,128)(2,1)S(1)}, bf16[256,256]{1,0:T(8,128)(2,1)S(1)}, u32[]{:S(2)}, u32[]{:S(2)}) collective-permute-start(bf16[256,256]{1,0:T(8,128)(2,1)S(1)} %collective-permute-done.24.refs_12_), channel_id=1, source_target_pairs={{1,3},{3,1},{5,7},{7,5},{9,11},{11,9},{13,15},{15,13},{17,19},{19,... | collective-permute-start | bytes 393224 | tf_op jit(solution)/shard_map/ppermute | solution.py:527
  76.7 6.2 %collective-permute-start.17 = (bf16[288,128]{1,0:T(8,128)(2,1)S(1)}, bf16[288,128]{1,0:T(8,128)(2,1)S(1)}, u32[]{:S(2)}, u32[]{:S(2)}) collective-permute-start(bf16[288,128]{1,0:T(8,128)(2,1)S(1)} %get-tuple-element.34), channel_id=1, source_target_pairs={{0,16},{8,24},{1,17},{9,25},{2,18},{10,26},{3,19},{11,27},{4,20},{... | collective-permute-start | bytes 221192 | tf_op jit(solution)/shard_map/ppermute | solution.py:571
  85.0 2.7 %collective-permute-start.26 = (bf16[2,2,64,2048]{3,2,1,0:T(8,128)(2,1)S(1)}, bf16[2,2,64,2048]{3,2,1,0:T(8,128)(2,1)S(1)}, u32[]{:S(2)}, u32[]{:S(2)}) collective-permute-start(bf16[2,2,64,2048]{3,2,1,0:T(8,128)(2,1)S(1)} %get-tuple-element.38), channel_id=1, source_target_pairs={{0,1},{1,0},{2,3},{3,2},{4,5},{5,4},{6,7},{7,6},{8,9},{9,8},{10,11... | collective-permute-start | bytes 3145736 | tf_op jit(solution)/shard_map/ppermute | solution.py:53
  88.0 8.4 %collective-permute-start.27 = (bf16[2,64,1024]{2,1,0:T(8,128)(2,1)S(1)}, bf16[2,64,1024]{2,1,0:T(8,128)(2,1)S(1)}, u32[]{:S(2)}, u32[]{:S(2)}) collective-permute-start(bf16[2,64,1024]{2,1,0:T(8,128)(2,1)S(1)} %get-tuple-element.40), channel_id=1, source_target_pairs={{0,4},{2,6},{4,0},{6,2},{1,5},{3,7},{5,1},{7,3},{8,12},{10,14},{12... | collective-permute-start | bytes 786440 | tf_op jit(solution)/shard_map/ppermute | solution.py:53
  89.2 9.4 %collective-permute-start.29 = (bf16[2,64,1024]{2,1,0:T(8,128)(2,1)S(1)}, bf16[2,64,1024]{2,1,0:T(8,128)(2,1)S(1)}, u32[]{:S(2)}, u32[]{:S(2)}) collective-permute-start(bf16[2,64,1024]{2,1,0:T(8,128)(2,1)S(1)} %get-tuple-element.42), channel_id=1, source_target_pairs={{0,8},{8,0},{16,24},{24,16},{1,9},{9,1},{17,25},{25,17},{2,10},{10... | collective-permute-start | bytes 786440 | tf_op jit(solution)/shard_map/ppermute | solution.py:53
  96.5 5.2 %collective-permute-start.28 = (bf16[64,1024]{1,0:T(8,128)(2,1)S(1)}, bf16[64,1024]{1,0:T(8,128)(2,1)S(1)}, u32[]{:S(2)}, u32[]{:S(2)}) collective-permute-start(bf16[64,1024]{1,0:T(8,128)(2,1)S(1)} %fusion.2), channel_id=1, source_target_pairs={{0,8},{8,0},{16,24},{24,16},{1,9},{9,1},{17,25},{25,17},{2,10},{10... | collective-permute-start | bytes 393224 | tf_op jit(solution)/shard_map/ppermute | solution.py:53
  98.8 5.0 %collective-permute-start.30 = (bf16[64,1024]{1,0:T(8,128)(2,1)S(1)}, bf16[64,1024]{1,0:T(8,128)(2,1)S(1)}, u32[]{:S(2)}, u32[]{:S(2)}) collective-permute-start(bf16[64,1024]{1,0:T(8,128)(2,1)S(1)} %fusion.3), channel_id=1, source_target_pairs={{0,4},{2,6},{4,0},{6,2},{1,5},{3,7},{5,1},{7,3},{8,12},{10,14},{12... | collective-permute-start | bytes 393224 | tf_op jit(solution)/shard_map/ppermute | solution.py:53

commit v6 on v5

--- a/solution.py
+++ b/solution.py
@@ -51,10 +51,6 @@
 def swapped(value, axis, bits):
     count = lax.axis_size(axis)
     return lax.ppermute(value, axis, [(source, source ^ bits) for source in range(count)])
-
-
-def picked(stack, place, axis=0):
-    return lax.dynamic_index_in_dim(stack, place, axis, False)
 
 
 def halves_divide(tokens, query_weight, pooling_input_weight, pooling_group_maps, decay_spike, out_weight):
@@ -408,19 +404,12 @@
 
 
 def join_kernel(*refs):
-    kept, received, left_send, right_send, left_keep, right_keep = refs
+    kept, received = refs[:2]
     _, _, half, row, _, _ = places()
-    middle = kept.shape[-1] // 2
-    left, right = pl.ds(0, middle), pl.ds(middle, middle)
-    for n in range(2):
-        for target, at in (
-            (left_send, (1 - row, n, slice(None), left)),
-            (right_send, (n, 1 - half, slice(None), right)),
-            (left_keep, (row, n, slice(None), left)),
-            (right_keep, (n, half, slice(None), right)),
-        ):
-            total = kept[at].astype(jnp.float32) + received[at].astype(jnp.float32)
-            target[n] = total.astype(target.dtype)
+    ends = ((1 - row, 1 - half), (1 - row, half), (row, 1 - half), (row, half))
+    for target, at in zip(refs[2:], ends):
+        total = kept[at].astype(jnp.float32) + received[at].astype(jnp.float32)
+        target[...] = total.astype(target.dtype)
 
 
 def by_halves(
@@ -439,7 +428,7 @@
     recurrent_output_weight,
 ):
     planes, members, cores = (lax.axis_size(axis) for axis in ("sp", "fs", "tp"))
-    _, _, half, row, _, _ = places()
+    plane, late, half, row, side, core = places()
     heads = decay_spike.shape[2]
     width = query_weight.shape[1] // heads
     features = tokens.shape[2]
@@ -591,26 +580,23 @@
         *near(*output_pieces, own_block, partner_local),
     )
     from_partner = swapped(sent, "tp", 1)
-    middle = features // 2
-
-    portion = (2, rows_each, middle)
-    left_send, right_send, left_keep, right_keep = pl.pallas_call(
+    portion = (rows_each, features)
+    across_send, row_send, plane_send, kept_rows = pl.pallas_call(
         join_kernel,
-        out_shape=[made(*portion)] * 2 + [made(*portion, kind=jnp.float32)] * 2,
+        out_shape=[made(*portion)] * 3 + [made(*portion, kind=jnp.float32)],
         in_specs=[vmem] * 2,
         out_specs=[vmem] * 4,
         compiler_params=pltpu.CompilerParams(vmem_limit_bytes=12 * MEBI),
         name="join",
     )(*near(kept, from_partner))
-    left_in = swapped(left_send, "fs", 2)
-    right_in = swapped(right_send, "sp", 1)
-    left_sum = left_keep + left_in.astype(jnp.float32)
-    right_sum = right_keep + right_in.astype(jnp.float32)
-    left_last = swapped(picked(left_sum, 1 - half).astype(jnp.bfloat16), "sp", 1)
-    right_last = swapped(picked(right_sum, 1 - row).astype(jnp.bfloat16), "fs", 2)
-    left_total = picked(left_sum, half) + left_last.astype(jnp.float32)
-    right_total = picked(right_sum, row) + right_last.astype(jnp.float32)
-    total = jnp.concatenate([left_total, right_total], axis=1)
+    corners = [
+        (p * members + f, (p ^ 1) * members + (f ^ 2)) for p in range(planes) for f in range(members)
+    ]
+    across = lax.ppermute(across_send, ("sp", "fs"), corners)
+    from_row = swapped(row_send, "fs", 2)
+    from_plane = swapped(plane_send, "sp", 1)
+    total = kept_rows + across.astype(jnp.float32) + from_row.astype(jnp.float32)
+    total = total + from_plane.astype(jnp.float32)
     return total.astype(jnp.bfloat16)[None]
 
 

time: 105 us -> 104 us (level)
  starting transfers between devices: 40.7 us -> 39.5 us
    ppermute x0 -> x1, waiting for transfers between devices: none -> 6.51 us  [by_halves(): across = lax.ppermute(across_send, ('sp', 'fs'), corners)]
    ppermute x14 -> x12, waiting for transfers between devices: 14.2 us -> 8.24 us  [swapped(): lax.ppermute(value, axis, [(source, source ^ bits) for source in range(co...]
    ppermute x14 -> x12, starting transfers between devices: 13.1 us -> 10.2 us  [swapped(): lax.ppermute(value, axis, [(source, source ^ bits) for source in range(co...]
    ppermute x0 -> x1, starting transfers between devices: none -> 1.66 us  [by_halves(): across = lax.ppermute(across_send, ('sp', 'fs'), corners)]
  transfers between devices with their start and end apart: 31 -> 30, of which waited for: 11 -> 10; matrix products, arithmetic and copies ran while one was open for 0% -> 0% of each run, Pallas kernels for 4% -> 5%
where the time goes in v6:
time: 104 us
  waiting for transfers between devices  53.8 us (52%)
  starting transfers between devices  39.5 us (38%)
  Pallas kernels  9.43 us (9%)
    ppermute x8, waiting for transfers between devices, shared(): arrived = lax.ppermute(pair[which], ('sp', 'tp'), pairs)  23.3 us
    ppermute x8, waiting for transfers between devices, shared(): pieces.append(lax.ppermute(arrived, ('fs', 'tp'), across))  13.8 us
    ppermute x8, starting transfers between devices, shared(): pieces.append(lax.ppermute(arrived, ('fs', 'tp'), across))  12.2 us
    ppermute x8, starting transfers between devices, shared(): arrived = lax.ppermute(pair[which], ('sp', 'tp'), pairs)  11.2 us
    ppermute x12, starting transfers between devices, swapped(): lax.ppermute(value, axis, [(source, source ^ bits) for source in range(co...  10.2 us
    ppermute x12, waiting for transfers between devices, swapped(): lax.ppermute(value, axis, [(source, source ^ bits) for source in range(co...  8.24 us
    ppermute x1, waiting for transfers between devices, by_halves(): across = lax.ppermute(across_send, ('sp', 'fs'), corners)  6.51 us
    ppermute x1, starting transfers between devices, by_halves(): lax.ppermute(carry, 'sp', [(p, p + 2) for p in range(planes - 2)])  4.22 us
  transfers between devices with their start and end apart: 30, of which 10 were waited for; matrix products, arithmetic and copies ran while one was open for 0% of the time, Pallas kernels for 5%

profile of v6, /device:TPU:0, one launch (start us, length us, event | category | flops | bytes accessed | tf_op | source)
XLA Modules:
  0.0 103.7 jit_solution(1430095387514925562)
XLA Ops:
  0.0 2.4 %pack.1 = (bf16[256,256]{1,0:T(8,128)(2,1)S(1)}, bf16[256,256]{1,0:T(8,128)(2,1)S(1)}, bf16[768,512]{1,0:T(8,128)(2,1)S(1)}, bf16[768,512]{1,0:T(8,128)(2,1)S(1)...) custom-call(f32[1,512]{1,0:T(1,128)} %bitcast.12, f32[1,512]{1,0:T(1,128)} %bitcast.13, ...), custom_call_target="tpu_custom_call" | custom-call | tf_op jit(solution)/shard_map/pack/pallas_call | solution.py:471
  2.4 4.1 %collective-permute-start.18 = (bf16[256,256]{1,0:T(8,128)(2,1)S(1)}, bf16[256,256]{1,0:T(8,128)(2,1)S(1)}, u32[]{:S(2)}, u32[]{:S(2)}) collective-permute-start(bf16[256,256]{1,0:T(8,128)(2,1)S(1)} %get-tuple-element.35), channel_id=1, source_target_pairs={{16,0},{8,1},{25,8},{17,9},{0,16},{24,17},{9,24},{1,25},{18,2},{10... | collective-permute-start | bytes 393224 | tf_op jit(solution)/shard_map/ppermute | solution.py:512
  6.5 1.2 %first.1 = (bf16[256,512]{1,0:T(8,128)(2,1)S(1)}, bf16[256,512]{1,0:T(8,128)(2,1)S(1)}, bf16[72,2048]{1,0:T(8,128)(2,1)S(1)}) custom-call(bf16[64,2048]{1,0:T(8,128)(2,1)} %bitcast.10, f32[1,2048]{1,0:T(1,128)} %bitcast.11, f32[4,128]{1,0:T(4,128)} %bitcast.15, bf16[512,512]{1,0:T(8,128)(2,1)} %refs_3_.3, bf16[512,512]{1,0:T(8,128)(2,1)} %refs_4_.3, ...), custom_call_target="tpu_custom_call" | custom-call | tf_op jit(solution)/shard_map/first/pallas_call | solution.py:457
  8.1 1.3 %collective-permute-start.12 = (bf16[256,512]{1,0:T(8,128)(2,1)S(1)}, bf16[256,512]{1,0:T(8,128)(2,1)S(1)}, u32[]{:S(2)}, u32[]{:S(2)}) collective-permute-start(bf16[256,512]{1,0:T(8,128)(2,1)S(1)} %get-tuple-element.28), channel_id=1, source_target_pairs={{24,0},{1,8},{8,16},{17,24},{26,2},{3,10},{10,18},{19,26},{28,4},{... | collective-permute-start | bytes 786440 | tf_op jit(solution)/shard_map/ppermute | solution.py:512
  9.3 2.6 %collective-permute-start = (f32[2,128]{1,0:T(2,128)S(1)}, f32[2,128]{1,0:T(2,128)S(1)}, u32[]{:S(2)}, u32[]{:S(2)}) collective-permute-start(f32[2,128]{1,0:T(2,128)S(1)} %get-tuple-element.25), channel_id=1, source_target_pairs={{0,1},{1,0},{2,3},{3,2},{4,5},{5,4},{6,7},{7,6},{8,9},{9,8},{10,11... | collective-permute-start | bytes 3080 | tf_op jit(solution)/shard_map/ppermute | solution.py:53
  12.0 0.8 collective-permute-done.refs_1_
  13.5 1.3 %collective-permute-start.22 = (bf16[256,256]{1,0:T(8,128)(2,1)S(1)}, bf16[256,256]{1,0:T(8,128)(2,1)S(1)}, u32[]{:S(2)}, u32[]{:S(2)}) collective-permute-start(bf16[256,256]{1,0:T(8,128)(2,1)S(1)} %get-tuple-element.36), channel_id=1, source_target_pairs={{24,0},{1,8},{8,16},{17,24},{26,2},{3,10},{10,18},{19,26},{28,4},{... | collective-permute-start | bytes 393224 | tf_op jit(solution)/shard_map/ppermute | solution.py:512
  14.8 0.7 collective-permute-start.24
  15.5 14.5 %collective-permute-done.22.refs_10_ = bf16[256,256]{1,0:T(8,128)(2,1)S(1)} collective-permute-done((bf16[256,256]{1,0:T(8,128)(2,1)S(1)}, bf16[256,256]{1,0:T(8,128)(2,1)S(1)}, u32[]{:S(2)}, u32[]{:S(2)}) %collective-permute-start.22) | collective-permute-done | bytes 131104 | tf_op jit(solution)/shard_map/ppermute | solution.py:512
  30.0 2.5 %collective-permute-start.4 = (bf16[72,2048]{1,0:T(8,128)(2,1)S(1)}, bf16[72,2048]{1,0:T(8,128)(2,1)S(1)}, u32[]{:S(2)}, u32[]{:S(2)}) collective-permute-start(bf16[72,2048]{1,0:T(8,128)(2,1)S(1)} %get-tuple-element.26.refs_2_), channel_id=1, source_target_pairs={{0,8},{8,0},{16,24},{24,16},{1,9},{9,1},{17,25},{25,17},{2,10},{10... | collective-permute-start | bytes 884744 | tf_op jit(solution)/shard_map/ppermute | solution.py:53
  32.5 1.5 %collective-permute-start.2 = (bf16[72,2048]{1,0:T(8,128)(2,1)S(1)}, bf16[72,2048]{1,0:T(8,128)(2,1)S(1)}, u32[]{:S(2)}, u32[]{:S(2)}) collective-permute-start(bf16[72,2048]{1,0:T(8,128)(2,1)S(1)} %get-tuple-element.26.refs_2_), channel_id=1, source_target_pairs={{0,4},{2,6},{4,0},{6,2},{1,5},{3,7},{5,1},{7,3},{8,12},{10,14},{12... | collective-permute-start | bytes 884744 | tf_op jit(solution)/shard_map/ppermute | solution.py:53
  34.0 2.9 %collective-permute-start.8 = (bf16[256,512]{1,0:T(8,128)(2,1)S(1)}, bf16[256,512]{1,0:T(8,128)(2,1)S(1)}, u32[]{:S(2)}, u32[]{:S(2)}) collective-permute-start(bf16[256,512]{1,0:T(8,128)(2,1)S(1)} %get-tuple-element.27), channel_id=1, source_target_pairs={{16,0},{8,1},{25,8},{17,9},{0,16},{24,17},{9,24},{1,25},{18,2},{10... | collective-permute-start | bytes 786440 | tf_op jit(solution)/shard_map/ppermute | solution.py:512
  36.9 0.8 collective-permute-start.16
  37.6 8.8 %collective-permute-done.8.refs_10_ = bf16[256,512]{1,0:T(8,128)(2,1)S(1)} collective-permute-done((bf16[256,512]{1,0:T(8,128)(2,1)S(1)}, bf16[256,512]{1,0:T(8,128)(2,1)S(1)}, u32[]{:S(2)}, u32[]{:S(2)}) %collective-permute-start.8) | collective-permute-done | bytes 262176 | tf_op jit(solution)/shard_map/ppermute | solution.py:512
  46.4 1.5 %collective-permute-start.11 = (bf16[256,512]{1,0:T(8,128)(2,1)S(1)}, bf16[256,512]{1,0:T(8,128)(2,1)S(1)}, u32[]{:S(2)}, u32[]{:S(2)}) collective-permute-start(bf16[256,512]{1,0:T(8,128)(2,1)S(1)} %collective-permute-done.10.refs_12_), channel_id=1, source_target_pairs={{0,2},{1,3},{2,0},{3,1},{4,6},{5,7},{6,4},{7,5},{8,10},{9,11},{10,... | collective-permute-start | bytes 786440 | tf_op jit(solution)/shard_map/ppermute | solution.py:516
  47.9 2.4 %collective-permute-start.13 = (bf16[256,512]{1,0:T(8,128)(2,1)S(1)}, bf16[256,512]{1,0:T(8,128)(2,1)S(1)}, u32[]{:S(2)}, u32[]{:S(2)}) collective-permute-start(bf16[256,512]{1,0:T(8,128)(2,1)S(1)} %collective-permute-done.12.refs_14_), channel_id=1, source_target_pairs={{0,2},{2,0},{4,6},{6,4},{8,10},{10,8},{12,14},{14,12},{16,18},{18,... | collective-permute-start | bytes 786440 | tf_op jit(solution)/shard_map/ppermute | solution.py:516
  51.6 3.0 %collective-permute-done.11.refs_13_ = bf16[256,512]{1,0:T(8,128)(2,1)S(1)} collective-permute-done((bf16[256,512]{1,0:T(8,128)(2,1)S(1)}, bf16[256,512]{1,0:T(8,128)(2,1)S(1)}, u32[]{:S(2)}, u32[]{:S(2)}) %collective-permute-start.11) | collective-permute-done | bytes 262176 | tf_op jit(solution)/shard_map/ppermute | solution.py:516
  54.6 3.8 %collective-permute-done.13.refs_15_ = bf16[256,512]{1,0:T(8,128)(2,1)S(1)} collective-permute-done((bf16[256,512]{1,0:T(8,128)(2,1)S(1)}, bf16[256,512]{1,0:T(8,128)(2,1)S(1)}, u32[]{:S(2)}, u32[]{:S(2)}) %collective-permute-start.13) | collective-permute-done | bytes 262176 | tf_op jit(solution)/shard_map/ppermute | solution.py:516
  58.4 1.5 %collective-permute-start.9 = (bf16[256,512]{1,0:T(8,128)(2,1)S(1)}, bf16[256,512]{1,0:T(8,128)(2,1)S(1)}, u32[]{:S(2)}, u32[]{:S(2)}) collective-permute-start(bf16[256,512]{1,0:T(8,128)(2,1)S(1)} %collective-permute-done.8.refs_10_), channel_id=1, source_target_pairs={{0,2},{1,3},{2,0},{3,1},{4,6},{5,7},{6,4},{7,5},{8,10},{9,11},{10,... | collective-permute-start | bytes 786440 | tf_op jit(solution)/shard_map/ppermute | solution.py:516
  60.1 7.0 %collective-permute-done.9.refs_11_ = bf16[256,512]{1,0:T(8,128)(2,1)S(1)} collective-permute-done((bf16[256,512]{1,0:T(8,128)(2,1)S(1)}, bf16[256,512]{1,0:T(8,128)(2,1)S(1)}, u32[]{:S(2)}, u32[]{:S(2)}) %collective-permute-start.9) | collective-permute-done | bytes 262176 | tf_op jit(solution)/shard_map/ppermute | solution.py:516
  67.1 1.5 %collective-permute-start.19 = (bf16[256,256]{1,0:T(8,128)(2,1)S(1)}, bf16[256,256]{1,0:T(8,128)(2,1)S(1)}, u32[]{:S(2)}, u32[]{:S(2)}) collective-permute-start(bf16[256,256]{1,0:T(8,128)(2,1)S(1)} %collective-permute-done.18.refs_6_), channel_id=1, source_target_pairs={{0,2},{1,3},{2,0},{3,1},{4,6},{5,7},{6,4},{7,5},{8,10},{9,11},{10,... | collective-permute-start | bytes 393224 | tf_op jit(solution)/shard_map/ppermute | solution.py:516
  69.1 3.4 %collective-permute-start.23 = (bf16[256,256]{1,0:T(8,128)(2,1)S(1)}, bf16[256,256]{1,0:T(8,128)(2,1)S(1)}, u32[]{:S(2)}, u32[]{:S(2)}) collective-permute-start(bf16[256,256]{1,0:T(8,128)(2,1)S(1)} %collective-permute-done.22.refs_10_), channel_id=1, source_target_pairs={{0,2},{2,0},{4,6},{6,4},{8,10},{10,8},{12,14},{14,12},{16,18},{18,... | collective-permute-start | bytes 393224 | tf_op jit(solution)/shard_map/ppermute | solution.py:516
  73.2 3.4 %state.1 = (f32[512,128]{1,0:T(8,128)S(1)}, bf16[512,128]{1,0:T(8,128)(2,1)S(1)}, bf16[512,128]{1,0:T(8,128)(2,1)S(1)}, bf16[288,128]{1,0:T(8,128)(2,1)S(1)}) custom-call(f32[2,128]{1,0:T(2,128)S(1)} %get-tuple-element.24.refs_0_, f32[2,128]{1,0:T(2,128)S(1)} %collective-permute-done.refs_1_, bf16[72,2048]{1,0:T(8,128)(2,1)S(1)} %get-tuple-element.26.refs_2_, ...), custom_call_target="tpu_custom_call" | custom-call | tf_op jit(solution)/shard_map/state/pallas_call | solution.py:538
  76.7 4.2 %collective-permute-start.17 = (bf16[288,128]{1,0:T(8,128)(2,1)S(1)}, bf16[288,128]{1,0:T(8,128)(2,1)S(1)}, u32[]{:S(2)}, u32[]{:S(2)}) collective-permute-start(bf16[288,128]{1,0:T(8,128)(2,1)S(1)} %get-tuple-element.34), channel_id=1, source_target_pairs={{0,16},{8,24},{1,17},{9,25},{2,18},{10,26},{3,19},{11,27},{4,20},{... | collective-permute-start | bytes 221192 | tf_op jit(solution)/shard_map/ppermute | solution.py:560
  80.9 1.9 %collective-permute-done.17.refs_5_ = bf16[288,128]{1,0:T(8,128)(2,1)S(1)} collective-permute-done((bf16[288,128]{1,0:T(8,128)(2,1)S(1)}, bf16[288,128]{1,0:T(8,128)(2,1)S(1)}, u32[]{:S(2)}, u32[]{:S(2)}) %collective-permute-start.17) | collective-permute-done | bytes 73760 | tf_op jit(solution)/shard_map/ppermute | solution.py:560
  82.8 2.2 %output.1 = (bf16[2,2,64,2048]{3,2,1,0:T(8,128)(2,1)S(1)}, bf16[2,2,64,2048]{3,2,1,0:T(8,128)(2,1)S(1)}) custom-call(f32[2,128]{1,0:T(2,128)S(1)} %get-tuple-element.24.refs_0_, f32[2,128]{1,0:T(2,128)S(1)} %collective-permute-done.refs_1_, f32[512,128]{1,0:T(8,128)S(1)} %get-tuple-element.31.refs_2_, bf16[512,128]{1,0:T(8,128)(2,1)S(1)} %get-tuple-element.32.refs_3_, ...), custom_call_target="tpu_custom_call" | custom-call | tf_op jit(solution)/shard_map/output/pallas_call | solution.py:566
  85.1 2.6 %collective-permute-done.26.refs_1_ = bf16[2,2,64,2048]{3,2,1,0:T(8,128)(2,1)S(1)} collective-permute-done((bf16[2,2,64,2048]{3,2,1,0:T(8,128)(2,1)S(1)}, bf16[2,2,64,2048]{3,2,1,0:T(8,128)(2,1)S(1)}, u32[]{:S(2)}, u32[]{:S(2)}) %collective-permute-start.26) | collective-permute-done | bytes 1048608 | tf_op jit(solution)/shard_map/ppermute | solution.py:53
  88.0 1.7 %collective-permute-start.27 = (bf16[64,2048]{1,0:T(8,128)(2,1)S(1)}, bf16[64,2048]{1,0:T(8,128)(2,1)S(1)}, u32[]{:S(2)}, u32[]{:S(2)}) collective-permute-start(bf16[64,2048]{1,0:T(8,128)(2,1)S(1)} %get-tuple-element.40), channel_id=1, source_target_pairs={{0,12},{2,14},{4,8},{6,10},{8,4},{10,6},{12,0},{14,2},{16,28},{18,... | collective-permute-start | bytes 786440 | tf_op jit(solution)/shard_map/ppermute | solution.py:595
  89.6 2.0 %collective-permute-start.28 = (bf16[64,2048]{1,0:T(8,128)(2,1)S(1)}, bf16[64,2048]{1,0:T(8,128)(2,1)S(1)}, u32[]{:S(2)}, u32[]{:S(2)}) collective-permute-start(bf16[64,2048]{1,0:T(8,128)(2,1)S(1)} %get-tuple-element.41), channel_id=1, source_target_pairs={{0,4},{2,6},{4,0},{6,2},{1,5},{3,7},{5,1},{7,3},{8,12},{10,14},{12... | collective-permute-start | bytes 786440 | tf_op jit(solution)/shard_map/ppermute | solution.py:53
  91.6 6.5 %collective-permute-done.27 = bf16[64,2048]{1,0:T(8,128)(2,1)S(1)} collective-permute-done((bf16[64,2048]{1,0:T(8,128)(2,1)S(1)}, bf16[64,2048]{1,0:T(8,128)(2,1)S(1)}, u32[]{:S(2)}, u32[]{:S(2)}) %collective-permute-start.27) | collective-permute-done | bytes 262176 | tf_op jit(solution)/shard_map/ppermute | solution.py:595
  98.1 4.7 %collective-permute-done.28 = bf16[64,2048]{1,0:T(8,128)(2,1)S(1)} collective-permute-done((bf16[64,2048]{1,0:T(8,128)(2,1)S(1)}, bf16[64,2048]{1,0:T(8,128)(2,1)S(1)}, u32[]{:S(2)}, u32[]{:S(2)}) %collective-permute-start.28) | collective-permute-done | bytes 262176 | tf_op jit(solution)/shard_map/ppermute | solution.py:53
  102.9 0.8 fusion
  (34 shorter events, 4.0 us)
Async XLA Ops:
  2.4 11.1 %collective-permute-start.18 = (bf16[256,256]{1,0:T(8,128)(2,1)S(1)}, bf16[256,256]{1,0:T(8,128)(2,1)S(1)}, u32[]{:S(2)}, u32[]{:S(2)}) collective-permute-start(bf16[256,256]{1,0:T(8,128)(2,1)S(1)} %get-tuple-element.35), channel_id=1, source_target_pairs={{16,0},{8,1},{25,8},{17,9},{0,16},{24,17},{9,24},{1,25},{18,2},{10... | collective-permute-start | bytes 393224 | tf_op jit(solution)/shard_map/ppermute | solution.py:512
  6.5 8.3 %collective-permute-start.20 = (bf16[256,256]{1,0:T(8,128)(2,1)S(1)}, bf16[256,256]{1,0:T(8,128)(2,1)S(1)}, u32[]{:S(2)}, u32[]{:S(2)}) collective-permute-start(bf16[256,256]{1,0:T(8,128)(2,1)S(1)} %get-tuple-element.36), channel_id=1, source_target_pairs={{16,1},{8,0},{25,9},{17,8},{0,17},{24,16},{9,25},{1,24},{18,3},{10... | collective-permute-start | bytes 393224 | tf_op jit(solution)/shard_map/ppermute | solution.py:512
  7.8 26.2 %collective-permute-start.10 = (bf16[256,512]{1,0:T(8,128)(2,1)S(1)}, bf16[256,512]{1,0:T(8,128)(2,1)S(1)}, u32[]{:S(2)}, u32[]{:S(2)}) collective-permute-start(bf16[256,512]{1,0:T(8,128)(2,1)S(1)} %get-tuple-element.28), channel_id=1, source_target_pairs={{16,1},{8,0},{25,9},{17,8},{0,17},{24,16},{9,25},{1,24},{18,3},{10... | collective-permute-start | bytes 786440 | tf_op jit(solution)/shard_map/ppermute | solution.py:512
  8.1 25.9 %collective-permute-start.12 = (bf16[256,512]{1,0:T(8,128)(2,1)S(1)}, bf16[256,512]{1,0:T(8,128)(2,1)S(1)}, u32[]{:S(2)}, u32[]{:S(2)}) collective-permute-start(bf16[256,512]{1,0:T(8,128)(2,1)S(1)} %get-tuple-element.28), channel_id=1, source_target_pairs={{24,0},{1,8},{8,16},{17,24},{26,2},{3,10},{10,18},{19,26},{28,4},{... | collective-permute-start | bytes 786440 | tf_op jit(solution)/shard_map/ppermute | solution.py:512
  9.3 3.4 %collective-permute-start = (f32[2,128]{1,0:T(2,128)S(1)}, f32[2,128]{1,0:T(2,128)S(1)}, u32[]{:S(2)}, u32[]{:S(2)}) collective-permute-start(f32[2,128]{1,0:T(2,128)S(1)} %get-tuple-element.25), channel_id=1, source_target_pairs={{0,1},{1,0},{2,3},{3,2},{4,5},{5,4},{6,7},{7,6},{8,9},{9,8},{10,11... | collective-permute-start | bytes 3080 | tf_op jit(solution)/shard_map/ppermute | solution.py:53
  12.8 24.1 %collective-permute-start.14 = (bf16[256,512]{1,0:T(8,128)(2,1)S(1)}, bf16[256,512]{1,0:T(8,128)(2,1)S(1)}, u32[]{:S(2)}, u32[]{:S(2)}) collective-permute-start(bf16[256,512]{1,0:T(8,128)(2,1)S(1)} %get-tuple-element.27), channel_id=1, source_target_pairs={{24,1},{1,9},{8,17},{17,25},{26,3},{3,11},{10,19},{19,27},{28,5},{... | collective-permute-start | bytes 786440 | tf_op jit(solution)/shard_map/ppermute | solution.py:512
  13.5 16.5 %collective-permute-start.22 = (bf16[256,256]{1,0:T(8,128)(2,1)S(1)}, bf16[256,256]{1,0:T(8,128)(2,1)S(1)}, u32[]{:S(2)}, u32[]{:S(2)}) collective-permute-start(bf16[256,256]{1,0:T(8,128)(2,1)S(1)} %get-tuple-element.36), channel_id=1, source_target_pairs={{24,0},{1,8},{8,16},{17,24},{26,2},{3,10},{10,18},{19,26},{28,4},{... | collective-permute-start | bytes 393224 | tf_op jit(solution)/shard_map/ppermute | solution.py:512
  14.8 17.7 %collective-permute-start.24 = (bf16[256,256]{1,0:T(8,128)(2,1)S(1)}, bf16[256,256]{1,0:T(8,128)(2,1)S(1)}, u32[]{:S(2)}, u32[]{:S(2)}) collective-permute-start(bf16[256,256]{1,0:T(8,128)(2,1)S(1)} %get-tuple-element.35), channel_id=1, source_target_pairs={{24,1},{1,9},{8,17},{17,25},{26,3},{3,11},{10,19},{19,27},{28,5},{... | collective-permute-start | bytes 393224 | tf_op jit(solution)/shard_map/ppermute | solution.py:512
  30.0 17.8 %collective-permute-start.4 = (bf16[72,2048]{1,0:T(8,128)(2,1)S(1)}, bf16[72,2048]{1,0:T(8,128)(2,1)S(1)}, u32[]{:S(2)}, u32[]{:S(2)}) collective-permute-start(bf16[72,2048]{1,0:T(8,128)(2,1)S(1)} %get-tuple-element.26.refs_2_), channel_id=1, source_target_pairs={{0,8},{8,0},{16,24},{24,16},{1,9},{9,1},{17,25},{25,17},{2,10},{10... | collective-permute-start | bytes 884744 | tf_op jit(solution)/shard_map/ppermute | solution.py:53
  32.5 17.8 %collective-permute-start.2 = (bf16[72,2048]{1,0:T(8,128)(2,1)S(1)}, bf16[72,2048]{1,0:T(8,128)(2,1)S(1)}, u32[]{:S(2)}, u32[]{:S(2)}) collective-permute-start(bf16[72,2048]{1,0:T(8,128)(2,1)S(1)} %get-tuple-element.26.refs_2_), channel_id=1, source_target_pairs={{0,4},{2,6},{4,0},{6,2},{1,5},{3,7},{5,1},{7,3},{8,12},{10,14},{12... | collective-permute-start | bytes 884744 | tf_op jit(solution)/shard_map/ppermute | solution.py:53
  34.0 16.9 %collective-permute-start.1 = (bf16[72,2048]{1,0:T(8,128)(2,1)S(1)}, bf16[72,2048]{1,0:T(8,128)(2,1)S(1)}, u32[]{:S(2)}, u32[]{:S(2)}) collective-permute-start(bf16[72,2048]{1,0:T(8,128)(2,1)S(1)} %get-tuple-element.26.refs_2_), channel_id=1, source_target_pairs={{0,1},{1,0},{2,3},{3,2},{4,5},{5,4},{6,7},{7,6},{8,9},{9,8},{10,11... | collective-permute-start | bytes 884744 | tf_op jit(solution)/shard_map/ppermute | solution.py:53
  34.0 12.4 %collective-permute-start.8 = (bf16[256,512]{1,0:T(8,128)(2,1)S(1)}, bf16[256,512]{1,0:T(8,128)(2,1)S(1)}, u32[]{:S(2)}, u32[]{:S(2)}) collective-permute-start(bf16[256,512]{1,0:T(8,128)(2,1)S(1)} %get-tuple-element.27), channel_id=1, source_target_pairs={{16,0},{8,1},{25,8},{17,9},{0,16},{24,17},{9,24},{1,25},{18,2},{10... | collective-permute-start | bytes 786440 | tf_op jit(solution)/shard_map/ppermute | solution.py:512
  36.9 35.7 %collective-permute-start.16 = (bf16[768,512]{1,0:T(8,128)(2,1)S(1)}, bf16[768,512]{1,0:T(8,128)(2,1)S(1)}, u32[]{:S(2)}, u32[]{:S(2)}) collective-permute-start(bf16[768,512]{1,0:T(8,128)(2,1)S(1)} %get-tuple-element.30), channel_id=1, source_target_pairs={{0,1},{1,0},{2,3},{3,2},{4,5},{5,4},{6,7},{7,6},{8,9},{9,8},{10,11... | collective-permute-start | bytes 2359304 | tf_op jit(solution)/shard_map/ppermute | solution.py:53
  46.4 8.2 %collective-permute-start.11 = (bf16[256,512]{1,0:T(8,128)(2,1)S(1)}, bf16[256,512]{1,0:T(8,128)(2,1)S(1)}, u32[]{:S(2)}, u32[]{:S(2)}) collective-permute-start(bf16[256,512]{1,0:T(8,128)(2,1)S(1)} %collective-permute-done.10.refs_12_), channel_id=1, source_target_pairs={{0,2},{1,3},{2,0},{3,1},{4,6},{5,7},{6,4},{7,5},{8,10},{9,11},{10,... | collective-permute-start | bytes 786440 | tf_op jit(solution)/shard_map/ppermute | solution.py:516
  47.9 10.5 %collective-permute-start.13 = (bf16[256,512]{1,0:T(8,128)(2,1)S(1)}, bf16[256,512]{1,0:T(8,128)(2,1)S(1)}, u32[]{:S(2)}, u32[]{:S(2)}) collective-permute-start(bf16[256,512]{1,0:T(8,128)(2,1)S(1)} %collective-permute-done.12.refs_14_), channel_id=1, source_target_pairs={{0,2},{2,0},{4,6},{6,4},{8,10},{10,8},{12,14},{14,12},{16,18},{18,... | collective-permute-start | bytes 786440 | tf_op jit(solution)/shard_map/ppermute | solution.py:516
  50.3 9.5 %collective-permute-start.6 = (bf16[72,2048]{1,0:T(8,128)(2,1)S(1)}, bf16[72,2048]{1,0:T(8,128)(2,1)S(1)}, u32[]{:S(2)}, u32[]{:S(2)}) collective-permute-start(bf16[72,2048]{1,0:T(8,128)(2,1)S(1)} %collective-permute-done.4.refs_6_), channel_id=1, source_target_pairs={{0,4},{2,6},{4,0},{6,2},{1,5},{3,7},{5,1},{7,3},{8,12},{10,14},{12... | collective-permute-start | bytes 884744 | tf_op jit(solution)/shard_map/ppermute | solution.py:53
  50.9 7.5 %collective-permute-start.15 = (bf16[256,512]{1,0:T(8,128)(2,1)S(1)}, bf16[256,512]{1,0:T(8,128)(2,1)S(1)}, u32[]{:S(2)}, u32[]{:S(2)}) collective-permute-start(bf16[256,512]{1,0:T(8,128)(2,1)S(1)} %collective-permute-done.14.refs_16_), channel_id=1, source_target_pairs={{1,3},{3,1},{5,7},{7,5},{9,11},{11,9},{13,15},{15,13},{17,19},{19,... | collective-permute-start | bytes 786440 | tf_op jit(solution)/shard_map/ppermute | solution.py:516
  54.6 14.0 %collective-permute-start.5 = (bf16[72,2048]{1,0:T(8,128)(2,1)S(1)}, bf16[72,2048]{1,0:T(8,128)(2,1)S(1)}, u32[]{:S(2)}, u32[]{:S(2)}) collective-permute-start(bf16[72,2048]{1,0:T(8,128)(2,1)S(1)} %collective-permute-done.4.refs_6_), channel_id=1, source_target_pairs={{0,1},{1,0},{2,3},{3,2},{4,5},{5,4},{6,7},{7,6},{8,9},{9,8},{10,11... | collective-permute-start | bytes 884744 | tf_op jit(solution)/shard_map/ppermute | solution.py:53
  58.3 10.8 %collective-permute-start.3 = (bf16[72,2048]{1,0:T(8,128)(2,1)S(1)}, bf16[72,2048]{1,0:T(8,128)(2,1)S(1)}, u32[]{:S(2)}, u32[]{:S(2)}) collective-permute-start(bf16[72,2048]{1,0:T(8,128)(2,1)S(1)} %collective-permute-done.2.refs_4_), channel_id=1, source_target_pairs={{0,1},{1,0},{2,3},{3,2},{4,5},{5,4},{6,7},{7,6},{8,9},{9,8},{10,11... | collective-permute-start | bytes 884744 | tf_op jit(solution)/shard_map/ppermute | solution.py:53
  58.4 8.7 %collective-permute-start.9 = (bf16[256,512]{1,0:T(8,128)(2,1)S(1)}, bf16[256,512]{1,0:T(8,128)(2,1)S(1)}, u32[]{:S(2)}, u32[]{:S(2)}) collective-permute-start(bf16[256,512]{1,0:T(8,128)(2,1)S(1)} %collective-permute-done.8.refs_10_), channel_id=1, source_target_pairs={{0,2},{1,3},{2,0},{3,1},{4,6},{5,7},{6,4},{7,5},{8,10},{9,11},{10,... | collective-permute-start | bytes 786440 | tf_op jit(solution)/shard_map/ppermute | solution.py:516
  59.8 13.3 %collective-permute-start.7 = (bf16[72,2048]{1,0:T(8,128)(2,1)S(1)}, bf16[72,2048]{1,0:T(8,128)(2,1)S(1)}, u32[]{:S(2)}, u32[]{:S(2)}) collective-permute-start(bf16[72,2048]{1,0:T(8,128)(2,1)S(1)} %collective-permute-done.6.refs_8_), channel_id=1, source_target_pairs={{0,1},{1,0},{2,3},{3,2},{4,5},{5,4},{6,7},{7,6},{8,9},{9,8},{10,11... | collective-permute-start | bytes 884744 | tf_op jit(solution)/shard_map/ppermute | solution.py:53
  67.1 13.8 %collective-permute-start.19 = (bf16[256,256]{1,0:T(8,128)(2,1)S(1)}, bf16[256,256]{1,0:T(8,128)(2,1)S(1)}, u32[]{:S(2)}, u32[]{:S(2)}) collective-permute-start(bf16[256,256]{1,0:T(8,128)(2,1)S(1)} %collective-permute-done.18.refs_6_), channel_id=1, source_target_pairs={{0,2},{1,3},{2,0},{3,1},{4,6},{5,7},{6,4},{7,5},{8,10},{9,11},{10,... | collective-permute-start | bytes 393224 | tf_op jit(solution)/shard_map/ppermute | solution.py:516
  68.6 12.3 %collective-permute-start.21 = (bf16[256,256]{1,0:T(8,128)(2,1)S(1)}, bf16[256,256]{1,0:T(8,128)(2,1)S(1)}, u32[]{:S(2)}, u32[]{:S(2)}) collective-permute-start(bf16[256,256]{1,0:T(8,128)(2,1)S(1)} %collective-permute-done.20.refs_8_), channel_id=1, source_target_pairs={{0,2},{1,3},{2,0},{3,1},{4,6},{5,7},{6,4},{7,5},{8,10},{9,11},{10,... | collective-permute-start | bytes 393224 | tf_op jit(solution)/shard_map/ppermute | solution.py:516
  69.1 11.8 %collective-permute-start.23 = (bf16[256,256]{1,0:T(8,128)(2,1)S(1)}, bf16[256,256]{1,0:T(8,128)(2,1)S(1)}, u32[]{:S(2)}, u32[]{:S(2)}) collective-permute-start(bf16[256,256]{1,0:T(8,128)(2,1)S(1)} %collective-permute-done.22.refs_10_), channel_id=1, source_target_pairs={{0,2},{2,0},{4,6},{6,4},{8,10},{10,8},{12,14},{14,12},{16,18},{18,... | collective-permute-start | bytes 393224 | tf_op jit(solution)/shard_map/ppermute | solution.py:516
  72.5 8.4 %collective-permute-start.25 = (bf16[256,256]{1,0:T(8,128)(2,1)S(1)}, bf16[256,256]{1,0:T(8,128)(2,1)S(1)}, u32[]{:S(2)}, u32[]{:S(2)}) collective-permute-start(bf16[256,256]{1,0:T(8,128)(2,1)S(1)} %collective-permute-done.24.refs_12_), channel_id=1, source_target_pairs={{1,3},{3,1},{5,7},{7,5},{9,11},{11,9},{13,15},{15,13},{17,19},{19,... | collective-permute-start | bytes 393224 | tf_op jit(solution)/shard_map/ppermute | solution.py:516
  76.7 6.2 %collective-permute-start.17 = (bf16[288,128]{1,0:T(8,128)(2,1)S(1)}, bf16[288,128]{1,0:T(8,128)(2,1)S(1)}, u32[]{:S(2)}, u32[]{:S(2)}) collective-permute-start(bf16[288,128]{1,0:T(8,128)(2,1)S(1)} %get-tuple-element.34), channel_id=1, source_target_pairs={{0,16},{8,24},{1,17},{9,25},{2,18},{10,26},{3,19},{11,27},{4,20},{... | collective-permute-start | bytes 221192 | tf_op jit(solution)/shard_map/ppermute | solution.py:560
  85.0 2.7 %collective-permute-start.26 = (bf16[2,2,64,2048]{3,2,1,0:T(8,128)(2,1)S(1)}, bf16[2,2,64,2048]{3,2,1,0:T(8,128)(2,1)S(1)}, u32[]{:S(2)}, u32[]{:S(2)}) collective-permute-start(bf16[2,2,64,2048]{3,2,1,0:T(8,128)(2,1)S(1)} %get-tuple-element.38), channel_id=1, source_target_pairs={{0,1},{1,0},{2,3},{3,2},{4,5},{5,4},{6,7},{7,6},{8,9},{9,8},{10,11... | collective-permute-start | bytes 3145736 | tf_op jit(solution)/shard_map/ppermute | solution.py:53
  88.0 10.2 %collective-permute-start.27 = (bf16[64,2048]{1,0:T(8,128)(2,1)S(1)}, bf16[64,2048]{1,0:T(8,128)(2,1)S(1)}, u32[]{:S(2)}, u32[]{:S(2)}) collective-permute-start(bf16[64,2048]{1,0:T(8,128)(2,1)S(1)} %get-tuple-element.40), channel_id=1, source_target_pairs={{0,12},{2,14},{4,8},{6,10},{8,4},{10,6},{12,0},{14,2},{16,28},{18,... | collective-permute-start | bytes 786440 | tf_op jit(solution)/shard_map/ppermute | solution.py:595
  89.6 13.3 %collective-permute-start.28 = (bf16[64,2048]{1,0:T(8,128)(2,1)S(1)}, bf16[64,2048]{1,0:T(8,128)(2,1)S(1)}, u32[]{:S(2)}, u32[]{:S(2)}) collective-permute-start(bf16[64,2048]{1,0:T(8,128)(2,1)S(1)} %get-tuple-element.41), channel_id=1, source_target_pairs={{0,4},{2,6},{4,0},{6,2},{1,5},{3,7},{5,1},{7,3},{8,12},{10,14},{12... | collective-permute-start | bytes 786440 | tf_op jit(solution)/shard_map/ppermute | solution.py:53
  91.6 11.3 %collective-permute-start.29 = (bf16[64,2048]{1,0:T(8,128)(2,1)S(1)}, bf16[64,2048]{1,0:T(8,128)(2,1)S(1)}, u32[]{:S(2)}, u32[]{:S(2)}) collective-permute-start(bf16[64,2048]{1,0:T(8,128)(2,1)S(1)} %get-tuple-element.42), channel_id=1, source_target_pairs={{0,8},{8,0},{16,24},{24,16},{1,9},{9,1},{17,25},{25,17},{2,10},{10... | collective-permute-start | bytes 786440 | tf_op jit(solution)/shard_map/ppermute | solution.py:53
